TPU v7x, 512 devices: a whole 4x4x16 slice. The times are simulated.
512 devices in a mesh: kv: 16 (over y, x), tp: 32 (over z, core).
Axes of the slice: x: 4, y: 4, z: 16, core: 2. Of those that a mesh axis runs over, the one named last changes fastest.
Arguments:
- residual: bfloat16 [512, 2048], P('tp', 'kv'), may hold values from -64 to 64
- prior_state: float32 [512, 16, 128, 128], P('tp', 'kv'), may hold values from -6 to 6
- w_query: bfloat16 [2048, 2048], P('tp', 'kv'), may hold values from -0.125 to 0.125
- w_forget: bfloat16 [2048, 2048], P('tp', 'kv'), may hold values from -0.125 to 0.125
- w_value: bfloat16 [2048, 2048], P('tp', 'kv'), may hold values from -0.125 to 0.125
- w_outgate: bfloat16 [2048, 2048], P('tp', 'kv'), may hold values from -0.125 to 0.125
- forget_floor: float32 [2048], P('kv'), may hold values from 0.05 to 0.9
- group_gain: float32 [2048], P('kv'), may hold values from 0.1 to 1.9
- w_mix_out: bfloat16 [2048, 2048], P('kv', 'tp'), may hold values from -0.397747564 to 0.397747564
- gain_mix_pre: float32 [2048], replicated, may hold values from 0.1 to 1.9
- gain_mix_post: float32 [2048], replicated, may hold values from 0.05 to 1.9
- gain_mlp_pre: float32 [2048], replicated, may hold values from 0.1 to 1.9
- gain_mlp_post: float32 [2048], replicated, may hold values from 0.1 to 1.9
- w_up: bfloat16 [2048, 8192], P('tp', 'kv'), may hold values from -0.125 to 0.125
- w_down: bfloat16 [8192, 2048], P('kv', 'tp'), may hold values from -0.198873782 to 0.198873782
Outputs:
- layer_out: bfloat16 [512, 2048], P('tp', 'kv')
- new_state: float32 [512, 16, 128, 128], P('tp', 'kv')
All inputs are finite; a program needn't handle non-finite values.
Results may differ from a plain program's by a relative error of at most 0.015.
Values may be sent and summed in bfloat16 or wider, within the bound.
No kernel may reach another device: no remote copies, remote signals or barrier semaphores. Data moves between devices by JAX's collectives and lax.ppermute only.
A program may use at most 64 MiB of HBM per device.

v0:
```python
import jax
import jax.numpy as jnp
from jax import lax
from jax.experimental import pallas as pl
from jax.experimental.pallas import tpu as pltpu
from jax.sharding import Mesh
from jax.sharding import PartitionSpec as P

KV = ("y", "x")
TP = ("zh", "zo", "c")
HALVES = 2
CHIPS = 8
CORES = 2
EARLY = 48

epsilon = 1e-06


def exchange(blocks, axes):
    return lax.all_to_all(blocks, axes, 0, 0, tiled=True)


def pack_body(
    residual, wq, wf, wv, wg, mix, up, down, early_ref, late_ref, mlp_ref, spread_ref, sems
):
    rows, cols = wq.shape
    rest = rows - EARLY
    part = mix.shape[0] // 4
    hidden = up.shape[1]
    copies = [
        (up, mlp_ref.at[:, :hidden]),
        (down, mlp_ref.at[:, hidden:]),
    ]
    for k, w in enumerate((wq, wf, wv, wg)):
        at = slice(k * cols, (k + 1) * cols)
        copies.append((w.at[:EARLY], early_ref.at[:, at]))
        copies.append((w.at[EARLY:], late_ref.at[:rest, at]))
        copies.append((mix.at[k * part : (k + 1) * part], late_ref.at[rest:, at]))
    started = [
        pltpu.make_async_copy(src, dst, sems.at[k]) for k, (src, dst) in enumerate(copies)
    ]
    for copy in started:
        copy.start()
    spread_ref[...] = jnp.broadcast_to(residual[...][None], spread_ref.shape)
    for copy in started:
        copy.wait()


def pack(residual, wq, wf, wv, wg, mix, up, down, peers):
    rows, cols = wq.shape
    late = rows - EARLY + mix.shape[0] // 4
    anywhere = pl.BlockSpec(memory_space=pl.ANY)
    vmem = pl.BlockSpec(memory_space=pltpu.VMEM)
    return pl.pallas_call(
        pack_body,
        out_shape=(
            jax.ShapeDtypeStruct((EARLY, 4 * cols), wq.dtype),
            jax.ShapeDtypeStruct((late, 4 * cols), wq.dtype),
            jax.ShapeDtypeStruct((rows, up.shape[1] + down.shape[1]), wq.dtype),
            jax.ShapeDtypeStruct((peers, *residual.shape), residual.dtype),
        ),
        in_specs=[vmem] + [anywhere] * 7,
        out_specs=(vmem, vmem, vmem, vmem),
        scratch_shapes=[pltpu.SemaphoreType.DMA((14,))],
        name="pack",
    )(residual, wq, wf, wv, wg, mix, up, down)


def project_body(x_ref, gain_ref, early_ref, late_ref, own_ref, send_ref):
    zo = lax.axis_index("zo")
    groups, _, height, width = x_ref.shape
    rest = late_ref.shape[2] // 2
    squares = [None] * HALVES
    for f in range(groups):
        for h in range(HALVES):
            x = x_ref[f, h].astype(jnp.float32)
            squares[h] = x * x if f == 0 else squares[h] + x * x
    scale = [
        lax.rsqrt(jnp.sum(s, axis=-1, keepdims=True) / (groups * width) + epsilon)
        for s in squares
    ]
    total = None
    for k in range(CHIPS):
        f = HALVES * k + zo
        gain = gain_ref[pl.ds(f, 1)]
        x = jnp.concatenate(
            [
                (x_ref[f, h].astype(jnp.float32) * scale[h] * gain).astype(jnp.bfloat16)
                for h in range(HALVES)
            ],
            axis=0,
        )
        w = jnp.concatenate(
            [
                piece
                for c in range(CORES)
                for piece in (early_ref[k, c], late_ref[k, c, :rest])
            ],
            axis=0,
        )
        term = jnp.dot(x, w, preferred_element_type=jnp.float32)
        total = term if total is None else total + term
    mine = jnp.where(zo == 0, total[:height], total[height:])
    other = jnp.where(zo == 0, total[height:], total[:height])
    own_ref[...] = mine
    send_ref[...] = other.astype(send_ref.dtype)


def project(x, gain, early, late):
    height = x.shape[2]
    cols = early.shape[3]
    return pl.pallas_call(
        project_body,
        out_shape=(
            jax.ShapeDtypeStruct((height, cols), jnp.float32),
            jax.ShapeDtypeStruct((height, cols), jnp.bfloat16),
        ),
        name="project",
    )(x, gain, early, late)


def recur_body(
    own_ref, part_ref, prior_ref, floor_ref, gain_ref, state_ref, out_ref, read_ref
):
    zo = lax.axis_index("zo")
    pre = own_ref[...] + part_ref[1 - zo].astype(jnp.float32)
    pre = pre.astype(jnp.bfloat16).astype(jnp.float32)
    width = prior_ref.shape[1]
    query = jax.nn.silu(pre[:, :width])
    floor = floor_ref[...]
    forget = floor + (1.0 - floor) * jax.nn.sigmoid(pre[:, width : 2 * width])
    value = pre[:, 2 * width : 3 * width]
    gate = jax.nn.sigmoid(pre[:, 3 * width :])
    forget_t = forget.T
    query_t = query.T
    for b in range(prior_ref.shape[0]):
        keep = forget_t[:, b : b + 1]
        state = keep * prior_ref[b] + (1.0 - keep) * value[b : b + 1]
        state_ref[b] = state
        read_ref[b : b + 1] = jnp.sum(query_t[:, b : b + 1] * state, axis=0, keepdims=True)
    read = read_ref[...]
    scale = lax.rsqrt(jnp.mean(read * read, axis=-1, keepdims=True) + epsilon)
    out_ref[...] = (read * scale * gain_ref[...] * gate).astype(out_ref.dtype)


def recur(own, part, prior, floor, gain):
    rows, width, _ = prior.shape
    return pl.pallas_call(
        recur_body,
        out_shape=(
            jax.ShapeDtypeStruct(prior.shape, jnp.float32),
            jax.ShapeDtypeStruct((rows, width), jnp.bfloat16),
        ),
        scratch_shapes=[pltpu.VMEM((rows, width), jnp.float32)],
        name="recur",
    )(own, part, prior, floor, gain)


def mix_body(gated_ref, late_ref, out_ref, order_ref):
    height, width = gated_ref.shape[1:]
    rest = late_ref.shape[2] // 2
    for h in range(HALVES):
        order_ref[pl.ds(h, height, stride=HALVES)] = gated_ref[h].astype(jnp.float32)
    left = order_ref[...].astype(jnp.bfloat16)
    for k in range(CHIPS):
        right = jnp.concatenate(
            [
                late_ref[k, c, rest:, j * width : (j + 1) * width]
                for c in range(CORES)
                for j in range(4)
            ],
            axis=0,
        )
        out_ref[pl.ds(k, HALVES * height, stride=CHIPS)] = lax.dot_general(
            left, right, (((1,), (1,)), ((), ())), preferred_element_type=jnp.float32
        )


def mix_out(gated, late):
    height, width = gated.shape[1:]
    return pl.pallas_call(
        mix_body,
        out_shape=jax.ShapeDtypeStruct((CHIPS * HALVES * height, width), jnp.float32),
        scratch_shapes=[pltpu.VMEM((HALVES * height, width), jnp.float32)],
        name="mix_out",
    )(gated, late)


def row_body(sums_ref, x_ref, gain_ref, out_ref, mixed_ref):
    zo = lax.axis_index("zo")
    place = lax.axis_index("y") * lax.axis_size("x") + lax.axis_index("x")
    groups, width = gain_ref.shape
    for h in range(HALVES):
        total = sums_ref[0, h]
        for k in range(1, groups):
            total = total + sums_ref[k, h]
        mixed_ref[pl.ds(h, CHIPS, stride=HALVES)] = total
    mixed = mixed_ref[...]
    scale = lax.rsqrt(jnp.sum(mixed * mixed) / gain_ref.size + epsilon)
    stream = x_ref[:, zo].astype(jnp.float32)
    at = lax.broadcasted_iota(jnp.int32, stream.shape, 1) == place
    row = jnp.sum(jnp.where(at, stream, 0.0), axis=1)
    after = (row + mixed * scale * gain_ref[...]).astype(out_ref.dtype)
    out_ref[...] = jnp.broadcast_to(after[None], out_ref.shape)


def row_update(sums, x, gain):
    groups, width = gain.shape
    return pl.pallas_call(
        row_body,
        out_shape=jax.ShapeDtypeStruct((groups, groups, width), jnp.bfloat16),
        scratch_shapes=[pltpu.VMEM((groups, width), jnp.float32)],
        name="row_update",
    )(sums, x, gain)


def shards(
    residual,
    prior_state,
    w_query,
    w_forget,
    w_value,
    w_outgate,
    forget_floor,
    group_gain,
    w_mix_out,
    gain_mix_pre,
    gain_mix_post,
    gain_mlp_pre,
    gain_mlp_post,
    w_up,
    w_down,
):
    batch_rows, own_cols = residual.shape
    groups = lax.axis_size(KV)
    full_width = groups * own_cols
    place = lax.axis_index(KV)
    hidden = w_up.shape[1]

    early, late, mlp, spread = pack(
        residual,
        w_query,
        w_forget,
        w_value,
        w_outgate,
        w_mix_out.T,
        w_up,
        w_down.T,
        groups * HALVES,
    )
    mlp_weights = lax.all_gather(mlp, TP, axis=0, tiled=True)
    stream = exchange(spread, (*KV, "zo")).reshape(groups, HALVES, batch_rows, own_cols)
    early = lax.all_gather(early, ("zh", "c"), axis=0).reshape(CHIPS, CORES, *early.shape)
    late = lax.all_gather(late, ("zh", "c"), axis=0).reshape(CHIPS, CORES, *late.shape)
    own, send = project(stream, gain_mix_pre.reshape(groups, own_cols), early, late)
    part = lax.all_gather(send, "zo", axis=0)
    new_state, gated = recur(
        own, part, prior_state[:, 0], forget_floor[None], group_gain[None]
    )
    gated = lax.all_gather(gated, "zo", axis=0)
    mixed_part = mix_out(gated, late).reshape(groups * HALVES, CHIPS, own_cols)
    mixed = exchange(mixed_part, (*KV, "zo")).reshape(groups, HALVES, CHIPS, own_cols)
    after_row = row_update(mixed, stream, gain_mix_post.reshape(groups, own_cols))
    after = exchange(after_row, KV).astype(jnp.float32)
    after_scale = lax.rsqrt(
        jnp.sum(after * after, axis=(1, 2), keepdims=True) / full_width + epsilon
    )
    hidden_in = (after * after_scale * gain_mlp_pre.reshape(groups, own_cols)).astype(
        jnp.bfloat16
    )
    up_sum = jnp.dot(
        hidden_in.reshape(batch_rows, full_width),
        mlp_weights[:, :hidden],
        preferred_element_type=jnp.float32,
    )
    squared = jnp.square(jax.nn.relu(up_sum)).astype(jnp.bfloat16)
    channel_part = lax.dot_general(
        squared,
        mlp_weights[:, hidden:],
        (((1,), (1,)), ((), ())),
        preferred_element_type=jnp.float32,
    )
    channel = exchange(
        channel_part.astype(jnp.bfloat16)
        .reshape(batch_rows, groups, own_cols)
        .transpose(1, 0, 2),
        KV,
    )
    channel = jnp.sum(channel.astype(jnp.float32), axis=0)
    out_gain = lax.dynamic_index_in_dim(
        gain_mlp_post.reshape(groups, own_cols), place, 0, keepdims=True
    )
    after_own = lax.dynamic_index_in_dim(after, place, 1, keepdims=False)
    layer_out = (after_own + channel * out_gain).astype(jnp.bfloat16)
    return layer_out, new_state[:, None]


def solution(mesh):
    grid = Mesh(mesh.devices.reshape(4, 4, CHIPS, HALVES, CORES), (*KV, *TP))
    return jax.shard_map(
        shards,
        mesh=grid,
        in_specs=(
            P(TP, KV),
            P(TP, KV, None, None),
            P(TP, KV),
            P(TP, KV),
            P(TP, KV),
            P(TP, KV),
            P(KV),
            P(KV),
            P(KV, TP),
            P(),
            P(),
            P(),
            P(),
            P(TP, KV),
            P(KV, TP),
        ),
        out_specs=(P(TP, KV), P(TP, KV, None, None)),
        check_vma=False,
    )
```

profile of v0, /device:TPU:2, one launch (start us, length us, event | category | flops | bytes accessed | tf_op | source)
XLA Modules:
  0.0 143.8 jit_solution(4906337983012045118)
XLA Ops:
  7.2 0.0 copy-start
  7.2 0.0 copy-start.3
  7.2 0.0 all-gather.6.cloned.1.call-start
  7.2 2.4 %pack.1 = (bf16[48,512]{1,0:T(8,128)(2,1)}, bf16[32,512]{1,0:T(8,128)(2,1)}, bf16[64,1024]{1,0:T(8,128)(2,1)}, bf16[32,16,128]{2,1,0:T(8,128)(2,1)}) custom-call(bf16[16,128]{1,0:T(8,128)(2,1)} %residual.1, bf16[64,128]{1,0:T(8,128)(2,1)} %wq.1, bf16[64,128]{1,0:T(8,128)(2,1)} %wf.1, bf16[64,128]{1,0:T(8,128)(2,1)} %wv.1, bf16[64,128]{1,0:T(8,128)(2,1)} %wg.1, ...), custom_call_target="tpu_custom_call" | custom-call | tf_op jit(solution)/shard_map/pack/pallas_call | solution.py:54
  9.7 0.0 all-gather.6.cloned.1.call-update
  9.7 9.4 %all-to-all-start = ((bf16[32,16,128]{2,1,0:T(8,128)(2,1)}), bf16[32,16,128]{2,1,0:T(8,128)(2,1)S(1)}, u32[]{:S(2)}, u32[]{:S(2)}) async-start(bf16[32,16,128]{2,1,0:T(8,128)(2,1)} %get-tuple-element.10), calls=%async_computation | async-start | bytes 262144 | tf_op jit(solution)/shard_map/all_to_all | solution.py:20
  19.1 28.3 %all-gather.1 = bf16[512,512]{1,0:T(8,128)(2,1)} all-gather(bf16[32,512]{1,0:T(8,128)(2,1)} %get-tuple-element.12), channel_id=3, replica_groups=mesh['y'=4,'x'=4,'zh'=8,'zo'=2,'c'=2] {'zh','c'}, dimensions={0}, use_global_device_ids=true | all-gather | bytes 557056 | tf_op jit(solution)/shard_map/all_gather | solution.py:254
  47.4 23.2 %all-gather = bf16[768,512]{1,0:T(8,128)(2,1)} all-gather(bf16[48,512]{1,0:T(8,128)(2,1)} %get-tuple-element.11), channel_id=2, replica_groups=mesh['y'=4,'x'=4,'zh'=8,'zo'=2,'c'=2] {'zh','c'}, dimensions={0}, use_global_device_ids=true | all-gather | bytes 835584 | tf_op jit(solution)/shard_map/all_gather | solution.py:253
  70.6 0.0 all-to-all-done
  70.6 0.0 copy-start.1
  70.6 0.7 copy-done.1
  71.3 2.3 %project.1 = (f32[16,512]{1,0:T(8,128)}, bf16[16,512]{1,0:T(8,128)(2,1)}) custom-call(bf16[16,2,16,128]{3,2,1,0:T(8,128)(2,1)} %bitcast.39, f32[16,128]{1,0:T(8,128)} %bitcast.50, bf16[8,2,48,512]{3,2,1,0:T(8,128)(2,1)} %bitcast.38, bf16[8,2,32,512]{3,2,1,0:T(8,128)(2,1)} %bitcast.36), custom_call_target="tpu_custom_call" | custom-call | tf_op jit(solution)/shard_map/project/pallas_call | solution.py:112
  73.6 7.9 %all-gather.2 = bf16[32,512]{1,0:T(8,128)(2,1)} all-gather(bf16[16,512]{1,0:T(8,128)(2,1)} %get-tuple-element.14), channel_id=4, replica_groups=mesh['y'=4,'x'=4,'zh'=8,'zo'=2,'c'=2] {'zo'}, dimensions={0}, use_global_device_ids=true | all-gather | bytes 49152 | tf_op jit(solution)/shard_map/all_gather | solution.py:256
  81.5 3.2 %recur.1 = (f32[16,128,128]{2,1,0:T(8,128)}, bf16[16,128]{1,0:T(8,128)(2,1)}) custom-call(f32[16,512]{1,0:T(8,128)} %get-tuple-element.13.own_ref, bf16[2,16,512]{2,1,0:T(8,128)(2,1)} %bitcast.45, f32[16,128,128]{2,1,0:T(8,128)} %bitcast.41, f32[1,128]{1,0:T(1,128)} %bitcast.53, f32[1,128]{1,0:T(1,128)} %bitcast.54), custom_call_target="tpu_custom_call" | custom-call | tf_op jit(solution)/shard_map/recur/pallas_call | solution.py:148
  84.7 4.7 %all-gather.3 = bf16[32,128]{1,0:T(8,128)(2,1)} all-gather(bf16[16,128]{1,0:T(8,128)(2,1)} %get-tuple-element.15), channel_id=5, replica_groups=mesh['y'=4,'x'=4,'zh'=8,'zo'=2,'c'=2] {'zo'}, dimensions={0}, use_global_device_ids=true | all-gather | bytes 12288 | tf_op jit(solution)/shard_map/all_gather | solution.py:260
  89.4 2.0 %mix_out.1 = f32[256,128]{1,0:T(8,128)} custom-call(bf16[2,16,128]{2,1,0:T(8,128)(2,1)} %bitcast.48, bf16[8,2,32,512]{3,2,1,0:T(8,128)(2,1)} %bitcast.37), custom_call_target="tpu_custom_call" | custom-call | tf_op jit(solution)/shard_map/mix_out/pallas_call | solution.py:181
  91.4 8.6 %all-to-all-start.1 = ((f32[32,8,128]{2,1,0:T(8,128)}), f32[32,8,128]{2,1,0:T(8,128)S(1)}, u32[]{:S(2)}, u32[]{:S(2)}) async-start(f32[32,8,128]{2,1,0:T(8,128)} %bitcast.43), calls=%async_computation.1 | async-start | bytes 262144 | tf_op jit(solution)/shard_map/all_to_all | solution.py:20
  100.0 7.5 %all-to-all-done.1 = f32[32,8,128]{2,1,0:T(8,128)S(1)} async-done(((f32[32,8,128]{2,1,0:T(8,128)}), f32[32,8,128]{2,1,0:T(8,128)S(1)}, u32[]{:S(2)}, u32[]{:S(2)}) %all-to-all-start.1) | async-done | bytes 131104 | tf_op jit(solution)/shard_map/all_to_all | solution.py:20
  107.5 0.0 copy-start.2
  107.5 0.6 copy-done.2
  108.1 1.8 %row_update.1 = bf16[16,16,128]{2,1,0:T(8,128)(2,1)} custom-call(f32[16,2,8,128]{3,2,1,0:T(8,128)} %bitcast.42, bf16[16,2,16,128]{3,2,1,0:T(8,128)(2,1)} %bitcast.40, f32[16,128]{1,0:T(8,128)} %bitcast.52), custom_call_target="tpu_custom_call" | custom-call | tf_op jit(solution)/shard_map/row_update/pallas_call | solution.py:209
  109.9 4.8 %all-to-all-start.2 = ((bf16[16,16,128]{2,1,0:T(8,128)(2,1)}), bf16[16,16,128]{2,1,0:T(8,128)(2,1)S(1)}, u32[]{:S(2)}, u32[]{:S(2)}) async-start(bf16[16,16,128]{2,1,0:T(8,128)(2,1)} %row_update.1), calls=%async_computation.2 | async-start | bytes 131072 | tf_op jit(solution)/shard_map/all_to_all | solution.py:20
  114.7 0.0 copy-done
  114.7 6.3 %all-to-all-done.2 = bf16[16,16,128]{2,1,0:T(8,128)(2,1)S(1)} async-done(((bf16[16,16,128]{2,1,0:T(8,128)(2,1)}), bf16[16,16,128]{2,1,0:T(8,128)(2,1)S(1)}, u32[]{:S(2)}, u32[]{:S(2)}) %all-to-all-start.2) | async-done | bytes 65568 | tf_op jit(solution)/shard_map/all_to_all | solution.py:20
  121.0 0.2 multiply_reduce_fusion
  121.2 0.0 copy-done.3
  121.2 0.1 multiply_convert_fusion
  121.3 0.0 all-gather.6.cloned.1.call-done
  121.4 3.2 %fusion.3 = bf16[2,16,8,128]{3,2,1,0:T(8,128)(2,1)S(1)} fusion(bf16[2048,1024]{1,0:T(8,128)(2,1)} %all-gather.6.cloned.1.call-done, bf16[2,8,16,128]{3,2,1,0:T(8,128)(2,1)S(1)} %bitcast.44), kind=kOutput, calls=%fused_computation.4 | convolution fusion | flops 67166208 | bytes 4325376 | tf_op jit(solution)/shard_map/dot_general | solution.py:277
  124.6 0.7 copy.28
  125.2 4.7 %all-to-all-start.3 = ((bf16[16,16,128]{2,1,0:T(8,128)(2,1)}), bf16[16,16,128]{2,1,0:T(8,128)(2,1)S(1)}, u32[]{:S(2)}, u32[]{:S(2)}) async-start(bf16[16,16,128]{2,1,0:T(8,128)(2,1)} %bitcast.34), calls=%async_computation.3 | async-start | bytes 131072 | tf_op jit(solution)/shard_map/all_to_all | solution.py:20
  130.0 6.4 %all-to-all-done.3 = bf16[16,16,128]{2,1,0:T(8,128)(2,1)S(1)} async-done(((bf16[16,16,128]{2,1,0:T(8,128)(2,1)}), bf16[16,16,128]{2,1,0:T(8,128)(2,1)S(1)}, u32[]{:S(2)}, u32[]{:S(2)}) %all-to-all-start.3) | async-done | bytes 65568 | tf_op jit(solution)/shard_map/all_to_all | solution.py:20
  136.3 0.6 add_convert_fusion
  (5 shorter events, 0.1 us)
Async XLA Ops:
  7.2 107.5 %copy-start = (f32[2048]{0:T(1024)S(1)}, f32[2048]{0:T(1024)}, u32[]{:S(2)}) copy-start(f32[2048]{0:T(1024)} %param.27) | copy-start | bytes 24580
  7.2 114.1 %copy-start.3 = (f32[2048]{0:T(1024)S(1)}, f32[2048]{0:T(1024)}, u32[]{:S(2)}) copy-start(f32[2048]{0:T(1024)} %param.26) | copy-start | bytes 24580
  7.2 114.2 %all-gather.6.cloned.1.call-start = ((), (), s32[]{:S(2)}) async-start(), calls=%async_computation.4 | async-start | bytes 4325376 | tf_op jit(solution)/shard_map/all_gather | solution.py:251
  9.7 60.9 %all-to-all-start = ((bf16[32,16,128]{2,1,0:T(8,128)(2,1)}), bf16[32,16,128]{2,1,0:T(8,128)(2,1)S(1)}, u32[]{:S(2)}, u32[]{:S(2)}) async-start(bf16[32,16,128]{2,1,0:T(8,128)(2,1)} %get-tuple-element.10), calls=%async_computation | async-start | bytes 262144 | tf_op jit(solution)/shard_map/all_to_all | solution.py:20
  70.6 0.7 copy-start.1
  91.4 16.1 %all-to-all-start.1 = ((f32[32,8,128]{2,1,0:T(8,128)}), f32[32,8,128]{2,1,0:T(8,128)S(1)}, u32[]{:S(2)}, u32[]{:S(2)}) async-start(f32[32,8,128]{2,1,0:T(8,128)} %bitcast.43), calls=%async_computation.1 | async-start | bytes 262144 | tf_op jit(solution)/shard_map/all_to_all | solution.py:20
  107.5 0.7 copy-start.2
  109.9 11.1 %all-to-all-start.2 = ((bf16[16,16,128]{2,1,0:T(8,128)(2,1)}), bf16[16,16,128]{2,1,0:T(8,128)(2,1)S(1)}, u32[]{:S(2)}, u32[]{:S(2)}) async-start(bf16[16,16,128]{2,1,0:T(8,128)(2,1)} %row_update.1), calls=%async_computation.2 | async-start | bytes 131072 | tf_op jit(solution)/shard_map/all_to_all | solution.py:20
  125.2 11.1 %all-to-all-start.3 = ((bf16[16,16,128]{2,1,0:T(8,128)(2,1)}), bf16[16,16,128]{2,1,0:T(8,128)(2,1)S(1)}, u32[]{:S(2)}, u32[]{:S(2)}) async-start(bf16[16,16,128]{2,1,0:T(8,128)(2,1)} %bitcast.34), calls=%async_computation.3 | async-start | bytes 131072 | tf_op jit(solution)/shard_map/all_to_all | solution.py:20
Sparse Core Ops, SparseCore 0:
  10.1 80.3 all-gather.5
where the time goes:
time: 144 us
  blocking collectives  64 us (44%)
  starting transfers between devices  27.5 us (19%)
  waiting for transfers between devices  20.2 us (14%)
  between operations  14.1 us (10%)
  Pallas kernels  11.8 us (8%)
  matrix products  3.19 us (2%)
  local copies, waits for them, and re-layouts  2.02 us (1%)
    all_gather x1, blocking collectives, shards(): lax.all_gather(late, ('zh', 'c'), axis=0).reshape(CHIPS, CORES, *late.shape)  28.3 us
    all_to_all x4, starting transfers between devices, exchange(): return lax.all_to_all(blocks, axes, 0, 0, tiled=True)  27.5 us
    all_gather x1, blocking collectives, shards(): lax.all_gather(early, ('zh', 'c'), axis=0)  23.2 us
    all_to_all x4, waiting for transfers between devices, exchange(): return lax.all_to_all(blocks, axes, 0, 0, tiled=True)  20.2 us
    all_gather x1, blocking collectives, shards(): part = lax.all_gather(send, 'zo', axis=0)  7.89 us
    all_gather x1, blocking collectives, shards(): gated = lax.all_gather(gated, 'zo', axis=0)  4.66 us
    pallas_call x1, Pallas kernels, recur(): pl.pallas_call(recur_body, out_shape=(jax.ShapeDtypeStruct(prior.shape, j...  3.25 us
    dot_general x1, matrix products, shards(): lax.dot_general(squared, mlp_weights[:, hidden:], (((1,), (1,)), ((), ())...  3.19 us
  transfers between devices with their start and end apart: 5, of which 3 were waited for; matrix products, arithmetic and copies ran while one was open for 0% of the time, Pallas kernels for 6%

commit v1 on v0

v1 whole, which is shorter than its diff:
```python
import jax
import jax.numpy as jnp
from jax import lax
from jax.experimental import pallas as pl
from jax.experimental.pallas import tpu as pltpu
from jax.sharding import Mesh
from jax.sharding import PartitionSpec as P

KV = ("y", "x")
TP = ("zh", "zo", "c")
HALVES = 2
CHIPS = 8
CORES = 2
EARLY = 48

epsilon = 1e-06


def exchange(blocks, axes):
    return lax.all_to_all(blocks, axes, 0, 0, tiled=True)


def near(value):
    return pltpu.with_memory_space_constraint(value, pltpu.VMEM)


def run_copies(copies, sems):
    started = [
        pltpu.make_async_copy(src, dst, sems.at[k]) for k, (src, dst) in enumerate(copies)
    ]
    for copy in started:
        copy.start()
    return started


def pack_long_body(up, down, mix, out_ref, sems):
    hidden = up.shape[1]
    copies = [
        (up, out_ref.at[:, :hidden]),
        (down, out_ref.at[:, hidden : 2 * hidden]),
        (mix, out_ref.at[:, 2 * hidden :]),
    ]
    for copy in run_copies(copies, sems):
        copy.wait()


def pack_long(up, down, mix):
    anywhere = pl.BlockSpec(memory_space=pl.ANY)
    rows = up.shape[0]
    return pl.pallas_call(
        pack_long_body,
        out_shape=jax.ShapeDtypeStruct(
            (rows, up.shape[1] + down.shape[1] + mix.shape[1]), up.dtype
        ),
        in_specs=[anywhere] * 3,
        out_specs=pl.BlockSpec(memory_space=pltpu.VMEM),
        scratch_shapes=[pltpu.SemaphoreType.DMA((3,))],
        name="pack_long",
    )(up, down, mix)


def pack_body(residual, wq, wf, wv, wg, early_ref, late_ref, spread_ref, sems):
    cols = wq.shape[1]
    copies = []
    for k, w in enumerate((wq, wf, wv, wg)):
        at = slice(k * cols, (k + 1) * cols)
        copies.append((w.at[:EARLY], early_ref.at[:, at]))
        copies.append((w.at[EARLY:], late_ref.at[:, at]))
    started = run_copies(copies, sems)
    spread_ref[...] = jnp.broadcast_to(residual[...][None], spread_ref.shape)
    for copy in started:
        copy.wait()


def pack(residual, wq, wf, wv, wg, peers):
    rows, cols = wq.shape
    anywhere = pl.BlockSpec(memory_space=pl.ANY)
    vmem = pl.BlockSpec(memory_space=pltpu.VMEM)
    return pl.pallas_call(
        pack_body,
        out_shape=(
            pltpu.VMEM((EARLY, 4 * cols), wq.dtype),
            pltpu.VMEM((rows - EARLY, 4 * cols), wq.dtype),
            pltpu.VMEM((peers, *residual.shape), residual.dtype),
        ),
        in_specs=[vmem] + [anywhere] * 4,
        out_specs=(vmem, vmem, vmem),
        scratch_shapes=[pltpu.SemaphoreType.DMA((8,))],
        name="pack",
    )(residual, wq, wf, wv, wg)


def project_body(x_ref, gain_ref, early_ref, late_ref, own_ref, send_ref):
    zo = lax.axis_index("zo")
    groups, _, height, width = x_ref.shape
    squares = [None] * HALVES
    for f in range(groups):
        for h in range(HALVES):
            x = x_ref[f, h].astype(jnp.float32)
            squares[h] = x * x if f == 0 else squares[h] + x * x
    scale = [
        lax.rsqrt(jnp.sum(s, axis=-1, keepdims=True) / (groups * width) + epsilon)
        for s in squares
    ]
    total = None
    for k in range(CHIPS):
        f = HALVES * k + zo
        gain = gain_ref[pl.ds(f, 1)]
        x = jnp.concatenate(
            [
                (x_ref[f, h].astype(jnp.float32) * scale[h] * gain).astype(jnp.bfloat16)
                for h in range(HALVES)
            ],
            axis=0,
        )
        w = jnp.concatenate(
            [
                piece
                for c in range(CORES)
                for piece in (early_ref[k, c], late_ref[k, c])
            ],
            axis=0,
        )
        term = jnp.dot(x, w, preferred_element_type=jnp.float32)
        total = term if total is None else total + term
    mine = jnp.where(zo == 0, total[:height], total[height:])
    other = jnp.where(zo == 0, total[height:], total[:height])
    own_ref[...] = mine
    send_ref[...] = other.astype(send_ref.dtype)


def project(x, gain, early, late):
    height = x.shape[2]
    cols = early.shape[3]
    return pl.pallas_call(
        project_body,
        out_shape=(
            pltpu.VMEM((height, cols), jnp.float32),
            pltpu.VMEM((height, cols), jnp.bfloat16),
        ),
        name="project",
    )(near(x), gain, near(early), near(late))


def recur_body(
    own_ref, part_ref, prior_ref, floor_ref, gain_ref, state_ref, out_ref, read_ref
):
    zo = lax.axis_index("zo")
    pre = own_ref[...] + part_ref[1 - zo].astype(jnp.float32)
    pre = pre.astype(jnp.bfloat16).astype(jnp.float32)
    width = prior_ref.shape[1]
    query = jax.nn.silu(pre[:, :width])
    floor = floor_ref[...]
    forget = floor + (1.0 - floor) * jax.nn.sigmoid(pre[:, width : 2 * width])
    value = pre[:, 2 * width : 3 * width]
    gate = jax.nn.sigmoid(pre[:, 3 * width :])
    forget_t = forget.T
    query_t = query.T
    for b in range(prior_ref.shape[0]):
        keep = forget_t[:, b : b + 1]
        state = keep * prior_ref[b] + (1.0 - keep) * value[b : b + 1]
        state_ref[b] = state
        read_ref[b : b + 1] = jnp.sum(query_t[:, b : b + 1] * state, axis=0, keepdims=True)
    read = read_ref[...]
    scale = lax.rsqrt(jnp.mean(read * read, axis=-1, keepdims=True) + epsilon)
    out_ref[...] = (read * scale * gain_ref[...] * gate).astype(out_ref.dtype)


def recur(own, part, prior, floor, gain):
    rows, width, _ = prior.shape
    return pl.pallas_call(
        recur_body,
        out_shape=(
            jax.ShapeDtypeStruct(prior.shape, jnp.float32),
            pltpu.VMEM((rows, width), jnp.bfloat16),
        ),
        scratch_shapes=[pltpu.VMEM((rows, width), jnp.float32)],
        name="recur",
    )(near(own), near(part), near(prior), floor, gain)


def mix_body(gated_ref, long_ref, out_ref, w_ref, sem):
    peers, groups, _, width = out_ref.shape
    copy = pltpu.make_async_copy(long_ref.at[:, long_ref.shape[1] - width :], w_ref, sem)
    copy.start()
    copy.wait()
    for f in range(groups):
        part = lax.dot_general(
            gated_ref[...],
            w_ref[f * width : (f + 1) * width],
            (((1,), (1,)), ((), ())),
            preferred_element_type=jnp.float32,
        ).astype(out_ref.dtype)
        for peer in range(peers):
            out_ref[peer, f] = part


def mix_out(gated, weights, groups):
    rows, width = gated.shape
    return pl.pallas_call(
        mix_body,
        out_shape=pltpu.VMEM((groups, groups, rows, width), jnp.bfloat16),
        in_specs=[
            pl.BlockSpec(memory_space=pltpu.VMEM),
            pl.BlockSpec(memory_space=pl.ANY),
        ],
        scratch_shapes=[
            pltpu.VMEM((weights.shape[0], width), jnp.bfloat16),
            pltpu.SemaphoreType.DMA(()),
        ],
        name="mix_out",
    )(near(gated), weights)


def mlp_body(
    parts_ref,
    x_ref,
    post_ref,
    pre_ref,
    long_ref,
    out_ref,
    own_ref,
    after_ref,
    up_ref,
    down_ref,
    sems,
):
    zo = lax.axis_index("zo")
    place = lax.axis_index("y") * lax.axis_size("x") + lax.axis_index("x")
    groups, width = pre_ref.shape
    full = groups * width
    units = up_ref.shape[1]
    copies = run_copies(
        [
            (long_ref.at[:, :units], up_ref),
            (long_ref.at[:, units : 2 * units], down_ref),
        ],
        sems,
    )
    squares = None
    mixed = []
    for f in range(groups):
        total = parts_ref[0, f].astype(jnp.float32)
        for k in range(1, groups):
            total = total + parts_ref[k, f].astype(jnp.float32)
        mixed.append(total)
        squares = total * total if f == 0 else squares + total * total
    scale = lax.rsqrt(jnp.sum(squares, axis=-1, keepdims=True) / full + epsilon)
    for f in range(groups):
        x = x_ref[f, zo].astype(jnp.float32)
        after = x + mixed[f] * scale * post_ref[f : f + 1]
        after = after.astype(jnp.bfloat16).astype(jnp.float32)
        after_ref[f] = after
        squares = after * after if f == 0 else squares + after * after
    scale = lax.rsqrt(jnp.sum(squares, axis=-1, keepdims=True) / full + epsilon)
    hidden = jnp.concatenate(
        [
            (after_ref[f] * scale * pre_ref[f : f + 1]).astype(jnp.bfloat16)
            for f in range(groups)
        ],
        axis=1,
    )
    copies[0].wait()
    up = jnp.dot(hidden, up_ref[...], preferred_element_type=jnp.float32)
    squared = jnp.square(jnp.maximum(up, 0.0)).astype(jnp.bfloat16)
    copies[1].wait()
    channel = lax.dot_general(
        squared, down_ref[...], (((1,), (1,)), ((), ())), preferred_element_type=jnp.float32
    )
    for f in range(groups):
        out_ref[f] = channel[:, f * width : (f + 1) * width].astype(out_ref.dtype)
    own_ref[...] = after_ref[place]


def mlp(parts, x, post, pre, weights, hidden):
    groups, _, rows, width = parts.shape
    vmem = pl.BlockSpec(memory_space=pltpu.VMEM)
    return pl.pallas_call(
        mlp_body,
        out_shape=(
            pltpu.VMEM((groups, rows, width), jnp.bfloat16),
            pltpu.VMEM((rows, width), jnp.float32),
        ),
        in_specs=[vmem] * 4 + [pl.BlockSpec(memory_space=pl.ANY)],
        scratch_shapes=[
            pltpu.VMEM((groups, rows, width), jnp.float32),
            pltpu.VMEM((weights.shape[0], hidden), jnp.bfloat16),
            pltpu.VMEM((weights.shape[0], hidden), jnp.bfloat16),
            pltpu.SemaphoreType.DMA((2,)),
        ],
        name="mlp",
    )(near(parts), near(x), post, pre, weights)


def shards(
    residual,
    prior_state,
    w_query,
    w_forget,
    w_value,
    w_outgate,
    forget_floor,
    group_gain,
    w_mix_out,
    gain_mix_pre,
    gain_mix_post,
    gain_mlp_pre,
    gain_mlp_post,
    w_up,
    w_down,
):
    batch_rows, own_cols = residual.shape
    groups = lax.axis_size(KV)
    place = lax.axis_index(KV)
    hidden = w_up.shape[1]

    long = lax.all_gather(
        pack_long(w_up, w_down.T, w_mix_out.T), TP, axis=0, tiled=True
    )
    early, late, spread = pack(
        residual, w_query, w_forget, w_value, w_outgate, groups * HALVES
    )
    stream = exchange(spread, (*KV, "zo")).reshape(groups, HALVES, batch_rows, own_cols)
    early = lax.all_gather(early, ("zh", "c"), axis=0).reshape(CHIPS, CORES, *early.shape)
    late = lax.all_gather(late, ("zh", "c"), axis=0).reshape(CHIPS, CORES, *late.shape)
    own, send = project(stream, gain_mix_pre.reshape(groups, own_cols), early, late)
    part = lax.all_gather(send, "zo", axis=0)
    new_state, gated = recur(
        own, part, prior_state[:, 0], forget_floor[None], group_gain[None]
    )
    mixed = exchange(mix_out(gated, long, groups), KV)
    channel_part, after_own = mlp(
        mixed,
        stream,
        gain_mix_post.reshape(groups, own_cols),
        gain_mlp_pre.reshape(groups, own_cols),
        long,
        hidden,
    )
    channel = jnp.sum(exchange(channel_part, KV).astype(jnp.float32), axis=0)
    out_gain = lax.dynamic_index_in_dim(
        gain_mlp_post.reshape(groups, own_cols), place, 0, keepdims=True
    )
    layer_out = (after_own + channel * out_gain).astype(jnp.bfloat16)
    return layer_out, new_state[:, None]


def solution(mesh):
    grid = Mesh(mesh.devices.reshape(4, 4, CHIPS, HALVES, CORES), (*KV, *TP))
    return jax.shard_map(
        shards,
        mesh=grid,
        in_specs=(
            P(TP, KV),
            P(TP, KV, None, None),
            P(TP, KV),
            P(TP, KV),
            P(TP, KV),
            P(TP, KV),
            P(KV),
            P(KV),
            P(KV, TP),
            P(),
            P(),
            P(),
            P(),
            P(TP, KV),
            P(KV, TP),
        ),
        out_specs=(P(TP, KV), P(TP, KV, None, None)),
        check_vma=False,
    )
```

time: 144 us -> 142 us (0.986)
  the two profiles are of different devices: /device:TPU:2 before, /device:TPU:1 now
where the time goes in v1:
time: 142 us
  blocking collectives  54.8 us (39%)
  waiting for transfers between devices  35.7 us (25%)
  starting transfers between devices  21 us (15%)
  Pallas kernels  14.3 us (10%)
  between operations  14.1 us (10%)
    all_gather x1, blocking collectives, shards(): lax.all_gather(late, ('zh', 'c'), axis=0).reshape(CHIPS, CORES, *late.shape)  26.8 us
    all_gather x1, blocking collectives, shards(): lax.all_gather(early, ('zh', 'c'), axis=0)  23.5 us
    all_to_all x3, waiting for transfers between devices, exchange(): return lax.all_to_all(blocks, axes, 0, 0, tiled=True)  22.9 us
    all_to_all x3, starting transfers between devices, exchange(): return lax.all_to_all(blocks, axes, 0, 0, tiled=True)  20.9 us
    all_gather x1, waiting for transfers between devices, shards(): lax.all_gather(pack_long(w_up, w_down.T, w_mix_out.T), TP, axis=0, tiled=...  12.8 us
    all_gather x1, blocking collectives, shards(): part = lax.all_gather(send, 'zo', axis=0)  4.51 us
    pallas_call x1, Pallas kernels, mlp(): pl.pallas_call(mlp_body, out_shape=(pltpu.VMEM((groups, rows, width), jnp...  4.4 us
  transfers between devices with their start and end apart: 4, of which 3 were waited for; matrix products, arithmetic and copies ran while one was open for 0% of the time, Pallas kernels for 4%

profile of v1, /device:TPU:1, one launch (start us, length us, event | category | flops | bytes accessed | tf_op | source)
XLA Modules:
  0.0 141.8 jit_solution(12070392556498864442)
XLA Ops:
  7.2 0.0 copy-start
  7.2 0.0 all-gather.5.cloned.1.call-start
  7.2 1.6 %pack_long.1 = bf16[64,1152]{1,0:T(8,128)(2,1)} custom-call(bf16[64,512]{1,0:T(8,128)(2,1)} %up.1, bf16[64,512]{1,0:T(8,128)(2,1)} %bitcast.25, bf16[64,128]{1,0:T(8,128)(2,1)} %bitcast.26), custom_call_target="tpu_custom_call" | custom-call | tf_op jit(solution)/shard_map/pack_long/pallas_call | solution.py:50
  8.8 0.0 all-gather.5.cloned.1.call-update
  8.8 2.2 %pack.1 = (bf16[48,512]{1,0:T(8,128)(2,1)S(1)}, bf16[16,512]{1,0:T(8,128)(2,1)S(1)}, bf16[32,16,128]{2,1,0:T(8,128)(2,1)}) custom-call(bf16[16,128]{1,0:T(8,128)(2,1)} %residual.1, bf16[64,128]{1,0:T(8,128)(2,1)} %wq.1, bf16[64,128]{1,0:T(8,128)(2,1)} %wf.1, bf16[64,128]{1,0:T(8,128)(2,1)} %wv.1, bf16[64,128]{1,0:T(8,128)(2,1)} %wg.1), custom_call_target="tpu_custom_call" | custom-call | tf_op jit(solution)/shard_map/pack/pallas_call | solution.py:79
  11.1 9.2 %all-to-all-start = ((bf16[32,16,128]{2,1,0:T(8,128)(2,1)}), bf16[32,16,128]{2,1,0:T(8,128)(2,1)S(1)}, u32[]{:S(2)}, u32[]{:S(2)}) async-start(bf16[32,16,128]{2,1,0:T(8,128)(2,1)} %get-tuple-element.11), calls=%async_computation | async-start | bytes 262144 | tf_op jit(solution)/shard_map/all_to_all | solution.py:20
  20.3 26.8 %all-gather.1 = bf16[256,512]{1,0:T(8,128)(2,1)S(1)} all-gather(bf16[16,512]{1,0:T(8,128)(2,1)S(1)} %get-tuple-element.13), channel_id=3, replica_groups=mesh['y'=4,'x'=4,'zh'=8,'zo'=2,'c'=2] {'zh','c'}, dimensions={0}, use_global_device_ids=true | all-gather | bytes 278528 | tf_op jit(solution)/shard_map/all_gather | solution.py:325
  47.0 23.5 %all-gather = bf16[768,512]{1,0:T(8,128)(2,1)S(1)} all-gather(bf16[48,512]{1,0:T(8,128)(2,1)S(1)} %get-tuple-element.12), channel_id=2, replica_groups=mesh['y'=4,'x'=4,'zh'=8,'zo'=2,'c'=2] {'zh','c'}, dimensions={0}, use_global_device_ids=true | all-gather | bytes 835584 | tf_op jit(solution)/shard_map/all_gather | solution.py:324
  70.6 0.0 all-to-all-done
  70.6 1.0 project.1
  71.6 4.5 %all-gather.2 = bf16[32,512]{1,0:T(8,128)(2,1)S(1)} all-gather(bf16[16,512]{1,0:T(8,128)(2,1)S(1)} %get-tuple-element.15), channel_id=4, replica_groups=mesh['y'=4,'x'=4,'zh'=8,'zo'=2,'c'=2] {'zo'}, dimensions={0}, use_global_device_ids=true | all-gather | bytes 49152 | tf_op jit(solution)/shard_map/all_gather | solution.py:327
  76.1 0.0 copy-start.1
  76.1 1.2 copy-done.1
  77.3 2.6 %recur.1 = (f32[16,128,128]{2,1,0:T(8,128)}, bf16[16,128]{1,0:T(8,128)(2,1)S(1)}) custom-call(f32[16,512]{1,0:T(8,128)S(1)} %get-tuple-element.14.own_ref, bf16[2,16,512]{2,1,0:T(8,128)(2,1)S(1)} %bitcast.24, f32[16,128,128]{2,1,0:T(8,128)S(1)} %bitcast.22, f32[1,128]{1,0:T(1,128)} %bitcast.30, f32[1,128]{1,0:T(1,128)} %bitcast.31), custom_call_target="tpu_custom_call" | custom-call | tf_op jit(solution)/shard_map/recur/pallas_call | solution.py:171
  80.0 12.8 %all-gather.5.cloned.1.call-done.long_ref = bf16[2048,1152]{1,0:T(8,128)(2,1)} async-done(((bf16[64,1152]{1,0:T(8,128)(2,1)}), bf16[2048,1152]{1,0:T(8,128)(2,1)}) %all-gather.5.cloned.1.call-update) | async-done | bytes 4718608 | tf_op jit(solution)/shard_map/all_gather | solution.py:317
  92.7 2.5 %mix_out.1 = bf16[16,16,16,128]{3,2,1,0:T(8,128)(2,1)} custom-call(bf16[16,128]{1,0:T(8,128)(2,1)S(1)} %get-tuple-element.16.gated_ref, bf16[2048,1152]{1,0:T(8,128)(2,1)} %all-gather.5.cloned.1.call-done.long_ref), custom_call_target="tpu_custom_call" | custom-call | tf_op jit(solution)/shard_map/mix_out/pallas_call | solution.py:200
  95.2 7.2 %all-to-all-start.1 = ((bf16[16,16,16,128]{3,2,1,0:T(8,128)(2,1)}), bf16[16,16,16,128]{3,2,1,0:T(8,128)(2,1)S(1)}, u32[]{:S(2)}, u32[]{:S(2)}) async-start(bf16[16,16,16,128]{3,2,1,0:T(8,128)(2,1)} %mix_out.1), calls=%async_computation.1 | async-start | bytes 2097152 | tf_op jit(solution)/shard_map/all_to_all | solution.py:20
  102.4 16.4 %all-to-all-done.1.parts_ref = bf16[16,16,16,128]{3,2,1,0:T(8,128)(2,1)S(1)} async-done(((bf16[16,16,16,128]{3,2,1,0:T(8,128)(2,1)}), bf16[16,16,16,128]{3,2,1,0:T(8,128)(2,1)S(1)}, u32[]{:S(2)}, u32[]{:S(2)}) %all-to-all-start.1) | async-done | bytes 1048608 | tf_op jit(solution)/shard_map/all_to_all | solution.py:20
  118.9 4.4 %mlp.1 = (bf16[16,16,128]{2,1,0:T(8,128)(2,1)}, f32[16,128]{1,0:T(8,128)S(1)}) custom-call(bf16[16,16,16,128]{3,2,1,0:T(8,128)(2,1)S(1)} %all-to-all-done.1.parts_ref, bf16[16,2,16,128]{3,2,1,0:T(8,128)(2,1)S(1)} %bitcast.21, f32[16,128]{1,0:T(8,128)} %bitcast.28, f32[16,128]{1,0:T(8,128)} %bitcast.29, bf16[2048,1152]{1,0:T(8,128)(2,1)} %all-gather.5.cloned.1.call-done.long_ref), custom_call_target="tpu_custom_call" | custom-call | tf_op jit(solution)/shard_map/mlp/pallas_call | solution.py:278
  123.3 4.5 %all-to-all-start.2 = ((bf16[16,16,128]{2,1,0:T(8,128)(2,1)}), bf16[16,16,128]{2,1,0:T(8,128)(2,1)S(1)}, u32[]{:S(2)}, u32[]{:S(2)}) async-start(bf16[16,16,128]{2,1,0:T(8,128)(2,1)} %get-tuple-element.18), calls=%async_computation.2 | async-start | bytes 131072 | tf_op jit(solution)/shard_map/all_to_all | solution.py:20
  127.8 0.0 copy-done
  127.8 6.5 %all-to-all-done.2 = bf16[16,16,128]{2,1,0:T(8,128)(2,1)S(1)} async-done(((bf16[16,16,128]{2,1,0:T(8,128)(2,1)}), bf16[16,16,128]{2,1,0:T(8,128)(2,1)S(1)}, u32[]{:S(2)}, u32[]{:S(2)}) %all-to-all-start.2) | async-done | bytes 65568 | tf_op jit(solution)/shard_map/all_to_all | solution.py:20
  134.3 0.6 add_convert_fusion
  (2 shorter events, 0.0 us)
Async XLA Ops:
  7.2 120.6 %copy-start = (f32[2048]{0:T(1024)S(1)}, f32[2048]{0:T(1024)}, u32[]{:S(2)}) copy-start(f32[2048]{0:T(1024)} %param.27) | copy-start | bytes 24580
  7.2 85.6 %all-gather.5.cloned.1.call-start = ((), (), s32[]{:S(2)}) async-start(), calls=%async_computation.3 | async-start | bytes 4866048 | tf_op jit(solution)/shard_map/all_gather | solution.py:317
  11.1 59.5 %all-to-all-start = ((bf16[32,16,128]{2,1,0:T(8,128)(2,1)}), bf16[32,16,128]{2,1,0:T(8,128)(2,1)S(1)}, u32[]{:S(2)}, u32[]{:S(2)}) async-start(bf16[32,16,128]{2,1,0:T(8,128)(2,1)} %get-tuple-element.11), calls=%async_computation | async-start | bytes 262144 | tf_op jit(solution)/shard_map/all_to_all | solution.py:20
  76.1 1.2 copy-start.1
  95.2 23.6 %all-to-all-start.1 = ((bf16[16,16,16,128]{3,2,1,0:T(8,128)(2,1)}), bf16[16,16,16,128]{3,2,1,0:T(8,128)(2,1)S(1)}, u32[]{:S(2)}, u32[]{:S(2)}) async-start(bf16[16,16,16,128]{3,2,1,0:T(8,128)(2,1)} %mix_out.1), calls=%async_computation.1 | async-start | bytes 2097152 | tf_op jit(solution)/shard_map/all_to_all | solution.py:20
  123.3 11.0 %all-to-all-start.2 = ((bf16[16,16,128]{2,1,0:T(8,128)(2,1)}), bf16[16,16,128]{2,1,0:T(8,128)(2,1)S(1)}, u32[]{:S(2)}, u32[]{:S(2)}) async-start(bf16[16,16,128]{2,1,0:T(8,128)(2,1)} %get-tuple-element.18), calls=%async_computation.2 | async-start | bytes 131072 | tf_op jit(solution)/shard_map/all_to_all | solution.py:20
Sparse Core Ops, SparseCore 0:
  10.1 82.5 all-gather.4

commit v2 on v1

--- a/solution.py
+++ b/solution.py
@@ -33,66 +33,68 @@
     return started
 
 
-def pack_long_body(up, down, mix, out_ref, sems):
+def pack_long_body(up, down, out_ref, sems):
     hidden = up.shape[1]
     copies = [
         (up, out_ref.at[:, :hidden]),
-        (down, out_ref.at[:, hidden : 2 * hidden]),
-        (mix, out_ref.at[:, 2 * hidden :]),
+        (down, out_ref.at[:, hidden:]),
     ]
     for copy in run_copies(copies, sems):
         copy.wait()
 
 
-def pack_long(up, down, mix):
+def pack_long(up, down):
     anywhere = pl.BlockSpec(memory_space=pl.ANY)
     rows = up.shape[0]
     return pl.pallas_call(
         pack_long_body,
-        out_shape=jax.ShapeDtypeStruct(
-            (rows, up.shape[1] + down.shape[1] + mix.shape[1]), up.dtype
-        ),
-        in_specs=[anywhere] * 3,
+        out_shape=jax.ShapeDtypeStruct((rows, up.shape[1] + down.shape[1]), up.dtype),
+        in_specs=[anywhere] * 2,
         out_specs=pl.BlockSpec(memory_space=pltpu.VMEM),
-        scratch_shapes=[pltpu.SemaphoreType.DMA((3,))],
+        scratch_shapes=[pltpu.SemaphoreType.DMA((2,))],
         name="pack_long",
-    )(up, down, mix)
-
-
-def pack_body(residual, wq, wf, wv, wg, early_ref, late_ref, spread_ref, sems):
-    cols = wq.shape[1]
+    )(up, down)
+
+
+def pack_body(residual, wq, wf, wv, wg, mix, early_ref, late_ref, spread_ref, sems):
+    rows, cols = wq.shape
+    rest = rows - EARLY
+    part = mix.shape[0] // 4
     copies = []
     for k, w in enumerate((wq, wf, wv, wg)):
         at = slice(k * cols, (k + 1) * cols)
         copies.append((w.at[:EARLY], early_ref.at[:, at]))
-        copies.append((w.at[EARLY:], late_ref.at[:, at]))
+        copies.append((w.at[EARLY:], late_ref.at[:rest, at]))
+        copies.append((mix.at[k * part : (k + 1) * part], late_ref.at[rest:, at]))
     started = run_copies(copies, sems)
     spread_ref[...] = jnp.broadcast_to(residual[...][None], spread_ref.shape)
     for copy in started:
         copy.wait()
 
 
-def pack(residual, wq, wf, wv, wg, peers):
+def pack(residual, wq, wf, wv, wg, mix, peers):
     rows, cols = wq.shape
+    late = rows - EARLY + mix.shape[0] // 4
     anywhere = pl.BlockSpec(memory_space=pl.ANY)
     vmem = pl.BlockSpec(memory_space=pltpu.VMEM)
     return pl.pallas_call(
         pack_body,
         out_shape=(
             pltpu.VMEM((EARLY, 4 * cols), wq.dtype),
-            pltpu.VMEM((rows - EARLY, 4 * cols), wq.dtype),
+            pltpu.VMEM((late, 4 * cols), wq.dtype),
             pltpu.VMEM((peers, *residual.shape), residual.dtype),
         ),
-        in_specs=[vmem] + [anywhere] * 4,
+        in_specs=[vmem] + [anywhere] * 5,
         out_specs=(vmem, vmem, vmem),
-        scratch_shapes=[pltpu.SemaphoreType.DMA((8,))],
+        scratch_shapes=[pltpu.SemaphoreType.DMA((12,))],
         name="pack",
-    )(residual, wq, wf, wv, wg)
+    )(residual, wq, wf, wv, wg, mix)
 
 
 def project_body(x_ref, gain_ref, early_ref, late_ref, own_ref, send_ref):
     zo = lax.axis_index("zo")
     groups, _, height, width = x_ref.shape
+    rest = late_ref.shape[2] // 2
     squares = [None] * HALVES
     for f in range(groups):
         for h in range(HALVES):
@@ -117,7 +119,7 @@
             [
                 piece
                 for c in range(CORES)
-                for piece in (early_ref[k, c], late_ref[k, c])
+                for piece in (early_ref[k, c], late_ref[k, c, :rest])
             ],
             axis=0,
         )
@@ -179,87 +181,102 @@
     )(near(own), near(part), near(prior), floor, gain)
 
 
-def mix_body(gated_ref, long_ref, out_ref, w_ref, sem):
-    peers, groups, _, width = out_ref.shape
-    copy = pltpu.make_async_copy(long_ref.at[:, long_ref.shape[1] - width :], w_ref, sem)
-    copy.start()
-    copy.wait()
-    for f in range(groups):
-        part = lax.dot_general(
-            gated_ref[...],
-            w_ref[f * width : (f + 1) * width],
-            (((1,), (1,)), ((), ())),
-            preferred_element_type=jnp.float32,
-        ).astype(out_ref.dtype)
-        for peer in range(peers):
-            out_ref[peer, f] = part
-
-
-def mix_out(gated, weights, groups):
-    rows, width = gated.shape
+def mix_body(gated_ref, late_ref, out_ref, order_ref):
+    height, width = gated_ref.shape[1:]
+    rest = late_ref.shape[2] // 2
+    for h in range(HALVES):
+        order_ref[pl.ds(h, height, stride=HALVES)] = gated_ref[h].astype(jnp.float32)
+    left = order_ref[...].astype(jnp.bfloat16)
+    for k in range(CHIPS):
+        right = jnp.concatenate(
+            [
+                late_ref[k, c, rest:, j * width : (j + 1) * width]
+                for c in range(CORES)
+                for j in range(4)
+            ],
+            axis=0,
+        )
+        out_ref[pl.ds(k, HALVES * height, stride=CHIPS)] = lax.dot_general(
+            left, right, (((1,), (1,)), ((), ())), preferred_element_type=jnp.float32
+        )
+
+
+def mix_out(gated, late):
+    height, width = gated.shape[1:]
     return pl.pallas_call(
         mix_body,
-        out_shape=pltpu.VMEM((groups, groups, rows, width), jnp.bfloat16),
-        in_specs=[
-            pl.BlockSpec(memory_space=pltpu.VMEM),
-            pl.BlockSpec(memory_space=pl.ANY),
-        ],
-        scratch_shapes=[
-            pltpu.VMEM((weights.shape[0], width), jnp.bfloat16),
-            pltpu.SemaphoreType.DMA(()),
-        ],
+        out_shape=pltpu.VMEM((CHIPS * HALVES * height, width), jnp.float32),
+        scratch_shapes=[pltpu.VMEM((HALVES * height, width), jnp.float32)],
         name="mix_out",
-    )(near(gated), weights)
+    )(near(gated), near(late))
+
+
+def row_body(sums_ref, x_ref, gain_ref, out_ref, mixed_ref):
+    zo = lax.axis_index("zo")
+    place = lax.axis_index("y") * lax.axis_size("x") + lax.axis_index("x")
+    groups, width = gain_ref.shape
+    for h in range(HALVES):
+        total = sums_ref[0, h]
+        for k in range(1, groups):
+            total = total + sums_ref[k, h]
+        mixed_ref[pl.ds(h, CHIPS, stride=HALVES)] = total
+    mixed = mixed_ref[...]
+    scale = lax.rsqrt(jnp.sum(mixed * mixed) / gain_ref.size + epsilon)
+    stream = x_ref[:, zo].astype(jnp.float32)
+    at = lax.broadcasted_iota(jnp.int32, stream.shape, 1) == place
+    row = jnp.sum(jnp.where(at, stream, 0.0), axis=1)
+    after = (row + mixed * scale * gain_ref[...]).astype(out_ref.dtype)
+    out_ref[...] = jnp.broadcast_to(after[None], out_ref.shape)
+
+
+def row_update(sums, x, gain):
+    groups, width = gain.shape
+    return pl.pallas_call(
+        row_body,
+        out_shape=pltpu.VMEM((groups, groups, width), jnp.bfloat16),
+        scratch_shapes=[pltpu.VMEM((groups, width), jnp.float32)],
+        name="row_update",
+    )(near(sums), near(x), gain)
 
 
 def mlp_body(
-    parts_ref,
-    x_ref,
+    row_ref,
+    pre_ref,
     post_ref,
-    pre_ref,
     long_ref,
     out_ref,
     own_ref,
+    gain_ref,
     after_ref,
     up_ref,
     down_ref,
     sems,
 ):
-    zo = lax.axis_index("zo")
     place = lax.axis_index("y") * lax.axis_size("x") + lax.axis_index("x")
     groups, width = pre_ref.shape
-    full = groups * width
+    height = row_ref.shape[0]
     units = up_ref.shape[1]
     copies = run_copies(
-        [
-            (long_ref.at[:, :units], up_ref),
-            (long_ref.at[:, units : 2 * units], down_ref),
-        ],
-        sems,
-    )
-    squares = None
-    mixed = []
-    for f in range(groups):
-        total = parts_ref[0, f].astype(jnp.float32)
-        for k in range(1, groups):
-            total = total + parts_ref[k, f].astype(jnp.float32)
-        mixed.append(total)
-        squares = total * total if f == 0 else squares + total * total
-    scale = lax.rsqrt(jnp.sum(squares, axis=-1, keepdims=True) / full + epsilon)
-    for f in range(groups):
-        x = x_ref[f, zo].astype(jnp.float32)
-        after = x + mixed[f] * scale * post_ref[f : f + 1]
-        after = after.astype(jnp.bfloat16).astype(jnp.float32)
-        after_ref[f] = after
-        squares = after * after if f == 0 else squares + after * after
-    scale = lax.rsqrt(jnp.sum(squares, axis=-1, keepdims=True) / full + epsilon)
+        [(long_ref.at[:, :units], up_ref), (long_ref.at[:, units:], down_ref)], sems
+    )
+    for row in range(height):
+        after_ref[row * groups : (row + 1) * groups] = row_ref[row].astype(jnp.float32)
+    after = [after_ref[pl.ds(f, height, stride=groups)] for f in range(groups)]
+    squares = after[0] * after[0]
+    for f in range(1, groups):
+        squares = squares + after[f] * after[f]
+    scale = lax.rsqrt(
+        jnp.sum(squares, axis=-1, keepdims=True) / (groups * width) + epsilon
+    )
     hidden = jnp.concatenate(
         [
-            (after_ref[f] * scale * pre_ref[f : f + 1]).astype(jnp.bfloat16)
+            (after[f] * scale * pre_ref[f : f + 1]).astype(jnp.bfloat16)
             for f in range(groups)
         ],
         axis=1,
     )
+    own_ref[...] = after_ref[pl.ds(place, height, stride=groups)]
+    gain_ref[...] = post_ref[pl.ds(place, 1)]
     copies[0].wait()
     up = jnp.dot(hidden, up_ref[...], preferred_element_type=jnp.float32)
     squared = jnp.square(jnp.maximum(up, 0.0)).astype(jnp.bfloat16)
@@ -269,27 +286,27 @@
     )
     for f in range(groups):
         out_ref[f] = channel[:, f * width : (f + 1) * width].astype(out_ref.dtype)
-    own_ref[...] = after_ref[place]
-
-
-def mlp(parts, x, post, pre, weights, hidden):
-    groups, _, rows, width = parts.shape
+
+
+def mlp(after, pre, post, weights, hidden):
+    rows, groups, width = after.shape
     vmem = pl.BlockSpec(memory_space=pltpu.VMEM)
     return pl.pallas_call(
         mlp_body,
         out_shape=(
             pltpu.VMEM((groups, rows, width), jnp.bfloat16),
             pltpu.VMEM((rows, width), jnp.float32),
-        ),
-        in_specs=[vmem] * 4 + [pl.BlockSpec(memory_space=pl.ANY)],
+            pltpu.VMEM((1, width), jnp.float32),
+        ),
+        in_specs=[vmem] * 3 + [pl.BlockSpec(memory_space=pl.ANY)],
         scratch_shapes=[
-            pltpu.VMEM((groups, rows, width), jnp.float32),
+            pltpu.VMEM((rows * groups, width), jnp.float32),
             pltpu.VMEM((weights.shape[0], hidden), jnp.bfloat16),
             pltpu.VMEM((weights.shape[0], hidden), jnp.bfloat16),
             pltpu.SemaphoreType.DMA((2,)),
         ],
         name="mlp",
-    )(near(parts), near(x), post, pre, weights)
+    )(near(after), pre, post, weights)
 
 
 def shards(
@@ -311,14 +328,11 @@
 ):
     batch_rows, own_cols = residual.shape
     groups = lax.axis_size(KV)
-    place = lax.axis_index(KV)
     hidden = w_up.shape[1]
 
-    long = lax.all_gather(
-        pack_long(w_up, w_down.T, w_mix_out.T), TP, axis=0, tiled=True
-    )
+    long = lax.all_gather(pack_long(w_up, w_down.T), TP, axis=0, tiled=True)
     early, late, spread = pack(
-        residual, w_query, w_forget, w_value, w_outgate, groups * HALVES
+        residual, w_query, w_forget, w_value, w_outgate, w_mix_out.T, groups * HALVES
     )
     stream = exchange(spread, (*KV, "zo")).reshape(groups, HALVES, batch_rows, own_cols)
     early = lax.all_gather(early, ("zh", "c"), axis=0).reshape(CHIPS, CORES, *early.shape)
@@ -328,19 +342,18 @@
     new_state, gated = recur(
         own, part, prior_state[:, 0], forget_floor[None], group_gain[None]
     )
-    mixed = exchange(mix_out(gated, long, groups), KV)
-    channel_part, after_own = mlp(
-        mixed,
-        stream,
-        gain_mix_post.reshape(groups, own_cols),
+    gated = lax.all_gather(gated, "zo", axis=0)
+    mixed_part = mix_out(gated, late).reshape(groups * HALVES, CHIPS, own_cols)
+    mixed = exchange(mixed_part, (*KV, "zo")).reshape(groups, HALVES, CHIPS, own_cols)
+    after_row = row_update(mixed, stream, gain_mix_post.reshape(groups, own_cols))
+    channel_part, after_own, out_gain = mlp(
+        exchange(after_row, KV),
         gain_mlp_pre.reshape(groups, own_cols),
+        gain_mlp_post.reshape(groups, own_cols),
         long,
         hidden,
     )
     channel = jnp.sum(exchange(channel_part, KV).astype(jnp.float32), axis=0)
-    out_gain = lax.dynamic_index_in_dim(
-        gain_mlp_post.reshape(groups, own_cols), place, 0, keepdims=True
-    )
     layer_out = (after_own + channel * out_gain).astype(jnp.bfloat16)
     return layer_out, new_state[:, None]
 

time: 142 us -> 134 us (0.944)
  the two profiles are of different devices: /device:TPU:1 before, /device:TPU:2 now
where the time goes in v2:
time: 134 us
  blocking collectives  97.1 us (72%)
  between operations  14.1 us (11%)
  Pallas kernels  12.3 us (9%)
  starting transfers between devices  9.45 us (7%)
    all_to_all x3, blocking collectives, exchange(): return lax.all_to_all(blocks, axes, 0, 0, tiled=True)  36.8 us
    all_gather x1, blocking collectives, shards(): lax.all_gather(late, ('zh', 'c'), axis=0).reshape(CHIPS, CORES, *late.shape)  26.9 us
    all_gather x1, blocking collectives, shards(): lax.all_gather(early, ('zh', 'c'), axis=0)  22.3 us
    all_to_all x1, starting transfers between devices, exchange(): return lax.all_to_all(blocks, axes, 0, 0, tiled=True)  9.41 us
    all_gather x1, blocking collectives, shards(): part = lax.all_gather(send, 'zo', axis=0)  6.49 us
    all_gather x1, blocking collectives, shards(): gated = lax.all_gather(gated, 'zo', axis=0)  4.57 us
    pallas_call x1, Pallas kernels, mlp(): pl.pallas_call(mlp_body, out_shape=(pltpu.VMEM((groups, rows, width), jnp...  3.63 us
  transfers between devices with their start and end apart: 2, of which 0 were waited for; matrix products, arithmetic and copies ran while one was open for 0% of the time, Pallas kernels for 5%

profile of v2, /device:TPU:2, one launch (start us, length us, event | category | flops | bytes accessed | tf_op | source)
XLA Modules:
  0.0 133.6 jit_solution(9265497074131875478)
XLA Ops:
  7.2 0.0 copy-start
  7.2 0.0 all-gather.6.cloned.1.call-start
  7.2 1.6 %pack_long.1 = bf16[64,1024]{1,0:T(8,128)(2,1)} custom-call(bf16[64,512]{1,0:T(8,128)(2,1)} %up.1, bf16[64,512]{1,0:T(8,128)(2,1)} %bitcast.31), custom_call_target="tpu_custom_call" | custom-call | tf_op jit(solution)/shard_map/pack_long/pallas_call | solution.py:49
  8.8 0.0 all-gather.6.cloned.1.call-update
  8.9 2.3 %pack.1 = (bf16[48,512]{1,0:T(8,128)(2,1)S(1)}, bf16[32,512]{1,0:T(8,128)(2,1)S(1)}, bf16[32,16,128]{2,1,0:T(8,128)(2,1)}) custom-call(bf16[16,128]{1,0:T(8,128)(2,1)} %residual.1, bf16[64,128]{1,0:T(8,128)(2,1)} %wq.1, bf16[64,128]{1,0:T(8,128)(2,1)} %wf.1, bf16[64,128]{1,0:T(8,128)(2,1)} %wv.1, bf16[64,128]{1,0:T(8,128)(2,1)} %wg.1, bf16[64,128]{1,0:T(8,128)(2,1)} %bitcast.32), custom_call_target="tpu_custom_call" | custom-call | tf_op jit(solution)/shard_map/pack/pallas_call | solution.py:80
  11.2 9.4 %all-to-all-start = ((bf16[32,16,128]{2,1,0:T(8,128)(2,1)}), bf16[32,16,128]{2,1,0:T(8,128)(2,1)S(1)}, u32[]{:S(2)}, u32[]{:S(2)}) async-start(bf16[32,16,128]{2,1,0:T(8,128)(2,1)} %get-tuple-element.12), calls=%async_computation | async-start | bytes 262144 | tf_op jit(solution)/shard_map/all_to_all | solution.py:20
  20.6 26.9 %all-gather.1 = bf16[512,512]{1,0:T(8,128)(2,1)S(1)} all-gather(bf16[32,512]{1,0:T(8,128)(2,1)S(1)} %get-tuple-element.14), channel_id=3, replica_groups=mesh['y'=4,'x'=4,'zh'=8,'zo'=2,'c'=2] {'zh','c'}, dimensions={0}, use_global_device_ids=true | all-gather | bytes 557056 | tf_op jit(solution)/shard_map/all_gather | solution.py:339
  47.5 22.3 %all-gather = bf16[768,512]{1,0:T(8,128)(2,1)S(1)} all-gather(bf16[48,512]{1,0:T(8,128)(2,1)S(1)} %get-tuple-element.13), channel_id=2, replica_groups=mesh['y'=4,'x'=4,'zh'=8,'zo'=2,'c'=2] {'zh','c'}, dimensions={0}, use_global_device_ids=true | all-gather | bytes 835584 | tf_op jit(solution)/shard_map/all_gather | solution.py:338
  69.8 0.0 all-to-all-done
  69.9 1.0 project.1
  70.9 6.5 %all-gather.2 = bf16[32,512]{1,0:T(8,128)(2,1)S(1)} all-gather(bf16[16,512]{1,0:T(8,128)(2,1)S(1)} %get-tuple-element.16), channel_id=4, replica_groups=mesh['y'=4,'x'=4,'zh'=8,'zo'=2,'c'=2] {'zo'}, dimensions={0}, use_global_device_ids=true | all-gather | bytes 49152 | tf_op jit(solution)/shard_map/all_gather | solution.py:341
  77.4 0.0 copy-done
  77.4 2.6 %recur.1 = (f32[16,128,128]{2,1,0:T(8,128)}, bf16[16,128]{1,0:T(8,128)(2,1)S(1)}) custom-call(f32[16,512]{1,0:T(8,128)S(1)} %get-tuple-element.15.own_ref, bf16[2,16,512]{2,1,0:T(8,128)(2,1)S(1)} %bitcast.28, f32[16,128,128]{2,1,0:T(8,128)S(1)} %bitcast.25, f32[1,128]{1,0:T(1,128)} %bitcast.37, f32[1,128]{1,0:T(1,128)} %bitcast.38), custom_call_target="tpu_custom_call" | custom-call | tf_op jit(solution)/shard_map/recur/pallas_call | solution.py:173
  80.0 4.6 %all-gather.3 = bf16[32,128]{1,0:T(8,128)(2,1)S(1)} all-gather(bf16[16,128]{1,0:T(8,128)(2,1)S(1)} %get-tuple-element.17), channel_id=5, replica_groups=mesh['y'=4,'x'=4,'zh'=8,'zo'=2,'c'=2] {'zo'}, dimensions={0}, use_global_device_ids=true | all-gather | bytes 12288 | tf_op jit(solution)/shard_map/all_gather | solution.py:345
  84.6 0.2 mix_out.1
  84.8 15.1 %all_to_all.20 = f32[32,8,128]{2,1,0:T(8,128)S(1)} all-to-all(f32[32,8,128]{2,1,0:T(8,128)S(1)} %bitcast.26), channel_id=1, replica_groups=mesh['y'=4,'x'=4,'zh'=8,'zo'=2,'c'=2] {'y','x','zo'}, dimensions={0} | all-to-all | bytes 262144 | tf_op jit(solution)/shard_map/all_to_all | solution.py:20
  100.0 0.9 row_update.1
  100.9 10.9 %all_to_all.21.row_ref = bf16[16,16,128]{2,1,0:T(8,128)(2,1)S(1)} all-to-all(bf16[16,16,128]{2,1,0:T(8,128)(2,1)S(1)} %row_update.1), channel_id=1, replica_groups=mesh['y'=4,'x'=4,'zh'=8,'zo'=2,'c'=2] {'y','x'}, dimensions={0} | all-to-all | bytes 131072 | tf_op jit(solution)/shard_map/all_to_all | solution.py:20
  111.7 0.0 all-gather.6.cloned.1.call-done.long_ref
  111.7 3.6 %mlp.1 = (bf16[16,16,128]{2,1,0:T(8,128)(2,1)S(1)}, f32[16,128]{1,0:T(8,128)S(1)}, f32[1,128]{1,0:T(1,128)S(1)}) custom-call(bf16[16,16,128]{2,1,0:T(8,128)(2,1)S(1)} %all_to_all.21.row_ref, f32[16,128]{1,0:T(8,128)} %bitcast.34, f32[16,128]{1,0:T(8,128)} %bitcast.35, bf16[2048,1024]{1,0:T(8,128)(2,1)} %all-gather.6.cloned.1.call-done.long_ref), custom_call_target="tpu_custom_call" | custom-call | tf_op jit(solution)/shard_map/mlp/pallas_call | solution.py:294
  115.4 10.8 %all_to_all.22 = bf16[16,16,128]{2,1,0:T(8,128)(2,1)S(1)} all-to-all(bf16[16,16,128]{2,1,0:T(8,128)(2,1)S(1)} %get-tuple-element.19), channel_id=1, replica_groups=mesh['y'=4,'x'=4,'zh'=8,'zo'=2,'c'=2] {'y','x'}, dimensions={0} | all-to-all | bytes 131072 | tf_op jit(solution)/shard_map/all_to_all | solution.py:20
  126.2 0.6 add_convert_fusion
  (1 shorter events, 0.0 us)
Async XLA Ops:
  7.2 70.2 %copy-start = (f32[16,1,128,128]{3,2,1,0:T(8,128)S(1)}, f32[16,1,128,128]{3,2,1,0:T(8,128)}, u32[]{:S(2)}) copy-start(f32[16,1,128,128]{3,2,1,0:T(8,128)} %param.16) | copy-start | bytes 3145732
  7.2 104.6 %all-gather.6.cloned.1.call-start = ((), (), s32[]{:S(2)}) async-start(), calls=%async_computation.4 | async-start | bytes 4325376 | tf_op jit(solution)/shard_map/all_gather | solution.py:333
  11.2 58.7 %all-to-all-start = ((bf16[32,16,128]{2,1,0:T(8,128)(2,1)}), bf16[32,16,128]{2,1,0:T(8,128)(2,1)S(1)}, u32[]{:S(2)}, u32[]{:S(2)}) async-start(bf16[32,16,128]{2,1,0:T(8,128)(2,1)} %get-tuple-element.12), calls=%async_computation | async-start | bytes 262144 | tf_op jit(solution)/shard_map/all_to_all | solution.py:20
Sparse Core Ops, SparseCore 0:
  10.1 81.8 all-gather.5

commit v3 on v2

--- a/solution.py
+++ b/solution.py
@@ -11,7 +11,7 @@
 HALVES = 2
 CHIPS = 8
 CORES = 2
-EARLY = 48
+EARLY = 56
 
 epsilon = 1e-06
 
@@ -33,46 +33,40 @@
     return started
 
 
-def pack_long_body(up, down, out_ref, sems):
-    hidden = up.shape[1]
-    copies = [
-        (up, out_ref.at[:, :hidden]),
-        (down, out_ref.at[:, hidden:]),
-    ]
-    for copy in run_copies(copies, sems):
-        copy.wait()
-
-
-def pack_long(up, down):
-    anywhere = pl.BlockSpec(memory_space=pl.ANY)
-    rows = up.shape[0]
-    return pl.pallas_call(
-        pack_long_body,
-        out_shape=jax.ShapeDtypeStruct((rows, up.shape[1] + down.shape[1]), up.dtype),
-        in_specs=[anywhere] * 2,
-        out_specs=pl.BlockSpec(memory_space=pltpu.VMEM),
-        scratch_shapes=[pltpu.SemaphoreType.DMA((2,))],
-        name="pack_long",
-    )(up, down)
-
-
-def pack_body(residual, wq, wf, wv, wg, mix, early_ref, late_ref, spread_ref, sems):
+def pack_body(
+    residual,
+    wq,
+    wf,
+    wv,
+    wg,
+    mix,
+    up,
+    down,
+    long_ref,
+    early_ref,
+    late_ref,
+    spread_ref,
+    stage_ref,
+    sems,
+):
     rows, cols = wq.shape
     rest = rows - EARLY
     part = mix.shape[0] // 4
-    copies = []
+    hidden = up.shape[1]
+    copies = [(up, long_ref.at[:, :hidden]), (down, long_ref.at[:, hidden:])]
     for k, w in enumerate((wq, wf, wv, wg)):
         at = slice(k * cols, (k + 1) * cols)
         copies.append((w.at[:EARLY], early_ref.at[:, at]))
-        copies.append((w.at[EARLY:], late_ref.at[:rest, at]))
-        copies.append((mix.at[k * part : (k + 1) * part], late_ref.at[rest:, at]))
+        copies.append((w.at[EARLY:], stage_ref.at[:rest, at]))
+        copies.append((mix.at[k * part : (k + 1) * part], stage_ref.at[rest:, at]))
     started = run_copies(copies, sems)
     spread_ref[...] = jnp.broadcast_to(residual[...][None], spread_ref.shape)
     for copy in started:
         copy.wait()
-
-
-def pack(residual, wq, wf, wv, wg, mix, peers):
+    late_ref[...] = jnp.broadcast_to(stage_ref[...][None], late_ref.shape)
+
+
+def pack(residual, wq, wf, wv, wg, mix, up, down, peers, sharers):
     rows, cols = wq.shape
     late = rows - EARLY + mix.shape[0] // 4
     anywhere = pl.BlockSpec(memory_space=pl.ANY)
@@ -80,21 +74,25 @@
     return pl.pallas_call(
         pack_body,
         out_shape=(
+            jax.ShapeDtypeStruct((rows, up.shape[1] + down.shape[1]), up.dtype),
             pltpu.VMEM((EARLY, 4 * cols), wq.dtype),
+            pltpu.VMEM((sharers, late, 4 * cols), wq.dtype),
+            pltpu.VMEM((peers, *residual.shape), residual.dtype),
+        ),
+        in_specs=[vmem] + [anywhere] * 7,
+        out_specs=(vmem,) * 4,
+        scratch_shapes=[
             pltpu.VMEM((late, 4 * cols), wq.dtype),
-            pltpu.VMEM((peers, *residual.shape), residual.dtype),
-        ),
-        in_specs=[vmem] + [anywhere] * 5,
-        out_specs=(vmem, vmem, vmem),
-        scratch_shapes=[pltpu.SemaphoreType.DMA((12,))],
+            pltpu.SemaphoreType.DMA((14,)),
+        ],
         name="pack",
-    )(residual, wq, wf, wv, wg, mix)
+    )(residual, wq, wf, wv, wg, mix, up, down)
 
 
 def project_body(x_ref, gain_ref, early_ref, late_ref, own_ref, send_ref):
     zo = lax.axis_index("zo")
     groups, _, height, width = x_ref.shape
-    rest = late_ref.shape[2] // 2
+    rest = late_ref.shape[2] - width // 8
     squares = [None] * HALVES
     for f in range(groups):
         for h in range(HALVES):
@@ -183,7 +181,7 @@
 
 def mix_body(gated_ref, late_ref, out_ref, order_ref):
     height, width = gated_ref.shape[1:]
-    rest = late_ref.shape[2] // 2
+    rest = late_ref.shape[2] - width // 8
     for h in range(HALVES):
         order_ref[pl.ds(h, height, stride=HALVES)] = gated_ref[h].astype(jnp.float32)
     left = order_ref[...].astype(jnp.bfloat16)
@@ -330,13 +328,22 @@
     groups = lax.axis_size(KV)
     hidden = w_up.shape[1]
 
-    long = lax.all_gather(pack_long(w_up, w_down.T), TP, axis=0, tiled=True)
-    early, late, spread = pack(
-        residual, w_query, w_forget, w_value, w_outgate, w_mix_out.T, groups * HALVES
-    )
+    long, early, late, spread = pack(
+        residual,
+        w_query,
+        w_forget,
+        w_value,
+        w_outgate,
+        w_mix_out.T,
+        w_up,
+        w_down.T,
+        groups * HALVES,
+        CHIPS * CORES,
+    )
+    long = lax.all_gather(long, TP, axis=0, tiled=True)
     stream = exchange(spread, (*KV, "zo")).reshape(groups, HALVES, batch_rows, own_cols)
+    late = exchange(late, ("zh", "c")).reshape(CHIPS, CORES, *late.shape[1:])
     early = lax.all_gather(early, ("zh", "c"), axis=0).reshape(CHIPS, CORES, *early.shape)
-    late = lax.all_gather(late, ("zh", "c"), axis=0).reshape(CHIPS, CORES, *late.shape)
     own, send = project(stream, gain_mix_pre.reshape(groups, own_cols), early, late)
     part = lax.all_gather(send, "zo", axis=0)
     new_state, gated = recur(

time: 134 us -> 149 us (1.11)
  blocking collectives: 97.1 us -> 108 us
  starting transfers between devices: 9.45 us -> 14.3 us
    all_gather x1 -> x0, blocking collectives: 26.9 us -> none  [shards(): lax.all_gather(late, ('zh', 'c'), axis=0).reshape(CHIPS, CORES, *late.shape)]
    all_gather x1, blocking collectives: 22.3 us -> 48.7 us  [shards(): lax.all_gather(early, ('zh', 'c'), axis=0)]
    all_to_all x3 -> x4, blocking collectives: 36.8 us -> 50.6 us  [exchange(): return lax.all_to_all(blocks, axes, 0, 0, tiled=True)]
    all_to_all x1, starting transfers between devices: 9.41 us -> 14.3 us  [exchange(): return lax.all_to_all(blocks, axes, 0, 0, tiled=True)]
    all_gather x1, blocking collectives: 6.49 us -> 4.41 us  [shards(): part = lax.all_gather(send, 'zo', axis=0)]
    pallas_call x2 -> x1, Pallas kernels: 3.9 us -> 2.57 us  [pack(): pl.pallas_call(pack_body, out_shape=(jax.ShapeDtypeStruct((rows, up.shape...]
  transfers between devices with their start and end apart: 2 -> 2, of which waited for: 0 -> 0; matrix products, arithmetic and copies ran while one was open for 0% -> 0% of each run, Pallas kernels for 5% -> 3%
where the time goes in v3:
time: 149 us; the launch traced here: 148 us
  blocking collectives  108 us (72%)
  starting transfers between devices  14.3 us (10%)
  between operations  14.1 us (9%)
  Pallas kernels  11 us (7%)
    all_to_all x4, blocking collectives, exchange(): return lax.all_to_all(blocks, axes, 0, 0, tiled=True)  50.6 us
    all_gather x1, blocking collectives, shards(): lax.all_gather(early, ('zh', 'c'), axis=0)  48.7 us
    all_to_all x1, starting transfers between devices, exchange(): return lax.all_to_all(blocks, axes, 0, 0, tiled=True)  14.3 us
    all_gather x1, blocking collectives, shards(): part = lax.all_gather(send, 'zo', axis=0)  4.41 us
    all_gather x1, blocking collectives, shards(): gated = lax.all_gather(gated, 'zo', axis=0)  4.35 us
    pallas_call x1, Pallas kernels, mlp(): pl.pallas_call(mlp_body, out_shape=(pltpu.VMEM((groups, rows, width), jnp...  3.63 us
  transfers between devices with their start and end apart: 2, of which 0 were waited for; matrix products, arithmetic and copies ran while one was open for 0% of the time, Pallas kernels for 3%

profile of v3, /device:TPU:2, one launch (start us, length us, event | category | flops | bytes accessed | tf_op | source)
XLA Modules:
  0.0 148.1 jit_solution(10927420319239969773)
XLA Ops:
  7.2 0.0 copy-start
  7.2 0.0 all-gather.5.cloned.1.call-start
  7.2 2.6 %pack.1 = (bf16[64,1024]{1,0:T(8,128)(2,1)}, bf16[56,512]{1,0:T(8,128)(2,1)S(1)}, bf16[16,24,512]{2,1,0:T(8,128)(2,1)}, bf16[32,16,128]{2,1,0:T(8,128)(2,1)S(1)}) custom-call(bf16[16,128]{1,0:T(8,128)(2,1)} %residual.1, bf16[64,128]{1,0:T(8,128)(2,1)} %wq.1, bf16[64,128]{1,0:T(8,128)(2,1)} %wf.1, bf16[64,128]{1,0:T(8,128)(2,1)} %wv.1, bf16[64,128]{1,0:T(8,128)(2,1)} %wg.1, ...), custom_call_target="tpu_custom_call" | custom-call | tf_op jit(solution)/shard_map/pack/pallas_call | solution.py:74
  9.8 0.0 all-gather.5.cloned.1.call-update
  9.8 16.3 %all_to_all.25 = bf16[32,16,128]{2,1,0:T(8,128)(2,1)S(1)} all-to-all(bf16[32,16,128]{2,1,0:T(8,128)(2,1)S(1)} %get-tuple-element.13), channel_id=1, replica_groups=mesh['y'=4,'x'=4,'zh'=8,'zo'=2,'c'=2] {'y','x','zo'}, dimensions={0} | all-to-all | bytes 262144 | tf_op jit(solution)/shard_map/all_to_all | solution.py:20
  26.1 14.3 %all-to-all-start.1 = ((bf16[16,24,512]{2,1,0:T(8,128)(2,1)}), bf16[16,24,512]{2,1,0:T(8,128)(2,1)S(1)}, u32[]{:S(2)}, u32[]{:S(2)}) async-start(bf16[16,24,512]{2,1,0:T(8,128)(2,1)} %get-tuple-element.15), calls=%async_computation.1 | async-start | bytes 786432 | tf_op jit(solution)/shard_map/all_to_all | solution.py:20
  40.4 48.7 %all-gather = bf16[896,512]{1,0:T(8,128)(2,1)S(1)} all-gather(bf16[56,512]{1,0:T(8,128)(2,1)S(1)} %get-tuple-element.14), channel_id=2, replica_groups=mesh['y'=4,'x'=4,'zh'=8,'zo'=2,'c'=2] {'zh','c'}, dimensions={0}, use_global_device_ids=true | all-gather | bytes 974848 | tf_op jit(solution)/shard_map/all_gather | solution.py:346
  89.1 0.0 all-to-all-done.1
  89.1 1.0 project.1
  90.1 4.4 %all-gather.1 = bf16[32,512]{1,0:T(8,128)(2,1)S(1)} all-gather(bf16[16,512]{1,0:T(8,128)(2,1)S(1)} %get-tuple-element.17), channel_id=3, replica_groups=mesh['y'=4,'x'=4,'zh'=8,'zo'=2,'c'=2] {'zo'}, dimensions={0}, use_global_device_ids=true | all-gather | bytes 49152 | tf_op jit(solution)/shard_map/all_gather | solution.py:348
  94.6 0.0 copy-done
  94.6 2.6 %recur.1 = (f32[16,128,128]{2,1,0:T(8,128)}, bf16[16,128]{1,0:T(8,128)(2,1)S(1)}) custom-call(f32[16,512]{1,0:T(8,128)S(1)} %get-tuple-element.16.own_ref, bf16[2,16,512]{2,1,0:T(8,128)(2,1)S(1)} %bitcast.28, f32[16,128,128]{2,1,0:T(8,128)S(1)} %bitcast.25, f32[1,128]{1,0:T(1,128)} %bitcast.37, f32[1,128]{1,0:T(1,128)} %bitcast.38), custom_call_target="tpu_custom_call" | custom-call | tf_op jit(solution)/shard_map/recur/pallas_call | solution.py:171
  97.2 4.3 %all-gather.2 = bf16[32,128]{1,0:T(8,128)(2,1)S(1)} all-gather(bf16[16,128]{1,0:T(8,128)(2,1)S(1)} %get-tuple-element.18), channel_id=4, replica_groups=mesh['y'=4,'x'=4,'zh'=8,'zo'=2,'c'=2] {'zo'}, dimensions={0}, use_global_device_ids=true | all-gather | bytes 12288 | tf_op jit(solution)/shard_map/all_gather | solution.py:352
  101.5 0.2 mix_out.1
  101.8 12.6 %all_to_all.26 = f32[32,8,128]{2,1,0:T(8,128)S(1)} all-to-all(f32[32,8,128]{2,1,0:T(8,128)S(1)} %bitcast.26), channel_id=1, replica_groups=mesh['y'=4,'x'=4,'zh'=8,'zo'=2,'c'=2] {'y','x','zo'}, dimensions={0} | all-to-all | bytes 262144 | tf_op jit(solution)/shard_map/all_to_all | solution.py:20
  114.4 0.9 row_update.1
  115.3 10.9 %all_to_all.27.row_ref = bf16[16,16,128]{2,1,0:T(8,128)(2,1)S(1)} all-to-all(bf16[16,16,128]{2,1,0:T(8,128)(2,1)S(1)} %row_update.1), channel_id=1, replica_groups=mesh['y'=4,'x'=4,'zh'=8,'zo'=2,'c'=2] {'y','x'}, dimensions={0} | all-to-all | bytes 131072 | tf_op jit(solution)/shard_map/all_to_all | solution.py:20
  126.2 0.0 all-gather.5.cloned.1.call-done.long_ref
  126.2 3.6 %mlp.1 = (bf16[16,16,128]{2,1,0:T(8,128)(2,1)S(1)}, f32[16,128]{1,0:T(8,128)S(1)}, f32[1,128]{1,0:T(1,128)S(1)}) custom-call(bf16[16,16,128]{2,1,0:T(8,128)(2,1)S(1)} %all_to_all.27.row_ref, f32[16,128]{1,0:T(8,128)} %bitcast.34, f32[16,128]{1,0:T(8,128)} %bitcast.35, bf16[2048,1024]{1,0:T(8,128)(2,1)} %all-gather.5.cloned.1.call-done.long_ref), custom_call_target="tpu_custom_call" | custom-call | tf_op jit(solution)/shard_map/mlp/pallas_call | solution.py:292
  129.8 10.8 %all_to_all.28 = bf16[16,16,128]{2,1,0:T(8,128)(2,1)S(1)} all-to-all(bf16[16,16,128]{2,1,0:T(8,128)(2,1)S(1)} %get-tuple-element.21), channel_id=1, replica_groups=mesh['y'=4,'x'=4,'zh'=8,'zo'=2,'c'=2] {'y','x'}, dimensions={0} | all-to-all | bytes 131072 | tf_op jit(solution)/shard_map/all_to_all | solution.py:20
  140.6 0.6 add_convert_fusion
  (1 shorter events, 0.0 us)
Async XLA Ops:
  7.2 87.4 %copy-start = (f32[16,1,128,128]{3,2,1,0:T(8,128)S(1)}, f32[16,1,128,128]{3,2,1,0:T(8,128)}, u32[]{:S(2)}) copy-start(f32[16,1,128,128]{3,2,1,0:T(8,128)} %param.16) | copy-start | bytes 3145732
  7.2 119.0 %all-gather.5.cloned.1.call-start = ((), (), s32[]{:S(2)}) async-start(), calls=%async_computation.5 | async-start | bytes 4325376 | tf_op jit(solution)/shard_map/all_gather | solution.py:343
  26.1 63.0 %all-to-all-start.1 = ((bf16[16,24,512]{2,1,0:T(8,128)(2,1)}), bf16[16,24,512]{2,1,0:T(8,128)(2,1)S(1)}, u32[]{:S(2)}, u32[]{:S(2)}) async-start(bf16[16,24,512]{2,1,0:T(8,128)(2,1)} %get-tuple-element.15), calls=%async_computation.1 | async-start | bytes 786432 | tf_op jit(solution)/shard_map/all_to_all | solution.py:20
Sparse Core Ops, SparseCore 0:
  10.1 92.5 all-gather.4

commit v4 on v3

--- a/solution.py
+++ b/solution.py
@@ -7,11 +7,10 @@
 from jax.sharding import PartitionSpec as P
 
 KV = ("y", "x")
-TP = ("zh", "zo", "c")
-HALVES = 2
-CHIPS = 8
+TP = ("za", "zb", "c")
+PARTS = 4
+CHIPS = 4
 CORES = 2
-EARLY = 56
 
 epsilon = 1e-06
 
@@ -34,68 +33,47 @@
 
 
 def pack_body(
-    residual,
-    wq,
-    wf,
-    wv,
-    wg,
-    mix,
-    up,
-    down,
-    long_ref,
-    early_ref,
-    late_ref,
-    spread_ref,
-    stage_ref,
-    sems,
+    residual, wq, wf, wv, wg, mix, up, down, long_ref, short_ref, spread_ref, sems
 ):
     rows, cols = wq.shape
-    rest = rows - EARLY
     part = mix.shape[0] // 4
     hidden = up.shape[1]
     copies = [(up, long_ref.at[:, :hidden]), (down, long_ref.at[:, hidden:])]
     for k, w in enumerate((wq, wf, wv, wg)):
         at = slice(k * cols, (k + 1) * cols)
-        copies.append((w.at[:EARLY], early_ref.at[:, at]))
-        copies.append((w.at[EARLY:], stage_ref.at[:rest, at]))
-        copies.append((mix.at[k * part : (k + 1) * part], stage_ref.at[rest:, at]))
+        copies.append((w, short_ref.at[:rows, at]))
+        copies.append((mix.at[k * part : (k + 1) * part], short_ref.at[rows:, at]))
     started = run_copies(copies, sems)
     spread_ref[...] = jnp.broadcast_to(residual[...][None], spread_ref.shape)
     for copy in started:
         copy.wait()
-    late_ref[...] = jnp.broadcast_to(stage_ref[...][None], late_ref.shape)
-
-
-def pack(residual, wq, wf, wv, wg, mix, up, down, peers, sharers):
+
+
+def pack(residual, wq, wf, wv, wg, mix, up, down, peers):
     rows, cols = wq.shape
-    late = rows - EARLY + mix.shape[0] // 4
     anywhere = pl.BlockSpec(memory_space=pl.ANY)
     vmem = pl.BlockSpec(memory_space=pltpu.VMEM)
     return pl.pallas_call(
         pack_body,
         out_shape=(
             jax.ShapeDtypeStruct((rows, up.shape[1] + down.shape[1]), up.dtype),
-            pltpu.VMEM((EARLY, 4 * cols), wq.dtype),
-            pltpu.VMEM((sharers, late, 4 * cols), wq.dtype),
+            pltpu.VMEM((rows + mix.shape[0] // 4, 4 * cols), wq.dtype),
             pltpu.VMEM((peers, *residual.shape), residual.dtype),
         ),
         in_specs=[vmem] + [anywhere] * 7,
-        out_specs=(vmem,) * 4,
-        scratch_shapes=[
-            pltpu.VMEM((late, 4 * cols), wq.dtype),
-            pltpu.SemaphoreType.DMA((14,)),
-        ],
+        out_specs=(vmem,) * 3,
+        scratch_shapes=[pltpu.SemaphoreType.DMA((10,))],
         name="pack",
     )(residual, wq, wf, wv, wg, mix, up, down)
 
 
-def project_body(x_ref, gain_ref, early_ref, late_ref, own_ref, send_ref):
-    zo = lax.axis_index("zo")
+def project_body(x_ref, gain_ref, short_ref, out_ref):
+    zb = lax.axis_index("zb")
     groups, _, height, width = x_ref.shape
-    rest = late_ref.shape[2] - width // 8
-    squares = [None] * HALVES
+    rows = width // CORES
+    squares = [None] * PARTS
     for f in range(groups):
-        for h in range(HALVES):
+        for h in range(PARTS):
             x = x_ref[f, h].astype(jnp.float32)
             squares[h] = x * x if f == 0 else squares[h] + x * x
     scale = [
@@ -104,49 +82,34 @@
     ]
     total = None
     for k in range(CHIPS):
-        f = HALVES * k + zo
+        f = PARTS * k + zb
         gain = gain_ref[pl.ds(f, 1)]
         x = jnp.concatenate(
             [
                 (x_ref[f, h].astype(jnp.float32) * scale[h] * gain).astype(jnp.bfloat16)
-                for h in range(HALVES)
+                for h in range(PARTS)
             ],
             axis=0,
         )
-        w = jnp.concatenate(
-            [
-                piece
-                for c in range(CORES)
-                for piece in (early_ref[k, c], late_ref[k, c, :rest])
-            ],
-            axis=0,
-        )
+        w = jnp.concatenate([short_ref[k, c, :rows] for c in range(CORES)], axis=0)
         term = jnp.dot(x, w, preferred_element_type=jnp.float32)
         total = term if total is None else total + term
-    mine = jnp.where(zo == 0, total[:height], total[height:])
-    other = jnp.where(zo == 0, total[height:], total[:height])
-    own_ref[...] = mine
-    send_ref[...] = other.astype(send_ref.dtype)
-
-
-def project(x, gain, early, late):
-    height = x.shape[2]
-    cols = early.shape[3]
+    for h in range(PARTS):
+        out_ref[h] = total[h * height : (h + 1) * height].astype(out_ref.dtype)
+
+
+def project(x, gain, short):
     return pl.pallas_call(
         project_body,
-        out_shape=(
-            pltpu.VMEM((height, cols), jnp.float32),
-            pltpu.VMEM((height, cols), jnp.bfloat16),
-        ),
+        out_shape=pltpu.VMEM((PARTS, x.shape[2], short.shape[3]), jnp.bfloat16),
         name="project",
-    )(near(x), gain, near(early), near(late))
-
-
-def recur_body(
-    own_ref, part_ref, prior_ref, floor_ref, gain_ref, state_ref, out_ref, read_ref
-):
-    zo = lax.axis_index("zo")
-    pre = own_ref[...] + part_ref[1 - zo].astype(jnp.float32)
+    )(near(x), gain, near(short))
+
+
+def recur_body(part_ref, prior_ref, floor_ref, gain_ref, state_ref, out_ref, read_ref):
+    pre = part_ref[0].astype(jnp.float32)
+    for k in range(1, PARTS):
+        pre = pre + part_ref[k].astype(jnp.float32)
     pre = pre.astype(jnp.bfloat16).astype(jnp.float32)
     width = prior_ref.shape[1]
     query = jax.nn.silu(pre[:, :width])
@@ -163,64 +126,65 @@
         read_ref[b : b + 1] = jnp.sum(query_t[:, b : b + 1] * state, axis=0, keepdims=True)
     read = read_ref[...]
     scale = lax.rsqrt(jnp.mean(read * read, axis=-1, keepdims=True) + epsilon)
-    out_ref[...] = (read * scale * gain_ref[...] * gate).astype(out_ref.dtype)
-
-
-def recur(own, part, prior, floor, gain):
+    gated = (read * scale * gain_ref[...] * gate).astype(out_ref.dtype)
+    out_ref[...] = jnp.broadcast_to(gated[None], out_ref.shape)
+
+
+def recur(part, prior, floor, gain):
     rows, width, _ = prior.shape
     return pl.pallas_call(
         recur_body,
         out_shape=(
             jax.ShapeDtypeStruct(prior.shape, jnp.float32),
-            pltpu.VMEM((rows, width), jnp.bfloat16),
+            pltpu.VMEM((PARTS, rows, width), jnp.bfloat16),
         ),
         scratch_shapes=[pltpu.VMEM((rows, width), jnp.float32)],
         name="recur",
-    )(near(own), near(part), near(prior), floor, gain)
-
-
-def mix_body(gated_ref, late_ref, out_ref, order_ref):
+    )(near(part), near(prior), floor, gain)
+
+
+def mix_body(gated_ref, short_ref, out_ref, order_ref):
     height, width = gated_ref.shape[1:]
-    rest = late_ref.shape[2] - width // 8
-    for h in range(HALVES):
-        order_ref[pl.ds(h, height, stride=HALVES)] = gated_ref[h].astype(jnp.float32)
+    rows = width // CORES
+    for h in range(PARTS):
+        order_ref[pl.ds(h, height, stride=PARTS)] = gated_ref[h].astype(jnp.float32)
     left = order_ref[...].astype(jnp.bfloat16)
     for k in range(CHIPS):
         right = jnp.concatenate(
             [
-                late_ref[k, c, rest:, j * width : (j + 1) * width]
+                short_ref[k, c, rows:, j * width : (j + 1) * width]
                 for c in range(CORES)
                 for j in range(4)
             ],
             axis=0,
         )
-        out_ref[pl.ds(k, HALVES * height, stride=CHIPS)] = lax.dot_general(
+        out_ref[pl.ds(k, PARTS * height, stride=CHIPS)] = lax.dot_general(
             left, right, (((1,), (1,)), ((), ())), preferred_element_type=jnp.float32
         )
 
 
-def mix_out(gated, late):
+def mix_out(gated, short):
     height, width = gated.shape[1:]
     return pl.pallas_call(
         mix_body,
-        out_shape=pltpu.VMEM((CHIPS * HALVES * height, width), jnp.float32),
-        scratch_shapes=[pltpu.VMEM((HALVES * height, width), jnp.float32)],
+        out_shape=pltpu.VMEM((CHIPS * PARTS * height, width), jnp.float32),
+        scratch_shapes=[pltpu.VMEM((PARTS * height, width), jnp.float32)],
         name="mix_out",
-    )(near(gated), near(late))
+    )(near(gated), near(short))
 
 
 def row_body(sums_ref, x_ref, gain_ref, out_ref, mixed_ref):
-    zo = lax.axis_index("zo")
+    zb = lax.axis_index("zb")
     place = lax.axis_index("y") * lax.axis_size("x") + lax.axis_index("x")
     groups, width = gain_ref.shape
-    for h in range(HALVES):
-        total = sums_ref[0, h]
-        for k in range(1, groups):
-            total = total + sums_ref[k, h]
-        mixed_ref[pl.ds(h, CHIPS, stride=HALVES)] = total
+    total = sums_ref[:groups]
+    for k in range(1, groups):
+        total = total + sums_ref[k * groups : (k + 1) * groups]
+    for h in range(PARTS):
+        mixed_ref[pl.ds(h, CHIPS, stride=PARTS)] = total[h * CHIPS : (h + 1) * CHIPS]
     mixed = mixed_ref[...]
     scale = lax.rsqrt(jnp.sum(mixed * mixed) / gain_ref.size + epsilon)
-    stream = x_ref[:, zo].astype(jnp.float32)
+    stream = x_ref[:, zb].astype(jnp.float32)
     at = lax.broadcasted_iota(jnp.int32, stream.shape, 1) == place
     row = jnp.sum(jnp.where(at, stream, 0.0), axis=1)
     after = (row + mixed * scale * gain_ref[...]).astype(out_ref.dtype)
@@ -328,7 +292,7 @@
     groups = lax.axis_size(KV)
     hidden = w_up.shape[1]
 
-    long, early, late, spread = pack(
+    long, short, spread = pack(
         residual,
         w_query,
         w_forget,
@@ -337,22 +301,20 @@
         w_mix_out.T,
         w_up,
         w_down.T,
-        groups * HALVES,
-        CHIPS * CORES,
+        groups * PARTS,
     )
     long = lax.all_gather(long, TP, axis=0, tiled=True)
-    stream = exchange(spread, (*KV, "zo")).reshape(groups, HALVES, batch_rows, own_cols)
-    late = exchange(late, ("zh", "c")).reshape(CHIPS, CORES, *late.shape[1:])
-    early = lax.all_gather(early, ("zh", "c"), axis=0).reshape(CHIPS, CORES, *early.shape)
-    own, send = project(stream, gain_mix_pre.reshape(groups, own_cols), early, late)
-    part = lax.all_gather(send, "zo", axis=0)
+    stream = exchange(spread, (*KV, "zb")).reshape(groups, PARTS, batch_rows, own_cols)
+    short = lax.all_gather(short, ("za", "c"), axis=0).reshape(CHIPS, CORES, *short.shape)
+    part = exchange(project(stream, gain_mix_pre.reshape(groups, own_cols), short), "zb")
     new_state, gated = recur(
-        own, part, prior_state[:, 0], forget_floor[None], group_gain[None]
-    )
-    gated = lax.all_gather(gated, "zo", axis=0)
-    mixed_part = mix_out(gated, late).reshape(groups * HALVES, CHIPS, own_cols)
-    mixed = exchange(mixed_part, (*KV, "zo")).reshape(groups, HALVES, CHIPS, own_cols)
-    after_row = row_update(mixed, stream, gain_mix_post.reshape(groups, own_cols))
+        part, prior_state[:, 0], forget_floor[None], group_gain[None]
+    )
+    mixed_part = mix_out(exchange(gated, "zb"), short)
+    mixed = exchange(mixed_part.reshape(groups * PARTS, CHIPS, own_cols), (*KV, "zb"))
+    after_row = row_update(
+        mixed.reshape(-1, own_cols), stream, gain_mix_post.reshape(groups, own_cols)
+    )
     channel_part, after_own, out_gain = mlp(
         exchange(after_row, KV),
         gain_mlp_pre.reshape(groups, own_cols),
@@ -366,7 +328,7 @@
 
 
 def solution(mesh):
-    grid = Mesh(mesh.devices.reshape(4, 4, CHIPS, HALVES, CORES), (*KV, *TP))
+    grid = Mesh(mesh.devices.reshape(4, 4, CHIPS, PARTS, CORES), (*KV, *TP))
     return jax.shard_map(
         shards,
         mesh=grid,

time: 149 us -> 130 us (0.87)
  blocking collectives: 108 us -> 90.2 us
  starting transfers between devices: 14.3 us -> 12.1 us
    all_gather x3 -> x1, blocking collectives: 57.5 us -> 26.4 us  [shards(): lax.all_gather(short, ('za', 'c'), axis=0)]
    all_to_all x4 -> x5, blocking collectives: 50.6 us -> 63.9 us  [exchange(): return lax.all_to_all(blocks, axes, 0, 0, tiled=True)]
    all_to_all x1, starting transfers between devices: 14.3 us -> 12.1 us  [exchange(): return lax.all_to_all(blocks, axes, 0, 0, tiled=True)]
  transfers between devices with their start and end apart: 2 -> 2, of which waited for: 0 -> 0; matrix products, arithmetic and copies ran while one was open for 0% -> 0% of each run, Pallas kernels for 3% -> 4%
where the time goes in v4:
time: 130 us; the launch traced here: 129 us
  blocking collectives  90.2 us (69%)
  between operations  14.1 us (11%)
  starting transfers between devices  12.1 us (9%)
  Pallas kernels  10.7 us (8%)
    all_to_all x5, blocking collectives, exchange(): return lax.all_to_all(blocks, axes, 0, 0, tiled=True)  63.9 us
    all_gather x1, blocking collectives, shards(): lax.all_gather(short, ('za', 'c'), axis=0)  26.4 us
    all_to_all x1, starting transfers between devices, exchange(): return lax.all_to_all(blocks, axes, 0, 0, tiled=True)  12.1 us
    pallas_call x1, Pallas kernels, mlp(): pl.pallas_call(mlp_body, out_shape=(pltpu.VMEM((groups, rows, width), jnp...  3.63 us
    pallas_call x1, Pallas kernels, recur(): pl.pallas_call(recur_body, out_shape=(jax.ShapeDtypeStruct(prior.shape, j...  2.62 us
  transfers between devices with their start and end apart: 2, of which 0 were waited for; matrix products, arithmetic and copies ran while one was open for 0% of the time, Pallas kernels for 4%

profile of v4, /device:TPU:2, one launch (start us, length us, event | category | flops | bytes accessed | tf_op | source)
XLA Modules:
  0.0 129.0 jit_solution(3649593851365751715)
XLA Ops:
  7.2 0.0 all-gather.3.cloned.1.call-start
  7.2 2.4 %pack.1 = (bf16[64,1024]{1,0:T(8,128)(2,1)}, bf16[80,512]{1,0:T(8,128)(2,1)S(1)}, bf16[64,16,128]{2,1,0:T(8,128)(2,1)}) custom-call(bf16[16,128]{1,0:T(8,128)(2,1)} %residual.1, bf16[64,128]{1,0:T(8,128)(2,1)} %wq.1, bf16[64,128]{1,0:T(8,128)(2,1)} %wf.1, bf16[64,128]{1,0:T(8,128)(2,1)} %wv.1, bf16[64,128]{1,0:T(8,128)(2,1)} %wg.1, ...), custom_call_target="tpu_custom_call" | custom-call | tf_op jit(solution)/shard_map/pack/pallas_call | solution.py:56
  9.6 0.0 all-gather.3.cloned.1.call-update
  9.7 12.1 %all-to-all-start = ((bf16[64,16,128]{2,1,0:T(8,128)(2,1)}), bf16[64,16,128]{2,1,0:T(8,128)(2,1)S(1)}, u32[]{:S(2)}, u32[]{:S(2)}) async-start(bf16[64,16,128]{2,1,0:T(8,128)(2,1)} %get-tuple-element.10), calls=%async_computation | async-start | bytes 524288 | tf_op jit(solution)/shard_map/all_to_all | solution.py:19
  21.8 26.4 %all-gather = bf16[640,512]{1,0:T(8,128)(2,1)S(1)} all-gather(bf16[80,512]{1,0:T(8,128)(2,1)S(1)} %get-tuple-element.11), channel_id=2, replica_groups=mesh['y'=4,'x'=4,'za'=4,'zb'=4,'c'=2] {'za','c'}, dimensions={0}, use_global_device_ids=true | all-gather | bytes 737280 | tf_op jit(solution)/shard_map/all_gather | solution.py:308
  48.1 0.0 all-to-all-done
  48.1 1.0 project.1
  49.1 16.1 %all_to_all.30.part_ref = bf16[4,16,512]{2,1,0:T(8,128)(2,1)S(1)} all-to-all(bf16[4,16,512]{2,1,0:T(8,128)(2,1)S(1)} %project.1), channel_id=1, replica_groups=mesh['y'=4,'x'=4,'za'=4,'zb'=4,'c'=2] {'zb'}, dimensions={0} | all-to-all | bytes 131072 | tf_op jit(solution)/shard_map/all_to_all | solution.py:19
  65.3 0.0 copy-start
  65.3 1.2 copy-done
  66.5 2.6 %recur.1 = (f32[16,128,128]{2,1,0:T(8,128)}, bf16[4,16,128]{2,1,0:T(8,128)(2,1)S(1)}) custom-call(bf16[4,16,512]{2,1,0:T(8,128)(2,1)S(1)} %all_to_all.30.part_ref, f32[16,128,128]{2,1,0:T(8,128)S(1)} %bitcast.21, f32[1,128]{1,0:T(1,128)} %bitcast.31, f32[1,128]{1,0:T(1,128)} %bitcast.32), custom_call_target="tpu_custom_call" | custom-call | tf_op jit(solution)/shard_map/recur/pallas_call | solution.py:135
  69.1 8.1 %all_to_all.31.gated_ref = bf16[4,16,128]{2,1,0:T(8,128)(2,1)S(1)} all-to-all(bf16[4,16,128]{2,1,0:T(8,128)(2,1)S(1)} %get-tuple-element.12), channel_id=1, replica_groups=mesh['y'=4,'x'=4,'za'=4,'zb'=4,'c'=2] {'zb'}, dimensions={0} | all-to-all | bytes 32768 | tf_op jit(solution)/shard_map/all_to_all | solution.py:19
  77.2 0.2 mix_out.1
  77.3 18.1 %all_to_all.32 = f32[64,4,128]{2,1,0:T(4,128)S(1)} all-to-all(f32[64,4,128]{2,1,0:T(4,128)S(1)} %bitcast.22), channel_id=1, replica_groups=mesh['y'=4,'x'=4,'za'=4,'zb'=4,'c'=2] {'y','x','zb'}, dimensions={0} | all-to-all | bytes 262144 | tf_op jit(solution)/shard_map/all_to_all | solution.py:19
  95.5 0.9 row_update.1
  96.4 10.8 %all_to_all.33.row_ref = bf16[16,16,128]{2,1,0:T(8,128)(2,1)S(1)} all-to-all(bf16[16,16,128]{2,1,0:T(8,128)(2,1)S(1)} %row_update.1), channel_id=1, replica_groups=mesh['y'=4,'x'=4,'za'=4,'zb'=4,'c'=2] {'y','x'}, dimensions={0} | all-to-all | bytes 131072 | tf_op jit(solution)/shard_map/all_to_all | solution.py:19
  107.1 0.0 all-gather.3.cloned.1.call-done.long_ref
  107.1 3.6 %mlp.1 = (bf16[16,16,128]{2,1,0:T(8,128)(2,1)S(1)}, f32[16,128]{1,0:T(8,128)S(1)}, f32[1,128]{1,0:T(1,128)S(1)}) custom-call(bf16[16,16,128]{2,1,0:T(8,128)(2,1)S(1)} %all_to_all.33.row_ref, f32[16,128]{1,0:T(8,128)} %bitcast.29, f32[16,128]{1,0:T(8,128)} %bitcast.30, bf16[2048,1024]{1,0:T(8,128)(2,1)} %all-gather.3.cloned.1.call-done.long_ref), custom_call_target="tpu_custom_call" | custom-call | tf_op jit(solution)/shard_map/mlp/pallas_call | solution.py:256
  110.8 10.8 %all_to_all.34 = bf16[16,16,128]{2,1,0:T(8,128)(2,1)S(1)} all-to-all(bf16[16,16,128]{2,1,0:T(8,128)(2,1)S(1)} %get-tuple-element.15), channel_id=1, replica_groups=mesh['y'=4,'x'=4,'za'=4,'zb'=4,'c'=2] {'y','x'}, dimensions={0} | all-to-all | bytes 131072 | tf_op jit(solution)/shard_map/all_to_all | solution.py:19
  121.6 0.6 add_convert_fusion
  (1 shorter events, 0.0 us)
Async XLA Ops:
  7.2 100.0 %all-gather.3.cloned.1.call-start = ((), (), s32[]{:S(2)}) async-start(), calls=%async_computation.6 | async-start | bytes 4325376 | tf_op jit(solution)/shard_map/all_gather | solution.py:306
  9.7 38.5 %all-to-all-start = ((bf16[64,16,128]{2,1,0:T(8,128)(2,1)}), bf16[64,16,128]{2,1,0:T(8,128)(2,1)S(1)}, u32[]{:S(2)}, u32[]{:S(2)}) async-start(bf16[64,16,128]{2,1,0:T(8,128)(2,1)} %get-tuple-element.10), calls=%async_computation | async-start | bytes 524288 | tf_op jit(solution)/shard_map/all_to_all | solution.py:19
  65.3 1.2 copy-start
Sparse Core Ops, SparseCore 0:
  10.1 80.8 all-gather.2

commit v5 on v4

--- a/solution.py
+++ b/solution.py
@@ -11,6 +11,8 @@
 PARTS = 4
 CHIPS = 4
 CORES = 2
+SLAB = 4
+PIECES = 4
 
 epsilon = 1e-06
 
@@ -106,7 +108,26 @@
     )(near(x), gain, near(short))
 
 
-def recur_body(part_ref, prior_ref, floor_ref, gain_ref, state_ref, out_ref, read_ref):
+def recur_body(
+    part_ref,
+    prior,
+    floor_ref,
+    gain_ref,
+    state,
+    out_ref,
+    prior_ref,
+    state_ref,
+    read_ref,
+    in_sems,
+    out_sems,
+):
+    rows = prior_ref.shape[0]
+    chunks = [slice(k, k + SLAB) for k in range(0, rows, SLAB)]
+    fetches = run_copies([(prior.at[c], prior_ref.at[c]) for c in chunks], in_sems)
+    stores = [
+        pltpu.make_async_copy(state_ref.at[c], state.at[c], out_sems.at[k])
+        for k, c in enumerate(chunks)
+    ]
     pre = part_ref[0].astype(jnp.float32)
     for k in range(1, PARTS):
         pre = pre + part_ref[k].astype(jnp.float32)
@@ -119,28 +140,44 @@
     gate = jax.nn.sigmoid(pre[:, 3 * width :])
     forget_t = forget.T
     query_t = query.T
-    for b in range(prior_ref.shape[0]):
+    for b in range(rows):
+        if b % SLAB == 0:
+            fetches[b // SLAB].wait()
         keep = forget_t[:, b : b + 1]
-        state = keep * prior_ref[b] + (1.0 - keep) * value[b : b + 1]
-        state_ref[b] = state
-        read_ref[b : b + 1] = jnp.sum(query_t[:, b : b + 1] * state, axis=0, keepdims=True)
+        fresh = keep * prior_ref[b] + (1.0 - keep) * value[b : b + 1]
+        state_ref[b] = fresh
+        read_ref[b : b + 1] = jnp.sum(query_t[:, b : b + 1] * fresh, axis=0, keepdims=True)
+        if b % SLAB == SLAB - 1:
+            stores[b // SLAB].start()
     read = read_ref[...]
     scale = lax.rsqrt(jnp.mean(read * read, axis=-1, keepdims=True) + epsilon)
     gated = (read * scale * gain_ref[...] * gate).astype(out_ref.dtype)
     out_ref[...] = jnp.broadcast_to(gated[None], out_ref.shape)
+    for store in stores:
+        store.wait()
 
 
 def recur(part, prior, floor, gain):
     rows, width, _ = prior.shape
+    anywhere = pl.BlockSpec(memory_space=pl.ANY)
+    vmem = pl.BlockSpec(memory_space=pltpu.VMEM)
     return pl.pallas_call(
         recur_body,
         out_shape=(
             jax.ShapeDtypeStruct(prior.shape, jnp.float32),
             pltpu.VMEM((PARTS, rows, width), jnp.bfloat16),
         ),
-        scratch_shapes=[pltpu.VMEM((rows, width), jnp.float32)],
+        in_specs=[vmem, anywhere, vmem, vmem],
+        out_specs=(anywhere, vmem),
+        scratch_shapes=[
+            pltpu.VMEM(prior.shape, jnp.float32),
+            pltpu.VMEM(prior.shape, jnp.float32),
+            pltpu.VMEM((rows, width), jnp.float32),
+            pltpu.SemaphoreType.DMA((rows // SLAB,)),
+            pltpu.SemaphoreType.DMA((rows // SLAB,)),
+        ],
         name="recur",
-    )(near(part), near(prior), floor, gain)
+    )(near(part), prior, floor, gain)
 
 
 def mix_body(gated_ref, short_ref, out_ref, order_ref):
@@ -218,8 +255,12 @@
     groups, width = pre_ref.shape
     height = row_ref.shape[0]
     units = up_ref.shape[1]
+    full = groups * width
+    pieces = [slice(k, k + full // PIECES) for k in range(0, full, full // PIECES)]
     copies = run_copies(
-        [(long_ref.at[:, :units], up_ref), (long_ref.at[:, units:], down_ref)], sems
+        [(long_ref.at[p, :units], up_ref.at[p]) for p in pieces]
+        + [(long_ref.at[p, units:], down_ref.at[p]) for p in pieces],
+        sems,
     )
     for row in range(height):
         after_ref[row * groups : (row + 1) * groups] = row_ref[row].astype(jnp.float32)
@@ -228,7 +269,7 @@
     for f in range(1, groups):
         squares = squares + after[f] * after[f]
     scale = lax.rsqrt(
-        jnp.sum(squares, axis=-1, keepdims=True) / (groups * width) + epsilon
+        jnp.sum(squares, axis=-1, keepdims=True) / full + epsilon
     )
     hidden = jnp.concatenate(
         [
@@ -239,15 +280,21 @@
     )
     own_ref[...] = after_ref[pl.ds(place, height, stride=groups)]
     gain_ref[...] = post_ref[pl.ds(place, 1)]
-    copies[0].wait()
-    up = jnp.dot(hidden, up_ref[...], preferred_element_type=jnp.float32)
+    up = None
+    for k, p in enumerate(pieces):
+        copies[k].wait()
+        term = jnp.dot(hidden[:, p], up_ref[p], preferred_element_type=jnp.float32)
+        up = term if up is None else up + term
     squared = jnp.square(jnp.maximum(up, 0.0)).astype(jnp.bfloat16)
-    copies[1].wait()
-    channel = lax.dot_general(
-        squared, down_ref[...], (((1,), (1,)), ((), ())), preferred_element_type=jnp.float32
-    )
-    for f in range(groups):
-        out_ref[f] = channel[:, f * width : (f + 1) * width].astype(out_ref.dtype)
+    for k, p in enumerate(pieces):
+        copies[PIECES + k].wait()
+        channel = lax.dot_general(
+            squared, down_ref[p], (((1,), (1,)), ((), ())), preferred_element_type=jnp.float32
+        )
+        for f in range(groups // PIECES):
+            out_ref[k * (groups // PIECES) + f] = channel[
+                :, f * width : (f + 1) * width
+            ].astype(out_ref.dtype)
 
 
 def mlp(after, pre, post, weights, hidden):
@@ -265,7 +312,7 @@
             pltpu.VMEM((rows * groups, width), jnp.float32),
             pltpu.VMEM((weights.shape[0], hidden), jnp.bfloat16),
             pltpu.VMEM((weights.shape[0], hidden), jnp.bfloat16),
-            pltpu.SemaphoreType.DMA((2,)),
+            pltpu.SemaphoreType.DMA((2 * PIECES,)),
         ],
         name="mlp",
     )(near(after), pre, post, weights)

time: 130 us -> 129 us (level)
  no operation moved by 1% of the time
where the time goes in v5:
time: 129 us; the launch traced here: 128 us
  blocking collectives  90.1 us (70%)
  between operations  14.1 us (11%)
  starting transfers between devices  12.1 us (9%)
  Pallas kernels  11.5 us (9%)
    all_to_all x5, blocking collectives, exchange(): return lax.all_to_all(blocks, axes, 0, 0, tiled=True)  63.8 us
    all_gather x1, blocking collectives, shards(): lax.all_gather(short, ('za', 'c'), axis=0)  26.4 us
    all_to_all x1, starting transfers between devices, exchange(): return lax.all_to_all(blocks, axes, 0, 0, tiled=True)  12.1 us
    pallas_call x1, Pallas kernels, mlp(): pl.pallas_call(mlp_body, out_shape=(pltpu.VMEM((groups, rows, width), jnp...  3.54 us
    pallas_call x1, Pallas kernels, recur(): pl.pallas_call(recur_body, out_shape=(jax.ShapeDtypeStruct(prior.shape, j...  3.52 us
  transfers between devices with their start and end apart: 2, of which 0 were waited for; matrix products, arithmetic and copies ran while one was open for 0% of the time, Pallas kernels for 4%

profile of v5, /device:TPU:2, one launch (start us, length us, event | category | flops | bytes accessed | tf_op | source)
XLA Modules:
  0.0 128.5 jit_solution(2543196833094172650)
XLA Ops:
  7.2 0.0 all-gather.3.cloned.1.call-start
  7.2 2.4 %pack.1 = (bf16[64,1024]{1,0:T(8,128)(2,1)}, bf16[80,512]{1,0:T(8,128)(2,1)S(1)}, bf16[64,16,128]{2,1,0:T(8,128)(2,1)}) custom-call(bf16[16,128]{1,0:T(8,128)(2,1)} %residual.1, bf16[64,128]{1,0:T(8,128)(2,1)} %wq.1, bf16[64,128]{1,0:T(8,128)(2,1)} %wf.1, bf16[64,128]{1,0:T(8,128)(2,1)} %wv.1, bf16[64,128]{1,0:T(8,128)(2,1)} %wg.1, ...), custom_call_target="tpu_custom_call" | custom-call | tf_op jit(solution)/shard_map/pack/pallas_call | solution.py:58
  9.6 0.0 all-gather.3.cloned.1.call-update
  9.7 12.1 %all-to-all-start = ((bf16[64,16,128]{2,1,0:T(8,128)(2,1)}), bf16[64,16,128]{2,1,0:T(8,128)(2,1)S(1)}, u32[]{:S(2)}, u32[]{:S(2)}) async-start(bf16[64,16,128]{2,1,0:T(8,128)(2,1)} %get-tuple-element.10), calls=%async_computation | async-start | bytes 524288 | tf_op jit(solution)/shard_map/all_to_all | solution.py:21
  21.8 26.4 %all-gather = bf16[640,512]{1,0:T(8,128)(2,1)S(1)} all-gather(bf16[80,512]{1,0:T(8,128)(2,1)S(1)} %get-tuple-element.11), channel_id=2, replica_groups=mesh['y'=4,'x'=4,'za'=4,'zb'=4,'c'=2] {'za','c'}, dimensions={0}, use_global_device_ids=true | all-gather | bytes 737280 | tf_op jit(solution)/shard_map/all_gather | solution.py:355
  48.1 0.0 all-to-all-done
  48.1 1.0 project.1
  49.1 16.1 %all_to_all.30.part_ref = bf16[4,16,512]{2,1,0:T(8,128)(2,1)S(1)} all-to-all(bf16[4,16,512]{2,1,0:T(8,128)(2,1)S(1)} %project.1), channel_id=1, replica_groups=mesh['y'=4,'x'=4,'za'=4,'zb'=4,'c'=2] {'zb'}, dimensions={0} | all-to-all | bytes 131072 | tf_op jit(solution)/shard_map/all_to_all | solution.py:21
  65.3 3.5 %recur.1 = (f32[16,128,128]{2,1,0:T(8,128)}, bf16[4,16,128]{2,1,0:T(8,128)(2,1)S(1)}) custom-call(bf16[4,16,512]{2,1,0:T(8,128)(2,1)S(1)} %all_to_all.30.part_ref, f32[16,128,128]{2,1,0:T(8,128)} %bitcast.24, f32[1,128]{1,0:T(1,128)} %bitcast.31, f32[1,128]{1,0:T(1,128)} %bitcast.32), custom_call_target="tpu_custom_call" | custom-call | tf_op jit(solution)/shard_map/recur/pallas_call | solution.py:164
  68.8 8.0 %all_to_all.31.gated_ref = bf16[4,16,128]{2,1,0:T(8,128)(2,1)S(1)} all-to-all(bf16[4,16,128]{2,1,0:T(8,128)(2,1)S(1)} %get-tuple-element.12), channel_id=1, replica_groups=mesh['y'=4,'x'=4,'za'=4,'zb'=4,'c'=2] {'zb'}, dimensions={0} | all-to-all | bytes 32768 | tf_op jit(solution)/shard_map/all_to_all | solution.py:21
  76.7 0.2 mix_out.1
  76.9 18.1 %all_to_all.32 = f32[64,4,128]{2,1,0:T(4,128)S(1)} all-to-all(f32[64,4,128]{2,1,0:T(4,128)S(1)} %bitcast.21), channel_id=1, replica_groups=mesh['y'=4,'x'=4,'za'=4,'zb'=4,'c'=2] {'y','x','zb'}, dimensions={0} | all-to-all | bytes 262144 | tf_op jit(solution)/shard_map/all_to_all | solution.py:21
  95.0 0.9 row_update.1
  95.9 10.7 %all_to_all.33.row_ref = bf16[16,16,128]{2,1,0:T(8,128)(2,1)S(1)} all-to-all(bf16[16,16,128]{2,1,0:T(8,128)(2,1)S(1)} %row_update.1), channel_id=1, replica_groups=mesh['y'=4,'x'=4,'za'=4,'zb'=4,'c'=2] {'y','x'}, dimensions={0} | all-to-all | bytes 131072 | tf_op jit(solution)/shard_map/all_to_all | solution.py:21
  106.7 0.0 all-gather.3.cloned.1.call-done.long_ref
  106.7 3.5 %mlp.1 = (bf16[16,16,128]{2,1,0:T(8,128)(2,1)S(1)}, f32[16,128]{1,0:T(8,128)S(1)}, f32[1,128]{1,0:T(1,128)S(1)}) custom-call(bf16[16,16,128]{2,1,0:T(8,128)(2,1)S(1)} %all_to_all.33.row_ref, f32[16,128]{1,0:T(8,128)} %bitcast.29, f32[16,128]{1,0:T(8,128)} %bitcast.30, bf16[2048,1024]{1,0:T(8,128)(2,1)} %all-gather.3.cloned.1.call-done.long_ref), custom_call_target="tpu_custom_call" | custom-call | tf_op jit(solution)/shard_map/mlp/pallas_call | solution.py:303
  110.2 10.8 %all_to_all.34 = bf16[16,16,128]{2,1,0:T(8,128)(2,1)S(1)} all-to-all(bf16[16,16,128]{2,1,0:T(8,128)(2,1)S(1)} %get-tuple-element.15), channel_id=1, replica_groups=mesh['y'=4,'x'=4,'za'=4,'zb'=4,'c'=2] {'y','x'}, dimensions={0} | all-to-all | bytes 131072 | tf_op jit(solution)/shard_map/all_to_all | solution.py:21
  121.1 0.6 add_convert_fusion
  (1 shorter events, 0.0 us)
Async XLA Ops:
  7.2 99.5 %all-gather.3.cloned.1.call-start = ((), (), s32[]{:S(2)}) async-start(), calls=%async_computation.6 | async-start | bytes 4325376 | tf_op jit(solution)/shard_map/all_gather | solution.py:353
  9.7 38.5 %all-to-all-start = ((bf16[64,16,128]{2,1,0:T(8,128)(2,1)}), bf16[64,16,128]{2,1,0:T(8,128)(2,1)S(1)}, u32[]{:S(2)}, u32[]{:S(2)}) async-start(bf16[64,16,128]{2,1,0:T(8,128)(2,1)} %get-tuple-element.10), calls=%async_computation | async-start | bytes 524288 | tf_op jit(solution)/shard_map/all_to_all | solution.py:21
Sparse Core Ops, SparseCore 0:
  10.1 80.7 all-gather.2

commit v6 on v5

--- a/solution.py
+++ b/solution.py
@@ -7,10 +7,10 @@
 from jax.sharding import PartitionSpec as P
 
 KV = ("y", "x")
-TP = ("za", "zb", "c")
+TP = ("zh", "zo", "c")
+NEAR = ("zo", "c")
 PARTS = 4
-CHIPS = 4
-CORES = 2
+CHIPS = 8
 SLAB = 4
 PIECES = 4
 
@@ -70,9 +70,9 @@
 
 
 def project_body(x_ref, gain_ref, short_ref, out_ref):
-    zb = lax.axis_index("zb")
+    zo, core = lax.axis_index("zo"), lax.axis_index("c")
     groups, _, height, width = x_ref.shape
-    rows = width // CORES
+    rows = width // 2
     squares = [None] * PARTS
     for f in range(groups):
         for h in range(PARTS):
@@ -82,18 +82,22 @@
         lax.rsqrt(jnp.sum(s, axis=-1, keepdims=True) / (groups * width) + epsilon)
         for s in squares
     ]
+    lane = lax.broadcasted_iota(jnp.int32, (1, width), 1)
+    here = (lane >= rows) == (core == 1)
     total = None
     for k in range(CHIPS):
-        f = PARTS * k + zb
+        f = 2 * k + zo
         gain = gain_ref[pl.ds(f, 1)]
         x = jnp.concatenate(
             [
-                (x_ref[f, h].astype(jnp.float32) * scale[h] * gain).astype(jnp.bfloat16)
+                jnp.where(
+                    here, x_ref[f, h].astype(jnp.float32) * scale[h] * gain, 0.0
+                ).astype(jnp.bfloat16)
                 for h in range(PARTS)
             ],
             axis=0,
         )
-        w = jnp.concatenate([short_ref[k, c, :rows] for c in range(CORES)], axis=0)
+        w = jnp.concatenate([short_ref[k, :rows]] * 2, axis=0)
         term = jnp.dot(x, w, preferred_element_type=jnp.float32)
         total = term if total is None else total + term
     for h in range(PARTS):
@@ -103,7 +107,7 @@
 def project(x, gain, short):
     return pl.pallas_call(
         project_body,
-        out_shape=pltpu.VMEM((PARTS, x.shape[2], short.shape[3]), jnp.bfloat16),
+        out_shape=pltpu.VMEM((PARTS, x.shape[2], short.shape[2]), jnp.bfloat16),
         name="project",
     )(near(x), gain, near(short))
 
@@ -151,8 +155,7 @@
             stores[b // SLAB].start()
     read = read_ref[...]
     scale = lax.rsqrt(jnp.mean(read * read, axis=-1, keepdims=True) + epsilon)
-    gated = (read * scale * gain_ref[...] * gate).astype(out_ref.dtype)
-    out_ref[...] = jnp.broadcast_to(gated[None], out_ref.shape)
+    out_ref[...] = (read * scale * gain_ref[...] * gate).astype(out_ref.dtype)
     for store in stores:
         store.wait()
 
@@ -165,7 +168,7 @@
         recur_body,
         out_shape=(
             jax.ShapeDtypeStruct(prior.shape, jnp.float32),
-            pltpu.VMEM((PARTS, rows, width), jnp.bfloat16),
+            pltpu.VMEM((rows, width), jnp.bfloat16),
         ),
         in_specs=[vmem, anywhere, vmem, vmem],
         out_specs=(anywhere, vmem),
@@ -182,20 +185,20 @@
 
 def mix_body(gated_ref, short_ref, out_ref, order_ref):
     height, width = gated_ref.shape[1:]
-    rows = width // CORES
+    rows = width // 2
     for h in range(PARTS):
         order_ref[pl.ds(h, height, stride=PARTS)] = gated_ref[h].astype(jnp.float32)
     left = order_ref[...].astype(jnp.bfloat16)
-    for k in range(CHIPS):
+    for k in range(CHIPS // 2):
         right = jnp.concatenate(
             [
-                short_ref[k, c, rows:, j * width : (j + 1) * width]
-                for c in range(CORES)
+                short_ref[2 * k + half, rows:, j * width : (j + 1) * width]
+                for half in range(2)
                 for j in range(4)
             ],
             axis=0,
         )
-        out_ref[pl.ds(k, PARTS * height, stride=CHIPS)] = lax.dot_general(
+        out_ref[pl.ds(k, PARTS * height, stride=CHIPS // 2)] = lax.dot_general(
             left, right, (((1,), (1,)), ((), ())), preferred_element_type=jnp.float32
         )
 
@@ -204,24 +207,31 @@
     height, width = gated.shape[1:]
     return pl.pallas_call(
         mix_body,
-        out_shape=pltpu.VMEM((CHIPS * PARTS * height, width), jnp.float32),
+        out_shape=pltpu.VMEM((CHIPS // 2 * PARTS * height, width), jnp.float32),
         scratch_shapes=[pltpu.VMEM((PARTS * height, width), jnp.float32)],
         name="mix_out",
     )(near(gated), near(short))
 
 
 def row_body(sums_ref, x_ref, gain_ref, out_ref, mixed_ref):
-    zb = lax.axis_index("zb")
+    own = 2 * lax.axis_index("zo") + lax.axis_index("c")
     place = lax.axis_index("y") * lax.axis_size("x") + lax.axis_index("x")
     groups, width = gain_ref.shape
+    pairs = CHIPS // 2
     total = sums_ref[:groups]
     for k in range(1, groups):
         total = total + sums_ref[k * groups : (k + 1) * groups]
-    for h in range(PARTS):
-        mixed_ref[pl.ds(h, CHIPS, stride=PARTS)] = total[h * CHIPS : (h + 1) * CHIPS]
+    first = lax.broadcasted_iota(jnp.int32, (pairs, width), 1) < width // 2
+    for h in range(2):
+        zero = total[2 * h * pairs : (2 * h + 1) * pairs]
+        one = total[(2 * h + 1) * pairs : (2 * h + 2) * pairs]
+        even = jnp.where(first, zero, pltpu.roll(one, width // 2, 1))
+        odd = jnp.where(first, pltpu.roll(zero, width // 2, 1), one)
+        mixed_ref[pl.ds(h, pairs, stride=4)] = even
+        mixed_ref[pl.ds(2 + h, pairs, stride=4)] = odd
     mixed = mixed_ref[...]
     scale = lax.rsqrt(jnp.sum(mixed * mixed) / gain_ref.size + epsilon)
-    stream = x_ref[:, zb].astype(jnp.float32)
+    stream = x_ref[:, own].astype(jnp.float32)
     at = lax.broadcasted_iota(jnp.int32, stream.shape, 1) == place
     row = jnp.sum(jnp.where(at, stream, 0.0), axis=1)
     after = (row + mixed * scale * gain_ref[...]).astype(out_ref.dtype)
@@ -351,14 +361,16 @@
         groups * PARTS,
     )
     long = lax.all_gather(long, TP, axis=0, tiled=True)
-    stream = exchange(spread, (*KV, "zb")).reshape(groups, PARTS, batch_rows, own_cols)
-    short = lax.all_gather(short, ("za", "c"), axis=0).reshape(CHIPS, CORES, *short.shape)
-    part = exchange(project(stream, gain_mix_pre.reshape(groups, own_cols), short), "zb")
+    stream = exchange(spread, (*KV, *NEAR)).reshape(groups, PARTS, batch_rows, own_cols)
+    short = lax.all_gather(short, "zh", axis=0)
+    part = exchange(project(stream, gain_mix_pre.reshape(groups, own_cols), short), NEAR)
     new_state, gated = recur(
         part, prior_state[:, 0], forget_floor[None], group_gain[None]
     )
-    mixed_part = mix_out(exchange(gated, "zb"), short)
-    mixed = exchange(mixed_part.reshape(groups * PARTS, CHIPS, own_cols), (*KV, "zb"))
+    mixed_part = mix_out(lax.all_gather(gated, NEAR, axis=0), short)
+    mixed = exchange(
+        mixed_part.reshape(groups * PARTS, CHIPS // 2, own_cols), (*KV, *NEAR)
+    )
     after_row = row_update(
         mixed.reshape(-1, own_cols), stream, gain_mix_post.reshape(groups, own_cols)
     )
@@ -375,7 +387,7 @@
 
 
 def solution(mesh):
-    grid = Mesh(mesh.devices.reshape(4, 4, CHIPS, PARTS, CORES), (*KV, *TP))
+    grid = Mesh(mesh.devices.reshape(4, 4, CHIPS, 2, 2), (*KV, *TP))
     return jax.shard_map(
         shards,
         mesh=grid,

time: 129 us -> 125 us (0.969)
  blocking collectives: 90.1 us -> 87.6 us
  starting transfers between devices: 12.1 us -> 10 us
    all_to_all x5 -> x4, blocking collectives: 63.8 us -> 43.9 us  [exchange(): return lax.all_to_all(blocks, axes, 0, 0, tiled=True)]
    all_gather x1 -> x2, blocking collectives: 26.4 us -> 43.7 us  [the longest x1 38.5 us: shards(): short = lax.all_gather(short, 'zh', axis=0)]
    all_to_all x1, starting transfers between devices: 12.1 us -> 9.97 us  [exchange(): return lax.all_to_all(blocks, axes, 0, 0, tiled=True)]
  transfers between devices with their start and end apart: 2 -> 2, of which waited for: 0 -> 0; matrix products, arithmetic and copies ran while one was open for 0% -> 0% of each run, Pallas kernels for 4% -> 5%
where the time goes in v6:
time: 125 us; the launch traced here: 124 us
  blocking collectives  87.6 us (70%)
  between operations  14.1 us (11%)
  Pallas kernels  11.7 us (9%)
  starting transfers between devices  10 us (8%)
    all_to_all x4, blocking collectives, exchange(): return lax.all_to_all(blocks, axes, 0, 0, tiled=True)  43.9 us
    all_gather x1, blocking collectives, shards(): short = lax.all_gather(short, 'zh', axis=0)  38.5 us
    all_to_all x1, starting transfers between devices, exchange(): return lax.all_to_all(blocks, axes, 0, 0, tiled=True)  9.97 us
    all_gather x1, blocking collectives, shards(): mixed_part = mix_out(lax.all_gather(gated, NEAR, axis=0), short)  5.21 us
    pallas_call x1, Pallas kernels, mlp(): pl.pallas_call(mlp_body, out_shape=(pltpu.VMEM((groups, rows, width), jnp...  3.54 us
    pallas_call x1, Pallas kernels, recur(): pl.pallas_call(recur_body, out_shape=(jax.ShapeDtypeStruct(prior.shape, j...  3.52 us
  transfers between devices with their start and end apart: 2, of which 0 were waited for; matrix products, arithmetic and copies ran while one was open for 0% of the time, Pallas kernels for 5%

profile of v6, /device:TPU:2, one launch (start us, length us, event | category | flops | bytes accessed | tf_op | source)
XLA Modules:
  0.0 124.0 jit_solution(17419124896698035756)
XLA Ops:
  7.2 0.0 all-gather.4.cloned.1.call-start
  7.2 2.4 %pack.1 = (bf16[64,1024]{1,0:T(8,128)(2,1)}, bf16[80,512]{1,0:T(8,128)(2,1)S(1)}, bf16[64,16,128]{2,1,0:T(8,128)(2,1)}) custom-call(bf16[16,128]{1,0:T(8,128)(2,1)} %residual.1, bf16[64,128]{1,0:T(8,128)(2,1)} %wq.1, bf16[64,128]{1,0:T(8,128)(2,1)} %wf.1, bf16[64,128]{1,0:T(8,128)(2,1)} %wv.1, bf16[64,128]{1,0:T(8,128)(2,1)} %wg.1, ...), custom_call_target="tpu_custom_call" | custom-call | tf_op jit(solution)/shard_map/pack/pallas_call | solution.py:58
  9.6 0.0 all-gather.4.cloned.1.call-update
  9.7 10.0 %all-to-all-start = ((bf16[64,16,128]{2,1,0:T(8,128)(2,1)}), bf16[64,16,128]{2,1,0:T(8,128)(2,1)S(1)}, u32[]{:S(2)}, u32[]{:S(2)}) async-start(bf16[64,16,128]{2,1,0:T(8,128)(2,1)} %get-tuple-element.10), calls=%async_computation | async-start | bytes 524288 | tf_op jit(solution)/shard_map/all_to_all | solution.py:21
  19.6 38.5 %all-gather = bf16[640,512]{1,0:T(8,128)(2,1)S(1)} all-gather(bf16[80,512]{1,0:T(8,128)(2,1)S(1)} %get-tuple-element.11), channel_id=2, replica_groups=mesh['y'=4,'x'=4,'zh'=8,'zo'=2,'c'=2] {'zh'}, dimensions={0}, use_global_device_ids=true | all-gather | bytes 737280 | tf_op jit(solution)/shard_map/all_gather | solution.py:365
  58.1 0.0 all-to-all-done
  58.1 1.1 project.1
  59.2 6.6 %all_to_all.25.part_ref = bf16[4,16,512]{2,1,0:T(8,128)(2,1)S(1)} all-to-all(bf16[4,16,512]{2,1,0:T(8,128)(2,1)S(1)} %project.1), channel_id=1, replica_groups=mesh['y'=4,'x'=4,'zh'=8,'zo'=2,'c'=2] {'zo','c'}, dimensions={0} | all-to-all | bytes 131072 | tf_op jit(solution)/shard_map/all_to_all | solution.py:21
  65.8 3.5 %recur.1 = (f32[16,128,128]{2,1,0:T(8,128)}, bf16[16,128]{1,0:T(8,128)(2,1)S(1)}) custom-call(bf16[4,16,512]{2,1,0:T(8,128)(2,1)S(1)} %all_to_all.25.part_ref, f32[16,128,128]{2,1,0:T(8,128)} %bitcast.26, f32[1,128]{1,0:T(1,128)} %bitcast.33, f32[1,128]{1,0:T(1,128)} %bitcast.34), custom_call_target="tpu_custom_call" | custom-call | tf_op jit(solution)/shard_map/recur/pallas_call | solution.py:167
  69.3 5.2 %all-gather.1 = bf16[64,128]{1,0:T(8,128)(2,1)S(1)} all-gather(bf16[16,128]{1,0:T(8,128)(2,1)S(1)} %get-tuple-element.12), channel_id=3, replica_groups=mesh['y'=4,'x'=4,'zh'=8,'zo'=2,'c'=2] {'zo','c'}, dimensions={0}, use_global_device_ids=true | all-gather | bytes 20480 | tf_op jit(solution)/shard_map/all_gather | solution.py:370
  74.5 0.2 mix_out.1
  74.7 15.8 %all_to_all.26 = f32[64,4,128]{2,1,0:T(4,128)S(1)} all-to-all(f32[64,4,128]{2,1,0:T(4,128)S(1)} %bitcast.22), channel_id=1, replica_groups=mesh['y'=4,'x'=4,'zh'=8,'zo'=2,'c'=2] {'y','x','zo','c'}, dimensions={0} | all-to-all | bytes 262144 | tf_op jit(solution)/shard_map/all_to_all | solution.py:21
  90.5 1.0 row_update.1
  91.4 10.8 %all_to_all.27.row_ref = bf16[16,16,128]{2,1,0:T(8,128)(2,1)S(1)} all-to-all(bf16[16,16,128]{2,1,0:T(8,128)(2,1)S(1)} %row_update.1), channel_id=1, replica_groups=mesh['y'=4,'x'=4,'zh'=8,'zo'=2,'c'=2] {'y','x'}, dimensions={0} | all-to-all | bytes 131072 | tf_op jit(solution)/shard_map/all_to_all | solution.py:21
  102.2 0.0 all-gather.4.cloned.1.call-done.long_ref
  102.2 3.5 %mlp.1 = (bf16[16,16,128]{2,1,0:T(8,128)(2,1)S(1)}, f32[16,128]{1,0:T(8,128)S(1)}, f32[1,128]{1,0:T(1,128)S(1)}) custom-call(bf16[16,16,128]{2,1,0:T(8,128)(2,1)S(1)} %all_to_all.27.row_ref, f32[16,128]{1,0:T(8,128)} %bitcast.31, f32[16,128]{1,0:T(8,128)} %bitcast.32, bf16[2048,1024]{1,0:T(8,128)(2,1)} %all-gather.4.cloned.1.call-done.long_ref), custom_call_target="tpu_custom_call" | custom-call | tf_op jit(solution)/shard_map/mlp/pallas_call | solution.py:313
  105.8 10.8 %all_to_all.28 = bf16[16,16,128]{2,1,0:T(8,128)(2,1)S(1)} all-to-all(bf16[16,16,128]{2,1,0:T(8,128)(2,1)S(1)} %get-tuple-element.15), channel_id=1, replica_groups=mesh['y'=4,'x'=4,'zh'=8,'zo'=2,'c'=2] {'y','x'}, dimensions={0} | all-to-all | bytes 131072 | tf_op jit(solution)/shard_map/all_to_all | solution.py:21
  116.6 0.6 add_convert_fusion
  (1 shorter events, 0.0 us)
Async XLA Ops:
  7.2 95.1 %all-gather.4.cloned.1.call-start = ((), (), s32[]{:S(2)}) async-start(), calls=%async_computation.5 | async-start | bytes 4325376 | tf_op jit(solution)/shard_map/all_gather | solution.py:363
  9.7 48.5 %all-to-all-start = ((bf16[64,16,128]{2,1,0:T(8,128)(2,1)}), bf16[64,16,128]{2,1,0:T(8,128)(2,1)S(1)}, u32[]{:S(2)}, u32[]{:S(2)}) async-start(bf16[64,16,128]{2,1,0:T(8,128)(2,1)} %get-tuple-element.10), calls=%async_computation | async-start | bytes 524288 | tf_op jit(solution)/shard_map/all_to_all | solution.py:21
Sparse Core Ops, SparseCore 0:
  10.1 80.4 all-gather.3

commit v7 on v6

--- a/solution.py
+++ b/solution.py
@@ -69,7 +69,7 @@
     )(residual, wq, wf, wv, wg, mix, up, down)
 
 
-def project_body(x_ref, gain_ref, short_ref, out_ref):
+def project_body(x_ref, gain_ref, short_ref, out_ref, mix_ref):
     zo, core = lax.axis_index("zo"), lax.axis_index("c")
     groups, _, height, width = x_ref.shape
     rows = width // 2
@@ -100,6 +100,10 @@
         w = jnp.concatenate([short_ref[k, :rows]] * 2, axis=0)
         term = jnp.dot(x, w, preferred_element_type=jnp.float32)
         total = term if total is None else total + term
+        for j in range(4):
+            mix_ref[k * rows + j * (rows // 4) : k * rows + (j + 1) * (rows // 4)] = (
+                short_ref[k, rows:, j * width : (j + 1) * width]
+            )
     for h in range(PARTS):
         out_ref[h] = total[h * height : (h + 1) * height].astype(out_ref.dtype)
 
@@ -107,24 +111,68 @@
 def project(x, gain, short):
     return pl.pallas_call(
         project_body,
-        out_shape=pltpu.VMEM((PARTS, x.shape[2], short.shape[2]), jnp.bfloat16),
+        out_shape=(
+            pltpu.VMEM((PARTS, x.shape[2], short.shape[2]), jnp.bfloat16),
+            pltpu.VMEM((CHIPS * x.shape[3] // 2, x.shape[3]), jnp.bfloat16),
+        ),
         name="project",
     )(near(x), gain, near(short))
 
 
-def recur_body(
-    part_ref,
-    prior,
-    floor_ref,
-    gain_ref,
-    state,
-    out_ref,
-    prior_ref,
-    state_ref,
-    read_ref,
-    in_sems,
-    out_sems,
+def gates(pre, floor):
+    width = floor.shape[1]
+    forget = floor + (1.0 - floor) * jax.nn.sigmoid(pre[:, width : 2 * width])
+    return forget, pre[:, 2 * width : 3 * width]
+
+
+def read_body(
+    part_ref, prior, floor_ref, gain_ref, out_ref, pre_ref, prior_ref, read_ref, sems
 ):
+    rows, width, _ = prior_ref.shape
+    chunks = [slice(k, k + SLAB) for k in range(0, rows, SLAB)]
+    fetches = run_copies([(prior.at[c], prior_ref.at[c]) for c in chunks], sems)
+    pre = part_ref[0].astype(jnp.float32)
+    for k in range(1, PARTS):
+        pre = pre + part_ref[k].astype(jnp.float32)
+    pre = pre.astype(jnp.bfloat16).astype(jnp.float32)
+    pre_ref[...] = pre
+    query = jax.nn.silu(pre[:, :width])
+    forget, value = gates(pre, floor_ref[...])
+    gate = jax.nn.sigmoid(pre[:, 3 * width :])
+    kept = (query * forget).T
+    fresh = jnp.sum(query * (1.0 - forget), axis=-1, keepdims=True) * value
+    for b in range(rows):
+        if b % SLAB == 0:
+            fetches[b // SLAB].wait()
+        read_ref[b : b + 1] = jnp.sum(
+            kept[:, b : b + 1] * prior_ref[b], axis=0, keepdims=True
+        )
+    read = read_ref[...] + fresh
+    scale = lax.rsqrt(jnp.mean(read * read, axis=-1, keepdims=True) + epsilon)
+    out_ref[...] = (read * scale * gain_ref[...] * gate).astype(out_ref.dtype)
+
+
+def read_out(part, prior, floor, gain):
+    rows, width, _ = prior.shape
+    vmem = pl.BlockSpec(memory_space=pltpu.VMEM)
+    return pl.pallas_call(
+        read_body,
+        out_shape=(
+            pltpu.VMEM((rows, width), jnp.bfloat16),
+            pltpu.VMEM((rows, part.shape[2]), jnp.float32),
+        ),
+        in_specs=[vmem, pl.BlockSpec(memory_space=pl.ANY), vmem, vmem],
+        out_specs=(vmem, vmem),
+        scratch_shapes=[
+            pltpu.VMEM(prior.shape, jnp.float32),
+            pltpu.VMEM((rows, width), jnp.float32),
+            pltpu.SemaphoreType.DMA((rows // SLAB,)),
+        ],
+        name="read_out",
+    )(near(part), prior, floor, gain)
+
+
+def update_body(pre_ref, prior, floor_ref, state, prior_ref, state_ref, in_sems, out_sems):
     rows = prior_ref.shape[0]
     chunks = [slice(k, k + SLAB) for k in range(0, rows, SLAB)]
     fetches = run_copies([(prior.at[c], prior_ref.at[c]) for c in chunks], in_sems)
@@ -132,104 +180,67 @@
         pltpu.make_async_copy(state_ref.at[c], state.at[c], out_sems.at[k])
         for k, c in enumerate(chunks)
     ]
-    pre = part_ref[0].astype(jnp.float32)
-    for k in range(1, PARTS):
-        pre = pre + part_ref[k].astype(jnp.float32)
-    pre = pre.astype(jnp.bfloat16).astype(jnp.float32)
-    width = prior_ref.shape[1]
-    query = jax.nn.silu(pre[:, :width])
-    floor = floor_ref[...]
-    forget = floor + (1.0 - floor) * jax.nn.sigmoid(pre[:, width : 2 * width])
-    value = pre[:, 2 * width : 3 * width]
-    gate = jax.nn.sigmoid(pre[:, 3 * width :])
-    forget_t = forget.T
-    query_t = query.T
+    forget, value = gates(pre_ref[...], floor_ref[...])
+    forget = forget.T
     for b in range(rows):
         if b % SLAB == 0:
             fetches[b // SLAB].wait()
-        keep = forget_t[:, b : b + 1]
-        fresh = keep * prior_ref[b] + (1.0 - keep) * value[b : b + 1]
-        state_ref[b] = fresh
-        read_ref[b : b + 1] = jnp.sum(query_t[:, b : b + 1] * fresh, axis=0, keepdims=True)
+        keep = forget[:, b : b + 1]
+        state_ref[b] = keep * prior_ref[b] + (1.0 - keep) * value[b : b + 1]
         if b % SLAB == SLAB - 1:
             stores[b // SLAB].start()
-    read = read_ref[...]
-    scale = lax.rsqrt(jnp.mean(read * read, axis=-1, keepdims=True) + epsilon)
-    out_ref[...] = (read * scale * gain_ref[...] * gate).astype(out_ref.dtype)
     for store in stores:
         store.wait()
 
 
-def recur(part, prior, floor, gain):
-    rows, width, _ = prior.shape
+def update(pre, prior, floor):
+    rows = prior.shape[0]
     anywhere = pl.BlockSpec(memory_space=pl.ANY)
     vmem = pl.BlockSpec(memory_space=pltpu.VMEM)
     return pl.pallas_call(
-        recur_body,
-        out_shape=(
-            jax.ShapeDtypeStruct(prior.shape, jnp.float32),
-            pltpu.VMEM((rows, width), jnp.bfloat16),
-        ),
-        in_specs=[vmem, anywhere, vmem, vmem],
-        out_specs=(anywhere, vmem),
+        update_body,
+        out_shape=jax.ShapeDtypeStruct(prior.shape, jnp.float32),
+        in_specs=[vmem, anywhere, vmem],
+        out_specs=anywhere,
         scratch_shapes=[
             pltpu.VMEM(prior.shape, jnp.float32),
             pltpu.VMEM(prior.shape, jnp.float32),
-            pltpu.VMEM((rows, width), jnp.float32),
             pltpu.SemaphoreType.DMA((rows // SLAB,)),
             pltpu.SemaphoreType.DMA((rows // SLAB,)),
         ],
-        name="recur",
-    )(near(part), prior, floor, gain)
-
-
-def mix_body(gated_ref, short_ref, out_ref, order_ref):
-    height, width = gated_ref.shape[1:]
+        name="update",
+    )(near(pre), prior, floor)
+
+
+def mix_body(gated_ref, w_ref, out_ref):
+    height, width = gated_ref.shape
     rows = width // 2
-    for h in range(PARTS):
-        order_ref[pl.ds(h, height, stride=PARTS)] = gated_ref[h].astype(jnp.float32)
-    left = order_ref[...].astype(jnp.bfloat16)
-    for k in range(CHIPS // 2):
-        right = jnp.concatenate(
-            [
-                short_ref[2 * k + half, rows:, j * width : (j + 1) * width]
-                for half in range(2)
-                for j in range(4)
-            ],
-            axis=0,
-        )
-        out_ref[pl.ds(k, PARTS * height, stride=CHIPS // 2)] = lax.dot_general(
-            left, right, (((1,), (1,)), ((), ())), preferred_element_type=jnp.float32
-        )
-
-
-def mix_out(gated, short):
-    height, width = gated.shape[1:]
+    left = gated_ref[...]
+    for k in range(CHIPS):
+        for zo in range(2):
+            right = jnp.concatenate(
+                [w_ref[2 * zo + c, k * rows : (k + 1) * rows] for c in range(2)], axis=0
+            )
+            out_ref[pl.ds(2 * k + zo, height, stride=2 * CHIPS)] = lax.dot_general(
+                left, right, (((1,), (1,)), ((), ())), preferred_element_type=jnp.float32
+            )
+
+
+def mix_out(gated, weights):
+    height, width = gated.shape
     return pl.pallas_call(
         mix_body,
-        out_shape=pltpu.VMEM((CHIPS // 2 * PARTS * height, width), jnp.float32),
-        scratch_shapes=[pltpu.VMEM((PARTS * height, width), jnp.float32)],
+        out_shape=pltpu.VMEM((2 * CHIPS * height, width), jnp.float32),
         name="mix_out",
-    )(near(gated), near(short))
-
-
-def row_body(sums_ref, x_ref, gain_ref, out_ref, mixed_ref):
+    )(near(gated), near(weights))
+
+
+def row_body(sums_ref, x_ref, gain_ref, out_ref):
     own = 2 * lax.axis_index("zo") + lax.axis_index("c")
     place = lax.axis_index("y") * lax.axis_size("x") + lax.axis_index("x")
-    groups, width = gain_ref.shape
-    pairs = CHIPS // 2
-    total = sums_ref[:groups]
-    for k in range(1, groups):
-        total = total + sums_ref[k * groups : (k + 1) * groups]
-    first = lax.broadcasted_iota(jnp.int32, (pairs, width), 1) < width // 2
-    for h in range(2):
-        zero = total[2 * h * pairs : (2 * h + 1) * pairs]
-        one = total[(2 * h + 1) * pairs : (2 * h + 2) * pairs]
-        even = jnp.where(first, zero, pltpu.roll(one, width // 2, 1))
-        odd = jnp.where(first, pltpu.roll(zero, width // 2, 1), one)
-        mixed_ref[pl.ds(h, pairs, stride=4)] = even
-        mixed_ref[pl.ds(2 + h, pairs, stride=4)] = odd
-    mixed = mixed_ref[...]
+    mixed = sums_ref[0]
+    for k in range(1, sums_ref.shape[0]):
+        mixed = mixed + sums_ref[k]
     scale = lax.rsqrt(jnp.sum(mixed * mixed) / gain_ref.size + epsilon)
     stream = x_ref[:, own].astype(jnp.float32)
     at = lax.broadcasted_iota(jnp.int32, stream.shape, 1) == place
@@ -243,7 +254,6 @@
     return pl.pallas_call(
         row_body,
         out_shape=pltpu.VMEM((groups, groups, width), jnp.bfloat16),
-        scratch_shapes=[pltpu.VMEM((groups, width), jnp.float32)],
         name="row_update",
     )(near(sums), near(x), gain)
 
@@ -363,17 +373,14 @@
     long = lax.all_gather(long, TP, axis=0, tiled=True)
     stream = exchange(spread, (*KV, *NEAR)).reshape(groups, PARTS, batch_rows, own_cols)
     short = lax.all_gather(short, "zh", axis=0)
-    part = exchange(project(stream, gain_mix_pre.reshape(groups, own_cols), short), NEAR)
-    new_state, gated = recur(
-        part, prior_state[:, 0], forget_floor[None], group_gain[None]
-    )
-    mixed_part = mix_out(lax.all_gather(gated, NEAR, axis=0), short)
-    mixed = exchange(
-        mixed_part.reshape(groups * PARTS, CHIPS // 2, own_cols), (*KV, *NEAR)
-    )
-    after_row = row_update(
-        mixed.reshape(-1, own_cols), stream, gain_mix_post.reshape(groups, own_cols)
-    )
+    part, mix = project(stream, gain_mix_pre.reshape(groups, own_cols), short)
+    part = exchange(part, NEAR)
+    prior = prior_state[:, 0]
+    gated, pre = read_out(part, prior, forget_floor[None], group_gain[None])
+    new_state = update(pre, prior, forget_floor[None])
+    mix = lax.all_gather(mix, NEAR, axis=0)
+    mixed = exchange(mix_out(gated, mix).reshape(batch_rows, groups, own_cols), KV)
+    after_row = row_update(mixed, stream, gain_mix_post.reshape(groups, own_cols))
     channel_part, after_own, out_gain = mlp(
         exchange(after_row, KV),
         gain_mlp_pre.reshape(groups, own_cols),

time: 125 us -> 125 us (level)
  blocking collectives: 87.6 us -> 73.6 us
  starting transfers between devices: 10 us -> 18 us
  Pallas kernels: 11.7 us -> 15.1 us
  waiting for transfers between devices: 0.02 us -> 3.17 us
    all_to_all x4 -> x2, blocking collectives: 43.9 us -> 24.4 us  [exchange(): return lax.all_to_all(blocks, axes, 0, 0, tiled=True)]
    all_to_all x1 -> x3, starting transfers between devices: 9.97 us -> 18 us  [exchange(): return lax.all_to_all(blocks, axes, 0, 0, tiled=True)]
    all_gather x1, blocking collectives: 5.21 us -> 10.6 us  [shards(): mix = lax.all_gather(mix, NEAR, axis=0)]
    all_to_all x1 -> x3, waiting for transfers between devices: 0.01 us -> 3.16 us  [exchange(): return lax.all_to_all(blocks, axes, 0, 0, tiled=True)]
    pallas_call x3 -> x4, Pallas kernels: 4.77 us -> 7.69 us  [the longest x1 3.21 us: update(): pl.pallas_call(update_body, out_shape=jax.ShapeDtypeStruct(prior.shape, j...]
  transfers between devices with their start and end apart: 2 -> 4, of which waited for: 0 -> 1; matrix products, arithmetic and copies ran while one was open for 0% -> 0% of each run, Pallas kernels for 5% -> 7%
where the time goes in v7:
time: 125 us
  blocking collectives  73.6 us (59%)
  starting transfers between devices  18 us (14%)
  Pallas kernels  15.1 us (12%)
  between operations  14.1 us (11%)
  waiting for transfers between devices  3.17 us (3%)
    all_gather x1, blocking collectives, shards(): short = lax.all_gather(short, 'zh', axis=0)  38.5 us
    all_to_all x2, blocking collectives, exchange(): return lax.all_to_all(blocks, axes, 0, 0, tiled=True)  24.4 us
    all_to_all x3, starting transfers between devices, exchange(): return lax.all_to_all(blocks, axes, 0, 0, tiled=True)  18 us
    all_gather x1, blocking collectives, shards(): mix = lax.all_gather(mix, NEAR, axis=0)  10.6 us
    pallas_call x1, Pallas kernels, mlp(): pl.pallas_call(mlp_body, out_shape=(pltpu.VMEM((groups, rows, width), jnp...  4.16 us
    pallas_call x1, Pallas kernels, update(): pl.pallas_call(update_body, out_shape=jax.ShapeDtypeStruct(prior.shape, j...  3.21 us
    all_to_all x3, waiting for transfers between devices, exchange(): return lax.all_to_all(blocks, axes, 0, 0, tiled=True)  3.16 us
  transfers between devices with their start and end apart: 4, of which 1 were waited for; matrix products, arithmetic and copies ran while one was open for 0% of the time, Pallas kernels for 7%

profile of v7, /device:TPU:2, one launch (start us, length us, event | category | flops | bytes accessed | tf_op | source)
XLA Modules:
  0.0 124.6 jit_solution(3227523522854518663)
XLA Ops:
  7.2 0.0 all-gather.4.cloned.1.call-start
  7.2 2.4 %pack.1 = (bf16[64,1024]{1,0:T(8,128)(2,1)}, bf16[80,512]{1,0:T(8,128)(2,1)S(1)}, bf16[64,16,128]{2,1,0:T(8,128)(2,1)}) custom-call(bf16[16,128]{1,0:T(8,128)(2,1)} %residual.1, bf16[64,128]{1,0:T(8,128)(2,1)} %wq.1, bf16[64,128]{1,0:T(8,128)(2,1)} %wf.1, bf16[64,128]{1,0:T(8,128)(2,1)} %wv.1, bf16[64,128]{1,0:T(8,128)(2,1)} %wg.1, ...), custom_call_target="tpu_custom_call" | custom-call | tf_op jit(solution)/shard_map/pack/pallas_call | solution.py:58
  9.6 0.0 all-gather.4.cloned.1.call-update
  9.7 10.0 %all-to-all-start = ((bf16[64,16,128]{2,1,0:T(8,128)(2,1)}), bf16[64,16,128]{2,1,0:T(8,128)(2,1)S(1)}, u32[]{:S(2)}, u32[]{:S(2)}) async-start(bf16[64,16,128]{2,1,0:T(8,128)(2,1)} %get-tuple-element.12), calls=%async_computation | async-start | bytes 524288 | tf_op jit(solution)/shard_map/all_to_all | solution.py:21
  19.6 38.5 %all-gather = bf16[640,512]{1,0:T(8,128)(2,1)S(1)} all-gather(bf16[80,512]{1,0:T(8,128)(2,1)S(1)} %get-tuple-element.13), channel_id=2, replica_groups=mesh['y'=4,'x'=4,'zh'=8,'zo'=2,'c'=2] {'zh'}, dimensions={0}, use_global_device_ids=true | all-gather | bytes 737280 | tf_op jit(solution)/shard_map/all_gather | solution.py:375
  58.1 0.0 all-to-all-done
  58.1 1.7 %project.1 = (bf16[4,16,512]{2,1,0:T(8,128)(2,1)}, bf16[512,128]{1,0:T(8,128)(2,1)S(1)}) custom-call(bf16[16,4,16,128]{3,2,1,0:T(8,128)(2,1)S(1)} %bitcast.18, f32[16,128]{1,0:T(8,128)} %bitcast.28, bf16[8,80,512]{2,1,0:T(8,128)(2,1)S(1)} %bitcast.17), custom_call_target="tpu_custom_call" | custom-call | tf_op jit(solution)/shard_map/project/pallas_call | solution.py:112
  59.9 3.3 %all-to-all-start.1 = ((bf16[4,16,512]{2,1,0:T(8,128)(2,1)}), bf16[4,16,512]{2,1,0:T(8,128)(2,1)S(1)}, u32[]{:S(2)}, u32[]{:S(2)}) async-start(bf16[4,16,512]{2,1,0:T(8,128)(2,1)} %get-tuple-element.14), calls=%async_computation.1 | async-start | bytes 131072 | tf_op jit(solution)/shard_map/all_to_all | solution.py:21
  63.2 10.6 %all-gather.1 = bf16[2048,128]{1,0:T(8,128)(2,1)S(1)} all-gather(bf16[512,128]{1,0:T(8,128)(2,1)S(1)} %get-tuple-element.16), channel_id=3, replica_groups=mesh['y'=4,'x'=4,'zh'=8,'zo'=2,'c'=2] {'zo','c'}, dimensions={0}, use_global_device_ids=true | all-gather | bytes 655360 | tf_op jit(solution)/shard_map/all_gather | solution.py:381
  73.8 0.0 all-to-all-done.1.part_ref
  73.8 2.4 %read_out.1 = (bf16[16,128]{1,0:T(8,128)(2,1)S(1)}, f32[16,512]{1,0:T(8,128)S(1)}) custom-call(bf16[4,16,512]{2,1,0:T(8,128)(2,1)S(1)} %all-to-all-done.1.part_ref, f32[16,128,128]{2,1,0:T(8,128)} %bitcast.23, f32[1,128]{1,0:T(1,128)} %bitcast.32, f32[1,128]{1,0:T(1,128)} %bitcast.34), custom_call_target="tpu_custom_call" | custom-call | tf_op jit(solution)/shard_map/read_out/pallas_call | solution.py:158
  76.2 0.4 mix_out.1
  76.6 13.7 %all_to_all.25.sums_ref = f32[16,16,128]{2,1,0:T(8,128)S(1)} all-to-all(f32[16,16,128]{2,1,0:T(8,128)S(1)} %bitcast.21), channel_id=1, replica_groups=mesh['y'=4,'x'=4,'zh'=8,'zo'=2,'c'=2] {'y','x'}, dimensions={0} | all-to-all | bytes 262144 | tf_op jit(solution)/shard_map/all_to_all | solution.py:21
  90.2 0.9 row_update.1
  91.1 10.7 %all_to_all.26.row_ref = bf16[16,16,128]{2,1,0:T(8,128)(2,1)S(1)} all-to-all(bf16[16,16,128]{2,1,0:T(8,128)(2,1)S(1)} %row_update.1), channel_id=1, replica_groups=mesh['y'=4,'x'=4,'zh'=8,'zo'=2,'c'=2] {'y','x'}, dimensions={0} | all-to-all | bytes 131072 | tf_op jit(solution)/shard_map/all_to_all | solution.py:21
  101.9 0.0 all-gather.4.cloned.1.call-done.long_ref
  101.9 4.2 %mlp.1 = (bf16[16,16,128]{2,1,0:T(8,128)(2,1)}, f32[16,128]{1,0:T(8,128)S(1)}, f32[1,128]{1,0:T(1,128)S(1)}) custom-call(bf16[16,16,128]{2,1,0:T(8,128)(2,1)S(1)} %all_to_all.26.row_ref, f32[16,128]{1,0:T(8,128)} %bitcast.30, f32[16,128]{1,0:T(8,128)} %bitcast.31, bf16[2048,1024]{1,0:T(8,128)(2,1)} %all-gather.4.cloned.1.call-done.long_ref), custom_call_target="tpu_custom_call" | custom-call | tf_op jit(solution)/shard_map/mlp/pallas_call | solution.py:323
  106.0 4.7 %all-to-all-start.4 = ((bf16[16,16,128]{2,1,0:T(8,128)(2,1)}), bf16[16,16,128]{2,1,0:T(8,128)(2,1)S(1)}, u32[]{:S(2)}, u32[]{:S(2)}) async-start(bf16[16,16,128]{2,1,0:T(8,128)(2,1)} %get-tuple-element.19), calls=%async_computation.4 | async-start | bytes 131072 | tf_op jit(solution)/shard_map/all_to_all | solution.py:21
  110.8 3.2 %update.1 = f32[16,128,128]{2,1,0:T(8,128)} custom-call(f32[16,512]{1,0:T(8,128)S(1)} %get-tuple-element.21.pre_ref, f32[16,128,128]{2,1,0:T(8,128)} %bitcast.24, f32[1,128]{1,0:T(1,128)} %bitcast.33), custom_call_target="tpu_custom_call" | custom-call | tf_op jit(solution)/shard_map/update/pallas_call | solution.py:200
  114.0 3.2 %all-to-all-done.4 = bf16[16,16,128]{2,1,0:T(8,128)(2,1)S(1)} async-done(((bf16[16,16,128]{2,1,0:T(8,128)(2,1)}), bf16[16,16,128]{2,1,0:T(8,128)(2,1)S(1)}, u32[]{:S(2)}, u32[]{:S(2)}) %all-to-all-start.4) | async-done | bytes 65568 | tf_op jit(solution)/shard_map/all_to_all | solution.py:21
  117.2 0.6 add_convert_fusion
  (1 shorter events, 0.0 us)
Async XLA Ops:
  7.2 94.7 %all-gather.4.cloned.1.call-start = ((), (), s32[]{:S(2)}) async-start(), calls=%async_computation.5 | async-start | bytes 4325376 | tf_op jit(solution)/shard_map/all_gather | solution.py:373
  9.7 48.5 %all-to-all-start = ((bf16[64,16,128]{2,1,0:T(8,128)(2,1)}), bf16[64,16,128]{2,1,0:T(8,128)(2,1)S(1)}, u32[]{:S(2)}, u32[]{:S(2)}) async-start(bf16[64,16,128]{2,1,0:T(8,128)(2,1)} %get-tuple-element.12), calls=%async_computation | async-start | bytes 524288 | tf_op jit(solution)/shard_map/all_to_all | solution.py:21
  59.9 13.9 %all-to-all-start.1 = ((bf16[4,16,512]{2,1,0:T(8,128)(2,1)}), bf16[4,16,512]{2,1,0:T(8,128)(2,1)S(1)}, u32[]{:S(2)}, u32[]{:S(2)}) async-start(bf16[4,16,512]{2,1,0:T(8,128)(2,1)} %get-tuple-element.14), calls=%async_computation.1 | async-start | bytes 131072 | tf_op jit(solution)/shard_map/all_to_all | solution.py:21
  106.0 11.1 %all-to-all-start.4 = ((bf16[16,16,128]{2,1,0:T(8,128)(2,1)}), bf16[16,16,128]{2,1,0:T(8,128)(2,1)S(1)}, u32[]{:S(2)}, u32[]{:S(2)}) async-start(bf16[16,16,128]{2,1,0:T(8,128)(2,1)} %get-tuple-element.19), calls=%async_computation.4 | async-start | bytes 131072 | tf_op jit(solution)/shard_map/all_to_all | solution.py:21
Sparse Core Ops, SparseCore 0:
  10.1 80.4 all-gather.3

commit v8 on v7

--- a/solution.py
+++ b/solution.py
@@ -35,7 +35,21 @@
 
 
 def pack_body(
-    residual, wq, wf, wv, wg, mix, up, down, long_ref, short_ref, spread_ref, sems
+    residual,
+    wq,
+    wf,
+    wv,
+    wg,
+    mix,
+    up,
+    down,
+    long,
+    short_ref,
+    spread,
+    long_ref,
+    spread_ref,
+    sems,
+    out_sems,
 ):
     rows, cols = wq.shape
     part = mix.shape[0] // 4
@@ -47,7 +61,15 @@
         copies.append((mix.at[k * part : (k + 1) * part], short_ref.at[rows:, at]))
     started = run_copies(copies, sems)
     spread_ref[...] = jnp.broadcast_to(residual[...][None], spread_ref.shape)
-    for copy in started:
+    outs = [
+        pltpu.make_async_copy(spread_ref, spread, out_sems.at[0]),
+        pltpu.make_async_copy(long_ref, long, out_sems.at[1]),
+    ]
+    outs[0].start()
+    for copy in started[:2]:
+        copy.wait()
+    outs[1].start()
+    for copy in started[2:] + outs:
         copy.wait()
 
 
@@ -55,16 +77,23 @@
     rows, cols = wq.shape
     anywhere = pl.BlockSpec(memory_space=pl.ANY)
     vmem = pl.BlockSpec(memory_space=pltpu.VMEM)
+    long = (rows, up.shape[1] + down.shape[1])
+    spread = (peers, *residual.shape)
     return pl.pallas_call(
         pack_body,
         out_shape=(
-            jax.ShapeDtypeStruct((rows, up.shape[1] + down.shape[1]), up.dtype),
+            jax.ShapeDtypeStruct(long, up.dtype),
             pltpu.VMEM((rows + mix.shape[0] // 4, 4 * cols), wq.dtype),
-            pltpu.VMEM((peers, *residual.shape), residual.dtype),
+            jax.ShapeDtypeStruct(spread, residual.dtype),
         ),
         in_specs=[vmem] + [anywhere] * 7,
-        out_specs=(vmem,) * 3,
-        scratch_shapes=[pltpu.SemaphoreType.DMA((10,))],
+        out_specs=(anywhere, vmem, anywhere),
+        scratch_shapes=[
+            pltpu.VMEM(long, up.dtype),
+            pltpu.VMEM(spread, residual.dtype),
+            pltpu.SemaphoreType.DMA((10,)),
+            pltpu.SemaphoreType.DMA((2,)),
+        ],
         name="pack",
     )(residual, wq, wf, wv, wg, mix, up, down)
 
@@ -212,7 +241,7 @@
     )(near(pre), prior, floor)
 
 
-def mix_body(gated_ref, w_ref, out_ref):
+def mix_body(gated_ref, w_ref, out_ref, sums_ref):
     height, width = gated_ref.shape
     rows = width // 2
     left = gated_ref[...]
@@ -221,16 +250,21 @@
             right = jnp.concatenate(
                 [w_ref[2 * zo + c, k * rows : (k + 1) * rows] for c in range(2)], axis=0
             )
-            out_ref[pl.ds(2 * k + zo, height, stride=2 * CHIPS)] = lax.dot_general(
+            sums_ref[pl.ds(2 * k + zo, height, stride=2 * CHIPS)] = lax.dot_general(
                 left, right, (((1,), (1,)), ((), ())), preferred_element_type=jnp.float32
             )
+    for row in range(height):
+        out_ref[row] = sums_ref[2 * CHIPS * row : 2 * CHIPS * (row + 1)].astype(
+            out_ref.dtype
+        )
 
 
 def mix_out(gated, weights):
     height, width = gated.shape
     return pl.pallas_call(
         mix_body,
-        out_shape=pltpu.VMEM((2 * CHIPS * height, width), jnp.float32),
+        out_shape=pltpu.VMEM((height, 2 * CHIPS, width), jnp.bfloat16),
+        scratch_shapes=[pltpu.VMEM((2 * CHIPS * height, width), jnp.float32)],
         name="mix_out",
     )(near(gated), near(weights))
 
@@ -238,9 +272,9 @@
 def row_body(sums_ref, x_ref, gain_ref, out_ref):
     own = 2 * lax.axis_index("zo") + lax.axis_index("c")
     place = lax.axis_index("y") * lax.axis_size("x") + lax.axis_index("x")
-    mixed = sums_ref[0]
+    mixed = sums_ref[0].astype(jnp.float32)
     for k in range(1, sums_ref.shape[0]):
-        mixed = mixed + sums_ref[k]
+        mixed = mixed + sums_ref[k].astype(jnp.float32)
     scale = lax.rsqrt(jnp.sum(mixed * mixed) / gain_ref.size + epsilon)
     stream = x_ref[:, own].astype(jnp.float32)
     at = lax.broadcasted_iota(jnp.int32, stream.shape, 1) == place
@@ -379,7 +413,7 @@
     gated, pre = read_out(part, prior, forget_floor[None], group_gain[None])
     new_state = update(pre, prior, forget_floor[None])
     mix = lax.all_gather(mix, NEAR, axis=0)
-    mixed = exchange(mix_out(gated, mix).reshape(batch_rows, groups, own_cols), KV)
+    mixed = exchange(mix_out(gated, mix), KV)
     after_row = row_update(mixed, stream, gain_mix_post.reshape(groups, own_cols))
     channel_part, after_own, out_gain = mlp(
         exchange(after_row, KV),

time: 125 us -> 125 us (level)
  no operation moved by 1% of the time
where the time goes in v8:
time: 125 us; the launch traced here: 124 us
  blocking collectives  73.4 us (59%)
  starting transfers between devices  18 us (14%)
  Pallas kernels  15.1 us (12%)
  between operations  14.1 us (11%)
  waiting for transfers between devices  3.17 us (3%)
    all_gather x1, blocking collectives, shards(): short = lax.all_gather(short, 'zh', axis=0)  39 us
    all_to_all x2, blocking collectives, exchange(): return lax.all_to_all(blocks, axes, 0, 0, tiled=True)  24.4 us
    all_to_all x3, starting transfers between devices, exchange(): return lax.all_to_all(blocks, axes, 0, 0, tiled=True)  18 us
    all_gather x1, blocking collectives, shards(): mix = lax.all_gather(mix, NEAR, axis=0)  9.99 us
    pallas_call x1, Pallas kernels, mlp(): pl.pallas_call(mlp_body, out_shape=(pltpu.VMEM((groups, rows, width), jnp...  4.16 us
    pallas_call x1, Pallas kernels, update(): pl.pallas_call(update_body, out_shape=jax.ShapeDtypeStruct(prior.shape, j...  3.21 us
    all_to_all x3, waiting for transfers between devices, exchange(): return lax.all_to_all(blocks, axes, 0, 0, tiled=True)  3.16 us
  transfers between devices with their start and end apart: 4, of which 1 were waited for; matrix products, arithmetic and copies ran while one was open for 0% of the time, Pallas kernels for 7%

profile of v8, /device:TPU:2, one launch (start us, length us, event | category | flops | bytes accessed | tf_op | source)
XLA Modules:
  0.0 124.4 jit_solution(17014652065498913954)
XLA Ops:
  7.2 0.0 all-gather.4.cloned.1.call-start
  7.2 2.3 %pack.1 = (bf16[64,1024]{1,0:T(8,128)(2,1)}, bf16[80,512]{1,0:T(8,128)(2,1)S(1)}, bf16[64,16,128]{2,1,0:T(8,128)(2,1)}) custom-call(bf16[16,128]{1,0:T(8,128)(2,1)} %residual.1, bf16[64,128]{1,0:T(8,128)(2,1)} %wq.1, bf16[64,128]{1,0:T(8,128)(2,1)} %wf.1, bf16[64,128]{1,0:T(8,128)(2,1)} %wv.1, bf16[64,128]{1,0:T(8,128)(2,1)} %wg.1, ...), custom_call_target="tpu_custom_call" | custom-call | tf_op jit(solution)/shard_map/pack/pallas_call | solution.py:82
  9.5 0.0 all-gather.4.cloned.1.call-update
  9.6 10.0 %all-to-all-start = ((bf16[64,16,128]{2,1,0:T(8,128)(2,1)}), bf16[64,16,128]{2,1,0:T(8,128)(2,1)S(1)}, u32[]{:S(2)}, u32[]{:S(2)}) async-start(bf16[64,16,128]{2,1,0:T(8,128)(2,1)} %get-tuple-element.12), calls=%async_computation | async-start | bytes 524288 | tf_op jit(solution)/shard_map/all_to_all | solution.py:21
  19.5 39.0 %all-gather = bf16[640,512]{1,0:T(8,128)(2,1)S(1)} all-gather(bf16[80,512]{1,0:T(8,128)(2,1)S(1)} %get-tuple-element.13), channel_id=2, replica_groups=mesh['y'=4,'x'=4,'zh'=8,'zo'=2,'c'=2] {'zh'}, dimensions={0}, use_global_device_ids=true | all-gather | bytes 737280 | tf_op jit(solution)/shard_map/all_gather | solution.py:409
  58.5 0.0 all-to-all-done
  58.5 1.7 %project.1 = (bf16[4,16,512]{2,1,0:T(8,128)(2,1)}, bf16[512,128]{1,0:T(8,128)(2,1)S(1)}) custom-call(bf16[16,4,16,128]{3,2,1,0:T(8,128)(2,1)S(1)} %bitcast.17, f32[16,128]{1,0:T(8,128)} %bitcast.26, bf16[8,80,512]{2,1,0:T(8,128)(2,1)S(1)} %bitcast.16), custom_call_target="tpu_custom_call" | custom-call | tf_op jit(solution)/shard_map/project/pallas_call | solution.py:141
  60.2 3.3 %all-to-all-start.1 = ((bf16[4,16,512]{2,1,0:T(8,128)(2,1)}), bf16[4,16,512]{2,1,0:T(8,128)(2,1)S(1)}, u32[]{:S(2)}, u32[]{:S(2)}) async-start(bf16[4,16,512]{2,1,0:T(8,128)(2,1)} %get-tuple-element.14), calls=%async_computation.1 | async-start | bytes 131072 | tf_op jit(solution)/shard_map/all_to_all | solution.py:21
  63.5 10.0 %all-gather.1 = bf16[2048,128]{1,0:T(8,128)(2,1)S(1)} all-gather(bf16[512,128]{1,0:T(8,128)(2,1)S(1)} %get-tuple-element.16), channel_id=3, replica_groups=mesh['y'=4,'x'=4,'zh'=8,'zo'=2,'c'=2] {'zo','c'}, dimensions={0}, use_global_device_ids=true | all-gather | bytes 655360 | tf_op jit(solution)/shard_map/all_gather | solution.py:415
  73.5 0.0 all-to-all-done.1.part_ref
  73.5 2.4 %read_out.1 = (bf16[16,128]{1,0:T(8,128)(2,1)S(1)}, f32[16,512]{1,0:T(8,128)S(1)}) custom-call(bf16[4,16,512]{2,1,0:T(8,128)(2,1)S(1)} %all-to-all-done.1.part_ref, f32[16,128,128]{2,1,0:T(8,128)} %bitcast.21, f32[1,128]{1,0:T(1,128)} %bitcast.30, f32[1,128]{1,0:T(1,128)} %bitcast.32), custom_call_target="tpu_custom_call" | custom-call | tf_op jit(solution)/shard_map/read_out/pallas_call | solution.py:187
  75.9 0.4 mix_out.1
  76.3 13.6 %all_to_all.25.sums_ref = bf16[16,16,128]{2,1,0:T(8,128)(2,1)S(1)} all-to-all(bf16[16,16,128]{2,1,0:T(8,128)(2,1)S(1)} %mix_out.1), channel_id=1, replica_groups=mesh['y'=4,'x'=4,'zh'=8,'zo'=2,'c'=2] {'y','x'}, dimensions={0} | all-to-all | bytes 131072 | tf_op jit(solution)/shard_map/all_to_all | solution.py:21
  89.9 0.9 row_update.1
  90.8 10.8 %all_to_all.26.row_ref = bf16[16,16,128]{2,1,0:T(8,128)(2,1)S(1)} all-to-all(bf16[16,16,128]{2,1,0:T(8,128)(2,1)S(1)} %row_update.1), channel_id=1, replica_groups=mesh['y'=4,'x'=4,'zh'=8,'zo'=2,'c'=2] {'y','x'}, dimensions={0} | all-to-all | bytes 131072 | tf_op jit(solution)/shard_map/all_to_all | solution.py:21
  101.6 0.0 all-gather.4.cloned.1.call-done.long_ref
  101.6 4.2 %mlp.1 = (bf16[16,16,128]{2,1,0:T(8,128)(2,1)}, f32[16,128]{1,0:T(8,128)S(1)}, f32[1,128]{1,0:T(1,128)S(1)}) custom-call(bf16[16,16,128]{2,1,0:T(8,128)(2,1)S(1)} %all_to_all.26.row_ref, f32[16,128]{1,0:T(8,128)} %bitcast.27, f32[16,128]{1,0:T(8,128)} %bitcast.28, bf16[2048,1024]{1,0:T(8,128)(2,1)} %all-gather.4.cloned.1.call-done.long_ref), custom_call_target="tpu_custom_call" | custom-call | tf_op jit(solution)/shard_map/mlp/pallas_call | solution.py:357
  105.8 4.7 %all-to-all-start.4 = ((bf16[16,16,128]{2,1,0:T(8,128)(2,1)}), bf16[16,16,128]{2,1,0:T(8,128)(2,1)S(1)}, u32[]{:S(2)}, u32[]{:S(2)}) async-start(bf16[16,16,128]{2,1,0:T(8,128)(2,1)} %get-tuple-element.19), calls=%async_computation.4 | async-start | bytes 131072 | tf_op jit(solution)/shard_map/all_to_all | solution.py:21
  110.5 3.2 %update.1 = f32[16,128,128]{2,1,0:T(8,128)} custom-call(f32[16,512]{1,0:T(8,128)S(1)} %get-tuple-element.21.pre_ref, f32[16,128,128]{2,1,0:T(8,128)} %bitcast.22, f32[1,128]{1,0:T(1,128)} %bitcast.31), custom_call_target="tpu_custom_call" | custom-call | tf_op jit(solution)/shard_map/update/pallas_call | solution.py:229
  113.7 3.2 %all-to-all-done.4 = bf16[16,16,128]{2,1,0:T(8,128)(2,1)S(1)} async-done(((bf16[16,16,128]{2,1,0:T(8,128)(2,1)}), bf16[16,16,128]{2,1,0:T(8,128)(2,1)S(1)}, u32[]{:S(2)}, u32[]{:S(2)}) %all-to-all-start.4) | async-done | bytes 65568 | tf_op jit(solution)/shard_map/all_to_all | solution.py:21
  116.9 0.6 add_convert_fusion
  (1 shorter events, 0.0 us)
Async XLA Ops:
  7.2 94.4 %all-gather.4.cloned.1.call-start = ((), (), s32[]{:S(2)}) async-start(), calls=%async_computation.5 | async-start | bytes 4325376 | tf_op jit(solution)/shard_map/all_gather | solution.py:407
  9.6 48.9 %all-to-all-start = ((bf16[64,16,128]{2,1,0:T(8,128)(2,1)}), bf16[64,16,128]{2,1,0:T(8,128)(2,1)S(1)}, u32[]{:S(2)}, u32[]{:S(2)}) async-start(bf16[64,16,128]{2,1,0:T(8,128)(2,1)} %get-tuple-element.12), calls=%async_computation | async-start | bytes 524288 | tf_op jit(solution)/shard_map/all_to_all | solution.py:21
  60.2 13.3 %all-to-all-start.1 = ((bf16[4,16,512]{2,1,0:T(8,128)(2,1)}), bf16[4,16,512]{2,1,0:T(8,128)(2,1)S(1)}, u32[]{:S(2)}, u32[]{:S(2)}) async-start(bf16[4,16,512]{2,1,0:T(8,128)(2,1)} %get-tuple-element.14), calls=%async_computation.1 | async-start | bytes 131072 | tf_op jit(solution)/shard_map/all_to_all | solution.py:21
  105.8 11.1 %all-to-all-start.4 = ((bf16[16,16,128]{2,1,0:T(8,128)(2,1)}), bf16[16,16,128]{2,1,0:T(8,128)(2,1)S(1)}, u32[]{:S(2)}, u32[]{:S(2)}) async-start(bf16[16,16,128]{2,1,0:T(8,128)(2,1)} %get-tuple-element.19), calls=%async_computation.4 | async-start | bytes 131072 | tf_op jit(solution)/shard_map/all_to_all | solution.py:21
Sparse Core Ops, SparseCore 0:
  10.1 80.9 all-gather.3

commit v9 on v6

--- a/solution.py
+++ b/solution.py
@@ -11,6 +11,7 @@
 NEAR = ("zo", "c")
 PARTS = 4
 CHIPS = 8
+RINGS = [[2 * zh + (zh + g) % 2 for zh in range(CHIPS)] for g in range(2)]
 SLAB = 4
 PIECES = 4
 
@@ -35,7 +36,21 @@
 
 
 def pack_body(
-    residual, wq, wf, wv, wg, mix, up, down, long_ref, short_ref, spread_ref, sems
+    residual,
+    wq,
+    wf,
+    wv,
+    wg,
+    mix,
+    up,
+    down,
+    long,
+    short_ref,
+    spread,
+    long_ref,
+    spread_ref,
+    sems,
+    out_sems,
 ):
     rows, cols = wq.shape
     part = mix.shape[0] // 4
@@ -47,7 +62,15 @@
         copies.append((mix.at[k * part : (k + 1) * part], short_ref.at[rows:, at]))
     started = run_copies(copies, sems)
     spread_ref[...] = jnp.broadcast_to(residual[...][None], spread_ref.shape)
-    for copy in started:
+    outs = [
+        pltpu.make_async_copy(spread_ref, spread, out_sems.at[0]),
+        pltpu.make_async_copy(long_ref, long, out_sems.at[1]),
+    ]
+    outs[0].start()
+    for copy in started[:2]:
+        copy.wait()
+    outs[1].start()
+    for copy in started[2:] + outs:
         copy.wait()
 
 
@@ -55,22 +78,30 @@
     rows, cols = wq.shape
     anywhere = pl.BlockSpec(memory_space=pl.ANY)
     vmem = pl.BlockSpec(memory_space=pltpu.VMEM)
+    long = (rows, up.shape[1] + down.shape[1])
+    spread = (peers, *residual.shape)
     return pl.pallas_call(
         pack_body,
         out_shape=(
-            jax.ShapeDtypeStruct((rows, up.shape[1] + down.shape[1]), up.dtype),
+            jax.ShapeDtypeStruct(long, up.dtype),
             pltpu.VMEM((rows + mix.shape[0] // 4, 4 * cols), wq.dtype),
-            pltpu.VMEM((peers, *residual.shape), residual.dtype),
+            jax.ShapeDtypeStruct(spread, residual.dtype),
         ),
         in_specs=[vmem] + [anywhere] * 7,
-        out_specs=(vmem,) * 3,
-        scratch_shapes=[pltpu.SemaphoreType.DMA((10,))],
+        out_specs=(anywhere, vmem, anywhere),
+        scratch_shapes=[
+            pltpu.VMEM(long, up.dtype),
+            pltpu.VMEM(spread, residual.dtype),
+            pltpu.SemaphoreType.DMA((10,)),
+            pltpu.SemaphoreType.DMA((2,)),
+        ],
         name="pack",
     )(residual, wq, wf, wv, wg, mix, up, down)
 
 
 def project_body(x_ref, gain_ref, short_ref, out_ref):
-    zo, core = lax.axis_index("zo"), lax.axis_index("c")
+    zo = lax.axis_index("zo")
+    ring = lax.axis_index("c") + lax.axis_index("zh")
     groups, _, height, width = x_ref.shape
     rows = width // 2
     squares = [None] * PARTS
@@ -83,10 +114,10 @@
         for s in squares
     ]
     lane = lax.broadcasted_iota(jnp.int32, (1, width), 1)
-    here = (lane >= rows) == (core == 1)
     total = None
     for k in range(CHIPS):
         f = 2 * k + zo
+        here = (lane >= rows) == (lax.rem(ring + k, 2) == 1)
         gain = gain_ref[pl.ds(f, 1)]
         x = jnp.concatenate(
             [
@@ -222,11 +253,14 @@
     for k in range(1, groups):
         total = total + sums_ref[k * groups : (k + 1) * groups]
     first = lax.broadcasted_iota(jnp.int32, (pairs, width), 1) < width // 2
+    turned = lax.rem(lax.axis_index("zh"), 2) == 1
     for h in range(2):
-        zero = total[2 * h * pairs : (2 * h + 1) * pairs]
-        one = total[(2 * h + 1) * pairs : (2 * h + 2) * pairs]
-        even = jnp.where(first, zero, pltpu.roll(one, width // 2, 1))
-        odd = jnp.where(first, pltpu.roll(zero, width // 2, 1), one)
+        left = total[2 * h * pairs : (2 * h + 1) * pairs]
+        right = total[(2 * h + 1) * pairs : (2 * h + 2) * pairs]
+        zero = jnp.where(turned, right, left)
+        one = pltpu.roll(jnp.where(turned, left, right), width // 2, 1)
+        even = jnp.where(first, zero, one)
+        odd = jnp.where(first, one, zero)
         mixed_ref[pl.ds(h, pairs, stride=4)] = even
         mixed_ref[pl.ds(2 + h, pairs, stride=4)] = odd
     mixed = mixed_ref[...]
@@ -362,7 +396,7 @@
     )
     long = lax.all_gather(long, TP, axis=0, tiled=True)
     stream = exchange(spread, (*KV, *NEAR)).reshape(groups, PARTS, batch_rows, own_cols)
-    short = lax.all_gather(short, "zh", axis=0)
+    short = lax.all_gather(short, ("zh", "c"), axis=0, axis_index_groups=RINGS)
     part = exchange(project(stream, gain_mix_pre.reshape(groups, own_cols), short), NEAR)
     new_state, gated = recur(
         part, prior_state[:, 0], forget_floor[None], group_gain[None]

time: 125 us -> 123 us (0.984)
  blocking collectives: 87.6 us -> 86 us
    all_gather x1, blocking collectives: 38.5 us -> 35.6 us  [shards(): short = lax.all_gather(short, ('zh', 'c'), axis=0, axis_index_groups=RINGS)]
    all_to_all x4, blocking collectives: 43.9 us -> 45.3 us  [exchange(): return lax.all_to_all(blocks, axes, 0, 0, tiled=True)]
where the time goes in v9:
time: 123 us; the launch traced here: 122 us
  blocking collectives  86 us (70%)
  between operations  14.1 us (11%)
  Pallas kernels  11.6 us (9%)
  starting transfers between devices  10 us (8%)
    all_to_all x4, blocking collectives, exchange(): return lax.all_to_all(blocks, axes, 0, 0, tiled=True)  45.3 us
    all_gather x1, blocking collectives, shards(): short = lax.all_gather(short, ('zh', 'c'), axis=0, axis_index_groups=RINGS)  35.6 us
    all_to_all x1, starting transfers between devices, exchange(): return lax.all_to_all(blocks, axes, 0, 0, tiled=True)  9.97 us
    all_gather x1, blocking collectives, shards(): mixed_part = mix_out(lax.all_gather(gated, NEAR, axis=0), short)  5.21 us
    pallas_call x1, Pallas kernels, mlp(): pl.pallas_call(mlp_body, out_shape=(pltpu.VMEM((groups, rows, width), jnp...  3.54 us
    pallas_call x1, Pallas kernels, recur(): pl.pallas_call(recur_body, out_shape=(jax.ShapeDtypeStruct(prior.shape, j...  3.53 us
  transfers between devices with their start and end apart: 2, of which 0 were waited for; matrix products, arithmetic and copies ran while one was open for 0% of the time, Pallas kernels for 5%

profile of v9, /device:TPU:2, one launch (start us, length us, event | category | flops | bytes accessed | tf_op | source)
XLA Modules:
  0.0 122.4 jit_solution(5796399151526952567)
XLA Ops:
  7.2 0.0 all-gather.4.cloned.1.call-start
  7.2 2.3 %pack.1 = (bf16[64,1024]{1,0:T(8,128)(2,1)}, bf16[80,512]{1,0:T(8,128)(2,1)S(1)}, bf16[64,16,128]{2,1,0:T(8,128)(2,1)}) custom-call(bf16[16,128]{1,0:T(8,128)(2,1)} %residual.1, bf16[64,128]{1,0:T(8,128)(2,1)} %wq.1, bf16[64,128]{1,0:T(8,128)(2,1)} %wf.1, bf16[64,128]{1,0:T(8,128)(2,1)} %wv.1, bf16[64,128]{1,0:T(8,128)(2,1)} %wg.1, ...), custom_call_target="tpu_custom_call" | custom-call | tf_op jit(solution)/shard_map/pack/pallas_call | solution.py:83
  9.5 0.0 all-gather.4.cloned.1.call-update
  9.6 10.0 %all-to-all-start = ((bf16[64,16,128]{2,1,0:T(8,128)(2,1)}), bf16[64,16,128]{2,1,0:T(8,128)(2,1)S(1)}, u32[]{:S(2)}, u32[]{:S(2)}) async-start(bf16[64,16,128]{2,1,0:T(8,128)(2,1)} %get-tuple-element.10), calls=%async_computation | async-start | bytes 524288 | tf_op jit(solution)/shard_map/all_to_all | solution.py:22
  19.5 35.6 %all-gather = bf16[640,512]{1,0:T(8,128)(2,1)S(1)} all-gather(bf16[80,512]{1,0:T(8,128)(2,1)S(1)} %get-tuple-element.11), channel_id=2, replica_groups={{0,5,8,13,16,21,24,29},{1,4,9,12,17,20,25,28},{2,7,10,15,18,23,26,31},{..., dimensions={0}, use_global_device_ids=true | all-gather | bytes 737280 | tf_op jit(solution)/shard_map/all_gather | solution.py:399
  55.1 0.0 all-to-all-done
  55.1 1.1 project.1
  56.2 7.7 %all_to_all.25.part_ref = bf16[4,16,512]{2,1,0:T(8,128)(2,1)S(1)} all-to-all(bf16[4,16,512]{2,1,0:T(8,128)(2,1)S(1)} %project.1), channel_id=1, replica_groups=mesh['y'=4,'x'=4,'zh'=8,'zo'=2,'c'=2] {'zo','c'}, dimensions={0} | all-to-all | bytes 131072 | tf_op jit(solution)/shard_map/all_to_all | solution.py:22
  64.0 3.5 %recur.1 = (f32[16,128,128]{2,1,0:T(8,128)}, bf16[16,128]{1,0:T(8,128)(2,1)S(1)}) custom-call(bf16[4,16,512]{2,1,0:T(8,128)(2,1)S(1)} %all_to_all.25.part_ref, f32[16,128,128]{2,1,0:T(8,128)} %bitcast.26, f32[1,128]{1,0:T(1,128)} %bitcast.33, f32[1,128]{1,0:T(1,128)} %bitcast.34), custom_call_target="tpu_custom_call" | custom-call | tf_op jit(solution)/shard_map/recur/pallas_call | solution.py:198
  67.5 5.2 %all-gather.1 = bf16[64,128]{1,0:T(8,128)(2,1)S(1)} all-gather(bf16[16,128]{1,0:T(8,128)(2,1)S(1)} %get-tuple-element.12), channel_id=3, replica_groups=mesh['y'=4,'x'=4,'zh'=8,'zo'=2,'c'=2] {'zo','c'}, dimensions={0}, use_global_device_ids=true | all-gather | bytes 20480 | tf_op jit(solution)/shard_map/all_gather | solution.py:404
  72.7 0.2 mix_out.1
  72.9 16.1 %all_to_all.26 = f32[64,4,128]{2,1,0:T(4,128)S(1)} all-to-all(f32[64,4,128]{2,1,0:T(4,128)S(1)} %bitcast.22), channel_id=1, replica_groups=mesh['y'=4,'x'=4,'zh'=8,'zo'=2,'c'=2] {'y','x','zo','c'}, dimensions={0} | all-to-all | bytes 262144 | tf_op jit(solution)/shard_map/all_to_all | solution.py:22
  88.9 1.0 row_update.1
  89.9 10.7 %all_to_all.27.row_ref = bf16[16,16,128]{2,1,0:T(8,128)(2,1)S(1)} all-to-all(bf16[16,16,128]{2,1,0:T(8,128)(2,1)S(1)} %row_update.1), channel_id=1, replica_groups=mesh['y'=4,'x'=4,'zh'=8,'zo'=2,'c'=2] {'y','x'}, dimensions={0} | all-to-all | bytes 131072 | tf_op jit(solution)/shard_map/all_to_all | solution.py:22
  100.6 0.0 all-gather.4.cloned.1.call-done.long_ref
  100.6 3.5 %mlp.1 = (bf16[16,16,128]{2,1,0:T(8,128)(2,1)S(1)}, f32[16,128]{1,0:T(8,128)S(1)}, f32[1,128]{1,0:T(1,128)S(1)}) custom-call(bf16[16,16,128]{2,1,0:T(8,128)(2,1)S(1)} %all_to_all.27.row_ref, f32[16,128]{1,0:T(8,128)} %bitcast.31, f32[16,128]{1,0:T(8,128)} %bitcast.32, bf16[2048,1024]{1,0:T(8,128)(2,1)} %all-gather.4.cloned.1.call-done.long_ref), custom_call_target="tpu_custom_call" | custom-call | tf_op jit(solution)/shard_map/mlp/pallas_call | solution.py:347
  104.1 10.8 %all_to_all.28 = bf16[16,16,128]{2,1,0:T(8,128)(2,1)S(1)} all-to-all(bf16[16,16,128]{2,1,0:T(8,128)(2,1)S(1)} %get-tuple-element.15), channel_id=1, replica_groups=mesh['y'=4,'x'=4,'zh'=8,'zo'=2,'c'=2] {'y','x'}, dimensions={0} | all-to-all | bytes 131072 | tf_op jit(solution)/shard_map/all_to_all | solution.py:22
  114.9 0.6 add_convert_fusion
  (1 shorter events, 0.0 us)
Async XLA Ops:
  7.2 93.4 %all-gather.4.cloned.1.call-start = ((), (), s32[]{:S(2)}) async-start(), calls=%async_computation.5 | async-start | bytes 4325376 | tf_op jit(solution)/shard_map/all_gather | solution.py:397
  9.6 45.6 %all-to-all-start = ((bf16[64,16,128]{2,1,0:T(8,128)(2,1)}), bf16[64,16,128]{2,1,0:T(8,128)(2,1)S(1)}, u32[]{:S(2)}, u32[]{:S(2)}) async-start(bf16[64,16,128]{2,1,0:T(8,128)(2,1)} %get-tuple-element.10), calls=%async_computation | async-start | bytes 524288 | tf_op jit(solution)/shard_map/all_to_all | solution.py:22
Sparse Core Ops, SparseCore 0:
  10.1 80.5 all-gather.3

commit v10 on v8

--- a/solution.py
+++ b/solution.py
@@ -11,6 +11,7 @@
 NEAR = ("zo", "c")
 PARTS = 4
 CHIPS = 8
+RINGS = [[2 * zh + (zh + g) % 2 for zh in range(CHIPS)] for g in range(2)]
 SLAB = 4
 PIECES = 4
 
@@ -99,7 +100,8 @@
 
 
 def project_body(x_ref, gain_ref, short_ref, out_ref, mix_ref):
-    zo, core = lax.axis_index("zo"), lax.axis_index("c")
+    zo = lax.axis_index("zo")
+    ring = lax.axis_index("c") + lax.axis_index("zh")
     groups, _, height, width = x_ref.shape
     rows = width // 2
     squares = [None] * PARTS
@@ -112,10 +114,10 @@
         for s in squares
     ]
     lane = lax.broadcasted_iota(jnp.int32, (1, width), 1)
-    here = (lane >= rows) == (core == 1)
     total = None
     for k in range(CHIPS):
         f = 2 * k + zo
+        here = (lane >= rows) == (lax.rem(ring + k, 2) == 1)
         gain = gain_ref[pl.ds(f, 1)]
         x = jnp.concatenate(
             [
@@ -242,13 +244,18 @@
 
 
 def mix_body(gated_ref, w_ref, out_ref, sums_ref):
+    zh = lax.axis_index("zh")
     height, width = gated_ref.shape
     rows = width // 2
     left = gated_ref[...]
     for k in range(CHIPS):
         for zo in range(2):
             right = jnp.concatenate(
-                [w_ref[2 * zo + c, k * rows : (k + 1) * rows] for c in range(2)], axis=0
+                [
+                    w_ref[2 * zo + lax.rem(c + zh + k, 2), k * rows : (k + 1) * rows]
+                    for c in range(2)
+                ],
+                axis=0,
             )
             sums_ref[pl.ds(2 * k + zo, height, stride=2 * CHIPS)] = lax.dot_general(
                 left, right, (((1,), (1,)), ((), ())), preferred_element_type=jnp.float32
@@ -406,7 +413,7 @@
     )
     long = lax.all_gather(long, TP, axis=0, tiled=True)
     stream = exchange(spread, (*KV, *NEAR)).reshape(groups, PARTS, batch_rows, own_cols)
-    short = lax.all_gather(short, "zh", axis=0)
+    short = lax.all_gather(short, ("zh", "c"), axis=0, axis_index_groups=RINGS)
     part, mix = project(stream, gain_mix_pre.reshape(groups, own_cols), short)
     part = exchange(part, NEAR)
     prior = prior_state[:, 0]

time: 125 us -> 122 us (0.976)
  blocking collectives: 73.4 us -> 70.2 us
    all_gather x1, blocking collectives: 39 us -> 35.6 us  [shards(): short = lax.all_gather(short, ('zh', 'c'), axis=0, axis_index_groups=RINGS)]
where the time goes in v10:
time: 122 us
  blocking collectives  70.2 us (58%)
  starting transfers between devices  18.5 us (15%)
  Pallas kernels  15.1 us (12%)
  between operations  14.1 us (12%)
  waiting for transfers between devices  3.17 us (3%)
    all_gather x1, blocking collectives, shards(): short = lax.all_gather(short, ('zh', 'c'), axis=0, axis_index_groups=RINGS)  35.6 us
    all_to_all x2, blocking collectives, exchange(): return lax.all_to_all(blocks, axes, 0, 0, tiled=True)  24.4 us
    all_to_all x3, starting transfers between devices, exchange(): return lax.all_to_all(blocks, axes, 0, 0, tiled=True)  18.5 us
    all_gather x1, blocking collectives, shards(): mix = lax.all_gather(mix, NEAR, axis=0)  10.2 us
    pallas_call x1, Pallas kernels, mlp(): pl.pallas_call(mlp_body, out_shape=(pltpu.VMEM((groups, rows, width), jnp...  4.16 us
    pallas_call x1, Pallas kernels, update(): pl.pallas_call(update_body, out_shape=jax.ShapeDtypeStruct(prior.shape, j...  3.21 us
    all_to_all x3, waiting for transfers between devices, exchange(): return lax.all_to_all(blocks, axes, 0, 0, tiled=True)  3.16 us
  transfers between devices with their start and end apart: 4, of which 1 were waited for; matrix products, arithmetic and copies ran while one was open for 0% of the time, Pallas kernels for 7%

profile of v10, /device:TPU:2, one launch (start us, length us, event | category | flops | bytes accessed | tf_op | source)
XLA Modules:
  0.0 121.7 jit_solution(9468319639361376111)
XLA Ops:
  7.2 0.0 all-gather.4.cloned.1.call-start
  7.2 2.3 %pack.1 = (bf16[64,1024]{1,0:T(8,128)(2,1)}, bf16[80,512]{1,0:T(8,128)(2,1)S(1)}, bf16[64,16,128]{2,1,0:T(8,128)(2,1)}) custom-call(bf16[16,128]{1,0:T(8,128)(2,1)} %residual.1, bf16[64,128]{1,0:T(8,128)(2,1)} %wq.1, bf16[64,128]{1,0:T(8,128)(2,1)} %wf.1, bf16[64,128]{1,0:T(8,128)(2,1)} %wv.1, bf16[64,128]{1,0:T(8,128)(2,1)} %wg.1, ...), custom_call_target="tpu_custom_call" | custom-call | tf_op jit(solution)/shard_map/pack/pallas_call | solution.py:83
  9.5 0.0 all-gather.4.cloned.1.call-update
  9.6 10.0 %all-to-all-start = ((bf16[64,16,128]{2,1,0:T(8,128)(2,1)}), bf16[64,16,128]{2,1,0:T(8,128)(2,1)S(1)}, u32[]{:S(2)}, u32[]{:S(2)}) async-start(bf16[64,16,128]{2,1,0:T(8,128)(2,1)} %get-tuple-element.12), calls=%async_computation | async-start | bytes 524288 | tf_op jit(solution)/shard_map/all_to_all | solution.py:22
  19.5 35.6 %all-gather = bf16[640,512]{1,0:T(8,128)(2,1)S(1)} all-gather(bf16[80,512]{1,0:T(8,128)(2,1)S(1)} %get-tuple-element.13), channel_id=2, replica_groups={{0,5,8,13,16,21,24,29},{1,4,9,12,17,20,25,28},{2,7,10,15,18,23,26,31},{..., dimensions={0}, use_global_device_ids=true | all-gather | bytes 737280 | tf_op jit(solution)/shard_map/all_gather | solution.py:416
  55.1 0.0 all-to-all-done
  55.1 1.7 %project.1 = (bf16[4,16,512]{2,1,0:T(8,128)(2,1)}, bf16[512,128]{1,0:T(8,128)(2,1)S(1)}) custom-call(bf16[16,4,16,128]{3,2,1,0:T(8,128)(2,1)S(1)} %bitcast.17, f32[16,128]{1,0:T(8,128)} %bitcast.26, bf16[8,80,512]{2,1,0:T(8,128)(2,1)S(1)} %bitcast.16), custom_call_target="tpu_custom_call" | custom-call | tf_op jit(solution)/shard_map/project/pallas_call | solution.py:143
  56.8 3.7 %all-to-all-start.1 = ((bf16[4,16,512]{2,1,0:T(8,128)(2,1)}), bf16[4,16,512]{2,1,0:T(8,128)(2,1)S(1)}, u32[]{:S(2)}, u32[]{:S(2)}) async-start(bf16[4,16,512]{2,1,0:T(8,128)(2,1)} %get-tuple-element.14), calls=%async_computation.1 | async-start | bytes 131072 | tf_op jit(solution)/shard_map/all_to_all | solution.py:22
  60.6 10.2 %all-gather.1 = bf16[2048,128]{1,0:T(8,128)(2,1)S(1)} all-gather(bf16[512,128]{1,0:T(8,128)(2,1)S(1)} %get-tuple-element.16), channel_id=3, replica_groups=mesh['y'=4,'x'=4,'zh'=8,'zo'=2,'c'=2] {'zo','c'}, dimensions={0}, use_global_device_ids=true | all-gather | bytes 655360 | tf_op jit(solution)/shard_map/all_gather | solution.py:422
  70.8 0.0 all-to-all-done.1.part_ref
  70.8 2.4 %read_out.1 = (bf16[16,128]{1,0:T(8,128)(2,1)S(1)}, f32[16,512]{1,0:T(8,128)S(1)}) custom-call(bf16[4,16,512]{2,1,0:T(8,128)(2,1)S(1)} %all-to-all-done.1.part_ref, f32[16,128,128]{2,1,0:T(8,128)} %bitcast.21, f32[1,128]{1,0:T(1,128)} %bitcast.30, f32[1,128]{1,0:T(1,128)} %bitcast.32), custom_call_target="tpu_custom_call" | custom-call | tf_op jit(solution)/shard_map/read_out/pallas_call | solution.py:189
  73.2 0.4 mix_out.1
  73.6 13.6 %all_to_all.25.sums_ref = bf16[16,16,128]{2,1,0:T(8,128)(2,1)S(1)} all-to-all(bf16[16,16,128]{2,1,0:T(8,128)(2,1)S(1)} %mix_out.1), channel_id=1, replica_groups=mesh['y'=4,'x'=4,'zh'=8,'zo'=2,'c'=2] {'y','x'}, dimensions={0} | all-to-all | bytes 131072 | tf_op jit(solution)/shard_map/all_to_all | solution.py:22
  87.2 0.9 row_update.1
  88.1 10.8 %all_to_all.26.row_ref = bf16[16,16,128]{2,1,0:T(8,128)(2,1)S(1)} all-to-all(bf16[16,16,128]{2,1,0:T(8,128)(2,1)S(1)} %row_update.1), channel_id=1, replica_groups=mesh['y'=4,'x'=4,'zh'=8,'zo'=2,'c'=2] {'y','x'}, dimensions={0} | all-to-all | bytes 131072 | tf_op jit(solution)/shard_map/all_to_all | solution.py:22
  98.9 0.0 all-gather.4.cloned.1.call-done.long_ref
  98.9 4.2 %mlp.1 = (bf16[16,16,128]{2,1,0:T(8,128)(2,1)}, f32[16,128]{1,0:T(8,128)S(1)}, f32[1,128]{1,0:T(1,128)S(1)}) custom-call(bf16[16,16,128]{2,1,0:T(8,128)(2,1)S(1)} %all_to_all.26.row_ref, f32[16,128]{1,0:T(8,128)} %bitcast.27, f32[16,128]{1,0:T(8,128)} %bitcast.28, bf16[2048,1024]{1,0:T(8,128)(2,1)} %all-gather.4.cloned.1.call-done.long_ref), custom_call_target="tpu_custom_call" | custom-call | tf_op jit(solution)/shard_map/mlp/pallas_call | solution.py:364
  103.1 4.7 %all-to-all-start.4 = ((bf16[16,16,128]{2,1,0:T(8,128)(2,1)}), bf16[16,16,128]{2,1,0:T(8,128)(2,1)S(1)}, u32[]{:S(2)}, u32[]{:S(2)}) async-start(bf16[16,16,128]{2,1,0:T(8,128)(2,1)} %get-tuple-element.19), calls=%async_computation.4 | async-start | bytes 131072 | tf_op jit(solution)/shard_map/all_to_all | solution.py:22
  107.8 3.2 %update.1 = f32[16,128,128]{2,1,0:T(8,128)} custom-call(f32[16,512]{1,0:T(8,128)S(1)} %get-tuple-element.21.pre_ref, f32[16,128,128]{2,1,0:T(8,128)} %bitcast.22, f32[1,128]{1,0:T(1,128)} %bitcast.31), custom_call_target="tpu_custom_call" | custom-call | tf_op jit(solution)/shard_map/update/pallas_call | solution.py:231
  111.1 3.2 %all-to-all-done.4 = bf16[16,16,128]{2,1,0:T(8,128)(2,1)S(1)} async-done(((bf16[16,16,128]{2,1,0:T(8,128)(2,1)}), bf16[16,16,128]{2,1,0:T(8,128)(2,1)S(1)}, u32[]{:S(2)}, u32[]{:S(2)}) %all-to-all-start.4) | async-done | bytes 65568 | tf_op jit(solution)/shard_map/all_to_all | solution.py:22
  114.2 0.6 add_convert_fusion
  (1 shorter events, 0.0 us)
Async XLA Ops:
  7.2 91.8 %all-gather.4.cloned.1.call-start = ((), (), s32[]{:S(2)}) async-start(), calls=%async_computation.5 | async-start | bytes 4325376 | tf_op jit(solution)/shard_map/all_gather | solution.py:414
  9.6 45.5 %all-to-all-start = ((bf16[64,16,128]{2,1,0:T(8,128)(2,1)}), bf16[64,16,128]{2,1,0:T(8,128)(2,1)S(1)}, u32[]{:S(2)}, u32[]{:S(2)}) async-start(bf16[64,16,128]{2,1,0:T(8,128)(2,1)} %get-tuple-element.12), calls=%async_computation | async-start | bytes 524288 | tf_op jit(solution)/shard_map/all_to_all | solution.py:22
  56.8 13.9 %all-to-all-start.1 = ((bf16[4,16,512]{2,1,0:T(8,128)(2,1)}), bf16[4,16,512]{2,1,0:T(8,128)(2,1)S(1)}, u32[]{:S(2)}, u32[]{:S(2)}) async-start(bf16[4,16,512]{2,1,0:T(8,128)(2,1)} %get-tuple-element.14), calls=%async_computation.1 | async-start | bytes 131072 | tf_op jit(solution)/shard_map/all_to_all | solution.py:22
  103.1 11.1 %all-to-all-start.4 = ((bf16[16,16,128]{2,1,0:T(8,128)(2,1)}), bf16[16,16,128]{2,1,0:T(8,128)(2,1)S(1)}, u32[]{:S(2)}, u32[]{:S(2)}) async-start(bf16[16,16,128]{2,1,0:T(8,128)(2,1)} %get-tuple-element.19), calls=%async_computation.4 | async-start | bytes 131072 | tf_op jit(solution)/shard_map/all_to_all | solution.py:22
Sparse Core Ops, SparseCore 0:
  10.1 80.9 all-gather.3

commit v11 on v10

--- a/solution.py
+++ b/solution.py
@@ -304,13 +304,16 @@
     pre_ref,
     post_ref,
     long_ref,
-    out_ref,
+    out,
     own_ref,
     gain_ref,
     after_ref,
     up_ref,
     down_ref,
-    sems,
+    out_ref,
+    up_sems,
+    down_sems,
+    out_sems,
 ):
     place = lax.axis_index("y") * lax.axis_size("x") + lax.axis_index("x")
     groups, width = pre_ref.shape
@@ -318,11 +321,7 @@
     units = up_ref.shape[1]
     full = groups * width
     pieces = [slice(k, k + full // PIECES) for k in range(0, full, full // PIECES)]
-    copies = run_copies(
-        [(long_ref.at[p, :units], up_ref.at[p]) for p in pieces]
-        + [(long_ref.at[p, units:], down_ref.at[p]) for p in pieces],
-        sems,
-    )
+    ups = run_copies([(long_ref.at[p, :units], up_ref.at[p]) for p in pieces], up_sems)
     for row in range(height):
         after_ref[row * groups : (row + 1) * groups] = row_ref[row].astype(jnp.float32)
     after = [after_ref[pl.ds(f, height, stride=groups)] for f in range(groups)]
@@ -343,19 +342,35 @@
     gain_ref[...] = post_ref[pl.ds(place, 1)]
     up = None
     for k, p in enumerate(pieces):
-        copies[k].wait()
+        ups[k].wait()
+        if k == 0:
+            downs = run_copies(
+                [(long_ref.at[q, units:], down_ref.at[q]) for q in pieces], down_sems
+            )
         term = jnp.dot(hidden[:, p], up_ref[p], preferred_element_type=jnp.float32)
         up = term if up is None else up + term
     squared = jnp.square(jnp.maximum(up, 0.0)).astype(jnp.bfloat16)
+    some = groups // PIECES
+    outs = [
+        pltpu.make_async_copy(
+            out_ref.at[k * some : (k + 1) * some],
+            out.at[k * some : (k + 1) * some],
+            out_sems.at[k],
+        )
+        for k in range(PIECES)
+    ]
     for k, p in enumerate(pieces):
-        copies[PIECES + k].wait()
+        downs[k].wait()
         channel = lax.dot_general(
             squared, down_ref[p], (((1,), (1,)), ((), ())), preferred_element_type=jnp.float32
         )
-        for f in range(groups // PIECES):
-            out_ref[k * (groups // PIECES) + f] = channel[
-                :, f * width : (f + 1) * width
-            ].astype(out_ref.dtype)
+        for f in range(some):
+            out_ref[k * some + f] = channel[:, f * width : (f + 1) * width].astype(
+                out_ref.dtype
+            )
+        outs[k].start()
+    for copy in outs:
+        copy.wait()
 
 
 def mlp(after, pre, post, weights, hidden):
@@ -364,16 +379,20 @@
     return pl.pallas_call(
         mlp_body,
         out_shape=(
-            pltpu.VMEM((groups, rows, width), jnp.bfloat16),
+            jax.ShapeDtypeStruct((groups, rows, width), jnp.bfloat16),
             pltpu.VMEM((rows, width), jnp.float32),
             pltpu.VMEM((1, width), jnp.float32),
         ),
+        out_specs=(pl.BlockSpec(memory_space=pl.ANY), vmem, vmem),
         in_specs=[vmem] * 3 + [pl.BlockSpec(memory_space=pl.ANY)],
         scratch_shapes=[
             pltpu.VMEM((rows * groups, width), jnp.float32),
             pltpu.VMEM((weights.shape[0], hidden), jnp.bfloat16),
             pltpu.VMEM((weights.shape[0], hidden), jnp.bfloat16),
-            pltpu.SemaphoreType.DMA((2 * PIECES,)),
+            pltpu.VMEM((groups, rows, width), jnp.bfloat16),
+            pltpu.SemaphoreType.DMA((PIECES,)),
+            pltpu.SemaphoreType.DMA((PIECES,)),
+            pltpu.SemaphoreType.DMA((PIECES,)),
         ],
         name="mlp",
     )(near(after), pre, post, weights)

time: 122 us -> 123 us (level)
  no operation moved by 1% of the time
where the time goes in v11:
time: 123 us; the launch traced here: 122 us
  blocking collectives  70.2 us (57%)
  starting transfers between devices  18.5 us (15%)
  Pallas kernels  15.6 us (13%)
  between operations  14.1 us (11%)
  waiting for transfers between devices  3.17 us (3%)
    all_gather x1, blocking collectives, shards(): short = lax.all_gather(short, ('zh', 'c'), axis=0, axis_index_groups=RINGS)  35.6 us
    all_to_all x2, blocking collectives, exchange(): return lax.all_to_all(blocks, axes, 0, 0, tiled=True)  24.4 us
    all_to_all x3, starting transfers between devices, exchange(): return lax.all_to_all(blocks, axes, 0, 0, tiled=True)  18.5 us
    all_gather x1, blocking collectives, shards(): mix = lax.all_gather(mix, NEAR, axis=0)  10.2 us
    pallas_call x1, Pallas kernels, mlp(): pl.pallas_call(mlp_body, out_shape=(jax.ShapeDtypeStruct((groups, rows, w...  4.68 us
    pallas_call x1, Pallas kernels, update(): pl.pallas_call(update_body, out_shape=jax.ShapeDtypeStruct(prior.shape, j...  3.21 us
    all_to_all x3, waiting for transfers between devices, exchange(): return lax.all_to_all(blocks, axes, 0, 0, tiled=True)  3.16 us
  transfers between devices with their start and end apart: 4, of which 1 were waited for; matrix products, arithmetic and copies ran while one was open for 0% of the time, Pallas kernels for 7%

profile of v11, /device:TPU:2, one launch (start us, length us, event | category | flops | bytes accessed | tf_op | source)
XLA Modules:
  0.0 122.2 jit_solution(6206727550556038667)
XLA Ops:
  7.2 0.0 all-gather.4.cloned.1.call-start
  7.2 2.3 %pack.1 = (bf16[64,1024]{1,0:T(8,128)(2,1)}, bf16[80,512]{1,0:T(8,128)(2,1)S(1)}, bf16[64,16,128]{2,1,0:T(8,128)(2,1)}) custom-call(bf16[16,128]{1,0:T(8,128)(2,1)} %residual.1, bf16[64,128]{1,0:T(8,128)(2,1)} %wq.1, bf16[64,128]{1,0:T(8,128)(2,1)} %wf.1, bf16[64,128]{1,0:T(8,128)(2,1)} %wv.1, bf16[64,128]{1,0:T(8,128)(2,1)} %wg.1, ...), custom_call_target="tpu_custom_call" | custom-call | tf_op jit(solution)/shard_map/pack/pallas_call | solution.py:83
  9.5 0.0 all-gather.4.cloned.1.call-update
  9.6 10.0 %all-to-all-start = ((bf16[64,16,128]{2,1,0:T(8,128)(2,1)}), bf16[64,16,128]{2,1,0:T(8,128)(2,1)S(1)}, u32[]{:S(2)}, u32[]{:S(2)}) async-start(bf16[64,16,128]{2,1,0:T(8,128)(2,1)} %get-tuple-element.12), calls=%async_computation | async-start | bytes 524288 | tf_op jit(solution)/shard_map/all_to_all | solution.py:22
  19.5 35.6 %all-gather = bf16[640,512]{1,0:T(8,128)(2,1)S(1)} all-gather(bf16[80,512]{1,0:T(8,128)(2,1)S(1)} %get-tuple-element.13), channel_id=2, replica_groups={{0,5,8,13,16,21,24,29},{1,4,9,12,17,20,25,28},{2,7,10,15,18,23,26,31},{..., dimensions={0}, use_global_device_ids=true | all-gather | bytes 737280 | tf_op jit(solution)/shard_map/all_gather | solution.py:435
  55.1 0.0 all-to-all-done
  55.1 1.7 %project.1 = (bf16[4,16,512]{2,1,0:T(8,128)(2,1)}, bf16[512,128]{1,0:T(8,128)(2,1)S(1)}) custom-call(bf16[16,4,16,128]{3,2,1,0:T(8,128)(2,1)S(1)} %bitcast.17, f32[16,128]{1,0:T(8,128)} %bitcast.26, bf16[8,80,512]{2,1,0:T(8,128)(2,1)S(1)} %bitcast.16), custom_call_target="tpu_custom_call" | custom-call | tf_op jit(solution)/shard_map/project/pallas_call | solution.py:143
  56.8 3.7 %all-to-all-start.1 = ((bf16[4,16,512]{2,1,0:T(8,128)(2,1)}), bf16[4,16,512]{2,1,0:T(8,128)(2,1)S(1)}, u32[]{:S(2)}, u32[]{:S(2)}) async-start(bf16[4,16,512]{2,1,0:T(8,128)(2,1)} %get-tuple-element.14), calls=%async_computation.1 | async-start | bytes 131072 | tf_op jit(solution)/shard_map/all_to_all | solution.py:22
  60.6 10.2 %all-gather.1 = bf16[2048,128]{1,0:T(8,128)(2,1)S(1)} all-gather(bf16[512,128]{1,0:T(8,128)(2,1)S(1)} %get-tuple-element.16), channel_id=3, replica_groups=mesh['y'=4,'x'=4,'zh'=8,'zo'=2,'c'=2] {'zo','c'}, dimensions={0}, use_global_device_ids=true | all-gather | bytes 655360 | tf_op jit(solution)/shard_map/all_gather | solution.py:441
  70.8 0.0 all-to-all-done.1.part_ref
  70.8 2.4 %read_out.1 = (bf16[16,128]{1,0:T(8,128)(2,1)S(1)}, f32[16,512]{1,0:T(8,128)S(1)}) custom-call(bf16[4,16,512]{2,1,0:T(8,128)(2,1)S(1)} %all-to-all-done.1.part_ref, f32[16,128,128]{2,1,0:T(8,128)} %bitcast.21, f32[1,128]{1,0:T(1,128)} %bitcast.30, f32[1,128]{1,0:T(1,128)} %bitcast.32), custom_call_target="tpu_custom_call" | custom-call | tf_op jit(solution)/shard_map/read_out/pallas_call | solution.py:189
  73.2 0.4 mix_out.1
  73.6 13.6 %all_to_all.25.sums_ref = bf16[16,16,128]{2,1,0:T(8,128)(2,1)S(1)} all-to-all(bf16[16,16,128]{2,1,0:T(8,128)(2,1)S(1)} %mix_out.1), channel_id=1, replica_groups=mesh['y'=4,'x'=4,'zh'=8,'zo'=2,'c'=2] {'y','x'}, dimensions={0} | all-to-all | bytes 131072 | tf_op jit(solution)/shard_map/all_to_all | solution.py:22
  87.2 0.9 row_update.1
  88.1 10.8 %all_to_all.26.row_ref = bf16[16,16,128]{2,1,0:T(8,128)(2,1)S(1)} all-to-all(bf16[16,16,128]{2,1,0:T(8,128)(2,1)S(1)} %row_update.1), channel_id=1, replica_groups=mesh['y'=4,'x'=4,'zh'=8,'zo'=2,'c'=2] {'y','x'}, dimensions={0} | all-to-all | bytes 131072 | tf_op jit(solution)/shard_map/all_to_all | solution.py:22
  98.9 0.0 all-gather.4.cloned.1.call-done.long_ref
  98.9 4.7 %mlp.1 = (bf16[16,16,128]{2,1,0:T(8,128)(2,1)}, f32[16,128]{1,0:T(8,128)S(1)}, f32[1,128]{1,0:T(1,128)S(1)}) custom-call(bf16[16,16,128]{2,1,0:T(8,128)(2,1)S(1)} %all_to_all.26.row_ref, f32[16,128]{1,0:T(8,128)} %bitcast.27, f32[16,128]{1,0:T(8,128)} %bitcast.28, bf16[2048,1024]{1,0:T(8,128)(2,1)} %all-gather.4.cloned.1.call-done.long_ref), custom_call_target="tpu_custom_call" | custom-call | tf_op jit(solution)/shard_map/mlp/pallas_call | solution.py:379
  103.6 4.7 %all-to-all-start.4 = ((bf16[16,16,128]{2,1,0:T(8,128)(2,1)}), bf16[16,16,128]{2,1,0:T(8,128)(2,1)S(1)}, u32[]{:S(2)}, u32[]{:S(2)}) async-start(bf16[16,16,128]{2,1,0:T(8,128)(2,1)} %get-tuple-element.19), calls=%async_computation.4 | async-start | bytes 131072 | tf_op jit(solution)/shard_map/all_to_all | solution.py:22
  108.4 3.2 %update.1 = f32[16,128,128]{2,1,0:T(8,128)} custom-call(f32[16,512]{1,0:T(8,128)S(1)} %get-tuple-element.21.pre_ref, f32[16,128,128]{2,1,0:T(8,128)} %bitcast.22, f32[1,128]{1,0:T(1,128)} %bitcast.31), custom_call_target="tpu_custom_call" | custom-call | tf_op jit(solution)/shard_map/update/pallas_call | solution.py:231
  111.6 3.2 %all-to-all-done.4 = bf16[16,16,128]{2,1,0:T(8,128)(2,1)S(1)} async-done(((bf16[16,16,128]{2,1,0:T(8,128)(2,1)}), bf16[16,16,128]{2,1,0:T(8,128)(2,1)S(1)}, u32[]{:S(2)}, u32[]{:S(2)}) %all-to-all-start.4) | async-done | bytes 65568 | tf_op jit(solution)/shard_map/all_to_all | solution.py:22
  114.7 0.6 add_convert_fusion
  (1 shorter events, 0.0 us)
Async XLA Ops:
  7.2 91.8 %all-gather.4.cloned.1.call-start = ((), (), s32[]{:S(2)}) async-start(), calls=%async_computation.5 | async-start | bytes 4325376 | tf_op jit(solution)/shard_map/all_gather | solution.py:433
  9.6 45.5 %all-to-all-start = ((bf16[64,16,128]{2,1,0:T(8,128)(2,1)}), bf16[64,16,128]{2,1,0:T(8,128)(2,1)S(1)}, u32[]{:S(2)}, u32[]{:S(2)}) async-start(bf16[64,16,128]{2,1,0:T(8,128)(2,1)} %get-tuple-element.12), calls=%async_computation | async-start | bytes 524288 | tf_op jit(solution)/shard_map/all_to_all | solution.py:22
  56.8 13.9 %all-to-all-start.1 = ((bf16[4,16,512]{2,1,0:T(8,128)(2,1)}), bf16[4,16,512]{2,1,0:T(8,128)(2,1)S(1)}, u32[]{:S(2)}, u32[]{:S(2)}) async-start(bf16[4,16,512]{2,1,0:T(8,128)(2,1)} %get-tuple-element.14), calls=%async_computation.1 | async-start | bytes 131072 | tf_op jit(solution)/shard_map/all_to_all | solution.py:22
  103.6 11.1 %all-to-all-start.4 = ((bf16[16,16,128]{2,1,0:T(8,128)(2,1)}), bf16[16,16,128]{2,1,0:T(8,128)(2,1)S(1)}, u32[]{:S(2)}, u32[]{:S(2)}) async-start(bf16[16,16,128]{2,1,0:T(8,128)(2,1)} %get-tuple-element.19), calls=%async_computation.4 | async-start | bytes 131072 | tf_op jit(solution)/shard_map/all_to_all | solution.py:22
Sparse Core Ops, SparseCore 0:
  10.1 80.9 all-gather.3

commit v12 on v10

--- a/solution.py
+++ b/solution.py
@@ -12,8 +12,8 @@
 PARTS = 4
 CHIPS = 8
 RINGS = [[2 * zh + (zh + g) % 2 for zh in range(CHIPS)] for g in range(2)]
-SLAB = 4
-PIECES = 4
+SLAB = 8
+PIECES = 2
 
 epsilon = 1e-06
 
@@ -99,7 +99,7 @@
     )(residual, wq, wf, wv, wg, mix, up, down)
 
 
-def project_body(x_ref, gain_ref, short_ref, out_ref, mix_ref):
+def project_body(x_ref, gain_ref, short_ref, out, mix_ref, out_ref, sem):
     zo = lax.axis_index("zo")
     ring = lax.axis_index("c") + lax.axis_index("zh")
     groups, _, height, width = x_ref.shape
@@ -131,21 +131,30 @@
         w = jnp.concatenate([short_ref[k, :rows]] * 2, axis=0)
         term = jnp.dot(x, w, preferred_element_type=jnp.float32)
         total = term if total is None else total + term
+    for h in range(PARTS):
+        out_ref[h] = total[h * height : (h + 1) * height].astype(out_ref.dtype)
+    send = pltpu.make_async_copy(out_ref, out, sem)
+    send.start()
+    for k in range(CHIPS):
         for j in range(4):
             mix_ref[k * rows + j * (rows // 4) : k * rows + (j + 1) * (rows // 4)] = (
                 short_ref[k, rows:, j * width : (j + 1) * width]
             )
-    for h in range(PARTS):
-        out_ref[h] = total[h * height : (h + 1) * height].astype(out_ref.dtype)
+    send.wait()
 
 
 def project(x, gain, short):
+    vmem = pl.BlockSpec(memory_space=pltpu.VMEM)
+    part = (PARTS, x.shape[2], short.shape[2])
     return pl.pallas_call(
         project_body,
         out_shape=(
-            pltpu.VMEM((PARTS, x.shape[2], short.shape[2]), jnp.bfloat16),
+            jax.ShapeDtypeStruct(part, jnp.bfloat16),
             pltpu.VMEM((CHIPS * x.shape[3] // 2, x.shape[3]), jnp.bfloat16),
         ),
+        in_specs=[vmem] * 3,
+        out_specs=(pl.BlockSpec(memory_space=pl.ANY), vmem),
+        scratch_shapes=[pltpu.VMEM(part, jnp.bfloat16), pltpu.SemaphoreType.DMA(())],
         name="project",
     )(near(x), gain, near(short))
 

time: 122 us -> 122 us (level)
  no operation moved by 1% of the time
where the time goes in v12:
time: 122 us
  blocking collectives  70.2 us (58%)
  starting transfers between devices  18.5 us (15%)
  Pallas kernels  15 us (12%)
  between operations  14.1 us (12%)
  waiting for transfers between devices  3.16 us (3%)
    all_gather x1, blocking collectives, shards(): short = lax.all_gather(short, ('zh', 'c'), axis=0, axis_index_groups=RINGS)  35.6 us
    all_to_all x2, blocking collectives, exchange(): return lax.all_to_all(blocks, axes, 0, 0, tiled=True)  24.5 us
    all_to_all x3, starting transfers between devices, exchange(): return lax.all_to_all(blocks, axes, 0, 0, tiled=True)  18.5 us
    all_gather x1, blocking collectives, shards(): mix = lax.all_gather(mix, NEAR, axis=0)  10.2 us
    pallas_call x1, Pallas kernels, mlp(): pl.pallas_call(mlp_body, out_shape=(pltpu.VMEM((groups, rows, width), jnp...  4.12 us
    pallas_call x1, Pallas kernels, update(): pl.pallas_call(update_body, out_shape=jax.ShapeDtypeStruct(prior.shape, j...  3.22 us
    all_to_all x3, waiting for transfers between devices, exchange(): return lax.all_to_all(blocks, axes, 0, 0, tiled=True)  3.15 us
  transfers between devices with their start and end apart: 4, of which 1 were waited for; matrix products, arithmetic and copies ran while one was open for 0% of the time, Pallas kernels for 7%

profile of v12, /device:TPU:2, one launch (start us, length us, event | category | flops | bytes accessed | tf_op | source)
XLA Modules:
  0.0 121.6 jit_solution(11462035011895273160)
XLA Ops:
  7.2 0.0 all-gather.4.cloned.1.call-start
  7.2 2.3 %pack.1 = (bf16[64,1024]{1,0:T(8,128)(2,1)}, bf16[80,512]{1,0:T(8,128)(2,1)S(1)}, bf16[64,16,128]{2,1,0:T(8,128)(2,1)}) custom-call(bf16[16,128]{1,0:T(8,128)(2,1)} %residual.1, bf16[64,128]{1,0:T(8,128)(2,1)} %wq.1, bf16[64,128]{1,0:T(8,128)(2,1)} %wf.1, bf16[64,128]{1,0:T(8,128)(2,1)} %wv.1, bf16[64,128]{1,0:T(8,128)(2,1)} %wg.1, ...), custom_call_target="tpu_custom_call" | custom-call | tf_op jit(solution)/shard_map/pack/pallas_call | solution.py:83
  9.5 0.0 all-gather.4.cloned.1.call-update
  9.6 10.0 %all-to-all-start = ((bf16[64,16,128]{2,1,0:T(8,128)(2,1)}), bf16[64,16,128]{2,1,0:T(8,128)(2,1)S(1)}, u32[]{:S(2)}, u32[]{:S(2)}) async-start(bf16[64,16,128]{2,1,0:T(8,128)(2,1)} %get-tuple-element.12), calls=%async_computation | async-start | bytes 524288 | tf_op jit(solution)/shard_map/all_to_all | solution.py:22
  19.5 35.6 %all-gather = bf16[640,512]{1,0:T(8,128)(2,1)S(1)} all-gather(bf16[80,512]{1,0:T(8,128)(2,1)S(1)} %get-tuple-element.13), channel_id=2, replica_groups={{0,5,8,13,16,21,24,29},{1,4,9,12,17,20,25,28},{2,7,10,15,18,23,26,31},{..., dimensions={0}, use_global_device_ids=true | all-gather | bytes 737280 | tf_op jit(solution)/shard_map/all_gather | solution.py:425
  55.1 0.0 all-to-all-done
  55.1 1.7 %project.1 = (bf16[4,16,512]{2,1,0:T(8,128)(2,1)}, bf16[512,128]{1,0:T(8,128)(2,1)S(1)}) custom-call(bf16[16,4,16,128]{3,2,1,0:T(8,128)(2,1)S(1)} %bitcast.17, f32[16,128]{1,0:T(8,128)} %bitcast.26, bf16[8,80,512]{2,1,0:T(8,128)(2,1)S(1)} %bitcast.16), custom_call_target="tpu_custom_call" | custom-call | tf_op jit(solution)/shard_map/project/pallas_call | solution.py:149
  56.9 3.7 %all-to-all-start.1 = ((bf16[4,16,512]{2,1,0:T(8,128)(2,1)}), bf16[4,16,512]{2,1,0:T(8,128)(2,1)S(1)}, u32[]{:S(2)}, u32[]{:S(2)}) async-start(bf16[4,16,512]{2,1,0:T(8,128)(2,1)} %get-tuple-element.14), calls=%async_computation.1 | async-start | bytes 131072 | tf_op jit(solution)/shard_map/all_to_all | solution.py:22
  60.6 10.2 %all-gather.1 = bf16[2048,128]{1,0:T(8,128)(2,1)S(1)} all-gather(bf16[512,128]{1,0:T(8,128)(2,1)S(1)} %get-tuple-element.16), channel_id=3, replica_groups=mesh['y'=4,'x'=4,'zh'=8,'zo'=2,'c'=2] {'zo','c'}, dimensions={0}, use_global_device_ids=true | all-gather | bytes 655360 | tf_op jit(solution)/shard_map/all_gather | solution.py:431
  70.8 0.0 all-to-all-done.1.part_ref
  70.8 2.3 %read_out.1 = (bf16[16,128]{1,0:T(8,128)(2,1)S(1)}, f32[16,512]{1,0:T(8,128)S(1)}) custom-call(bf16[4,16,512]{2,1,0:T(8,128)(2,1)S(1)} %all-to-all-done.1.part_ref, f32[16,128,128]{2,1,0:T(8,128)} %bitcast.21, f32[1,128]{1,0:T(1,128)} %bitcast.30, f32[1,128]{1,0:T(1,128)} %bitcast.32), custom_call_target="tpu_custom_call" | custom-call | tf_op jit(solution)/shard_map/read_out/pallas_call | solution.py:198
  73.1 0.4 mix_out.1
  73.5 13.7 %all_to_all.25.sums_ref = bf16[16,16,128]{2,1,0:T(8,128)(2,1)S(1)} all-to-all(bf16[16,16,128]{2,1,0:T(8,128)(2,1)S(1)} %mix_out.1), channel_id=1, replica_groups=mesh['y'=4,'x'=4,'zh'=8,'zo'=2,'c'=2] {'y','x'}, dimensions={0} | all-to-all | bytes 131072 | tf_op jit(solution)/shard_map/all_to_all | solution.py:22
  87.2 0.9 row_update.1
  88.1 10.8 %all_to_all.26.row_ref = bf16[16,16,128]{2,1,0:T(8,128)(2,1)S(1)} all-to-all(bf16[16,16,128]{2,1,0:T(8,128)(2,1)S(1)} %row_update.1), channel_id=1, replica_groups=mesh['y'=4,'x'=4,'zh'=8,'zo'=2,'c'=2] {'y','x'}, dimensions={0} | all-to-all | bytes 131072 | tf_op jit(solution)/shard_map/all_to_all | solution.py:22
  98.9 0.0 all-gather.4.cloned.1.call-done.long_ref
  98.9 4.1 %mlp.1 = (bf16[16,16,128]{2,1,0:T(8,128)(2,1)}, f32[16,128]{1,0:T(8,128)S(1)}, f32[1,128]{1,0:T(1,128)S(1)}) custom-call(bf16[16,16,128]{2,1,0:T(8,128)(2,1)S(1)} %all_to_all.26.row_ref, f32[16,128]{1,0:T(8,128)} %bitcast.27, f32[16,128]{1,0:T(8,128)} %bitcast.28, bf16[2048,1024]{1,0:T(8,128)(2,1)} %all-gather.4.cloned.1.call-done.long_ref), custom_call_target="tpu_custom_call" | custom-call | tf_op jit(solution)/shard_map/mlp/pallas_call | solution.py:373
  103.0 4.7 %all-to-all-start.4 = ((bf16[16,16,128]{2,1,0:T(8,128)(2,1)}), bf16[16,16,128]{2,1,0:T(8,128)(2,1)S(1)}, u32[]{:S(2)}, u32[]{:S(2)}) async-start(bf16[16,16,128]{2,1,0:T(8,128)(2,1)} %get-tuple-element.19), calls=%async_computation.4 | async-start | bytes 131072 | tf_op jit(solution)/shard_map/all_to_all | solution.py:22
  107.8 3.2 %update.1 = f32[16,128,128]{2,1,0:T(8,128)} custom-call(f32[16,512]{1,0:T(8,128)S(1)} %get-tuple-element.21.pre_ref, f32[16,128,128]{2,1,0:T(8,128)} %bitcast.22, f32[1,128]{1,0:T(1,128)} %bitcast.31), custom_call_target="tpu_custom_call" | custom-call | tf_op jit(solution)/shard_map/update/pallas_call | solution.py:240
  111.0 3.1 %all-to-all-done.4 = bf16[16,16,128]{2,1,0:T(8,128)(2,1)S(1)} async-done(((bf16[16,16,128]{2,1,0:T(8,128)(2,1)}), bf16[16,16,128]{2,1,0:T(8,128)(2,1)S(1)}, u32[]{:S(2)}, u32[]{:S(2)}) %all-to-all-start.4) | async-done | bytes 65568 | tf_op jit(solution)/shard_map/all_to_all | solution.py:22
  114.2 0.6 add_convert_fusion
  (1 shorter events, 0.0 us)
Async XLA Ops:
  7.2 91.7 %all-gather.4.cloned.1.call-start = ((), (), s32[]{:S(2)}) async-start(), calls=%async_computation.5 | async-start | bytes 4325376 | tf_op jit(solution)/shard_map/all_gather | solution.py:423
  9.6 45.5 %all-to-all-start = ((bf16[64,16,128]{2,1,0:T(8,128)(2,1)}), bf16[64,16,128]{2,1,0:T(8,128)(2,1)S(1)}, u32[]{:S(2)}, u32[]{:S(2)}) async-start(bf16[64,16,128]{2,1,0:T(8,128)(2,1)} %get-tuple-element.12), calls=%async_computation | async-start | bytes 524288 | tf_op jit(solution)/shard_map/all_to_all | solution.py:22
  56.9 13.9 %all-to-all-start.1 = ((bf16[4,16,512]{2,1,0:T(8,128)(2,1)}), bf16[4,16,512]{2,1,0:T(8,128)(2,1)S(1)}, u32[]{:S(2)}, u32[]{:S(2)}) async-start(bf16[4,16,512]{2,1,0:T(8,128)(2,1)} %get-tuple-element.14), calls=%async_computation.1 | async-start | bytes 131072 | tf_op jit(solution)/shard_map/all_to_all | solution.py:22
  103.0 11.1 %all-to-all-start.4 = ((bf16[16,16,128]{2,1,0:T(8,128)(2,1)}), bf16[16,16,128]{2,1,0:T(8,128)(2,1)S(1)}, u32[]{:S(2)}, u32[]{:S(2)}) async-start(bf16[16,16,128]{2,1,0:T(8,128)(2,1)} %get-tuple-element.19), calls=%async_computation.4 | async-start | bytes 131072 | tf_op jit(solution)/shard_map/all_to_all | solution.py:22
Sparse Core Ops, SparseCore 0:
  10.1 80.9 all-gather.3

commit v13 on v12

--- a/solution.py
+++ b/solution.py
@@ -252,45 +252,52 @@
     )(near(pre), prior, floor)
 
 
-def mix_body(gated_ref, w_ref, out_ref, sums_ref):
-    zh = lax.axis_index("zh")
-    height, width = gated_ref.shape
-    rows = width // 2
-    left = gated_ref[...]
-    for k in range(CHIPS):
-        for zo in range(2):
-            right = jnp.concatenate(
-                [
-                    w_ref[2 * zo + lax.rem(c + zh + k, 2), k * rows : (k + 1) * rows]
-                    for c in range(2)
-                ],
-                axis=0,
+def mix_body(gated_ref, w_ref, out_ref, order_ref):
+    height, width = gated_ref.shape[1:]
+    pairs = CHIPS // 2
+    for c in range(2):
+        order_ref[pl.ds(c, height, stride=2)] = gated_ref[c].astype(jnp.float32)
+    left = order_ref[...].astype(jnp.bfloat16)
+    for zo in range(2):
+        for k in range(pairs):
+            out_ref[pl.ds(zo * pairs + k, 2 * height, stride=CHIPS)] = lax.dot_general(
+                left,
+                w_ref[zo, k * width : (k + 1) * width],
+                (((1,), (1,)), ((), ())),
+                preferred_element_type=jnp.float32,
             )
-            sums_ref[pl.ds(2 * k + zo, height, stride=2 * CHIPS)] = lax.dot_general(
-                left, right, (((1,), (1,)), ((), ())), preferred_element_type=jnp.float32
-            )
-    for row in range(height):
-        out_ref[row] = sums_ref[2 * CHIPS * row : 2 * CHIPS * (row + 1)].astype(
-            out_ref.dtype
-        )
 
 
 def mix_out(gated, weights):
-    height, width = gated.shape
+    height, width = gated.shape[1:]
     return pl.pallas_call(
         mix_body,
-        out_shape=pltpu.VMEM((height, 2 * CHIPS, width), jnp.bfloat16),
-        scratch_shapes=[pltpu.VMEM((2 * CHIPS * height, width), jnp.float32)],
+        out_shape=pltpu.VMEM((2 * CHIPS * height, width), jnp.float32),
+        scratch_shapes=[pltpu.VMEM((2 * height, width), jnp.float32)],
         name="mix_out",
     )(near(gated), near(weights))
 
 
-def row_body(sums_ref, x_ref, gain_ref, out_ref):
+def row_body(sums_ref, x_ref, gain_ref, out_ref, mixed_ref):
     own = 2 * lax.axis_index("zo") + lax.axis_index("c")
     place = lax.axis_index("y") * lax.axis_size("x") + lax.axis_index("x")
-    mixed = sums_ref[0].astype(jnp.float32)
-    for k in range(1, sums_ref.shape[0]):
-        mixed = mixed + sums_ref[k].astype(jnp.float32)
+    groups, width = gain_ref.shape
+    pairs = CHIPS // 2
+    total = sums_ref[:groups]
+    for k in range(1, groups):
+        total = total + sums_ref[k * groups : (k + 1) * groups]
+    first = lax.broadcasted_iota(jnp.int32, (pairs, width), 1) < width // 2
+    turned = lax.rem(lax.axis_index("zh"), 2) == 1
+    for h in range(2):
+        left = total[h * pairs : (h + 1) * pairs]
+        right = total[(2 + h) * pairs : (3 + h) * pairs]
+        zero = jnp.where(turned, right, left)
+        one = pltpu.roll(jnp.where(turned, left, right), width // 2, 1)
+        even = jnp.where(first, zero, one)
+        odd = jnp.where(first, one, zero)
+        mixed_ref[pl.ds(h, pairs, stride=4)] = even
+        mixed_ref[pl.ds(2 + h, pairs, stride=4)] = odd
+    mixed = mixed_ref[...]
     scale = lax.rsqrt(jnp.sum(mixed * mixed) / gain_ref.size + epsilon)
     stream = x_ref[:, own].astype(jnp.float32)
     at = lax.broadcasted_iota(jnp.int32, stream.shape, 1) == place
@@ -304,6 +311,7 @@
     return pl.pallas_call(
         row_body,
         out_shape=pltpu.VMEM((groups, groups, width), jnp.bfloat16),
+        scratch_shapes=[pltpu.VMEM((groups, width), jnp.float32)],
         name="row_update",
     )(near(sums), near(x), gain)
 
@@ -428,8 +436,10 @@
     prior = prior_state[:, 0]
     gated, pre = read_out(part, prior, forget_floor[None], group_gain[None])
     new_state = update(pre, prior, forget_floor[None])
-    mix = lax.all_gather(mix, NEAR, axis=0)
-    mixed = exchange(mix_out(gated, mix), KV)
+    mix = lax.all_gather(mix, "zo", axis=0)
+    gated = lax.all_gather(gated, "c", axis=0)
+    mixed = mix_out(gated, mix).reshape(2 * groups, CHIPS, own_cols)
+    mixed = exchange(mixed, (*KV, "c")).reshape(-1, own_cols)
     after_row = row_update(mixed, stream, gain_mix_post.reshape(groups, own_cols))
     channel_part, after_own, out_gain = mlp(
         exchange(after_row, KV),

time: 122 us -> 124 us (1.016)
  blocking collectives: 70.2 us -> 71.7 us
    all_gather x1 -> x2, blocking collectives: 10.2 us -> 11.1 us  [the longest x1 9.33 us: shards(): mix = lax.all_gather(mix, 'zo', axis=0)]
where the time goes in v13:
time: 124 us; the launch traced here: 123 us
  blocking collectives  71.7 us (58%)
  starting transfers between devices  18.5 us (15%)
  Pallas kernels  14.9 us (12%)
  between operations  14.1 us (11%)
  waiting for transfers between devices  3.16 us (3%)
    all_gather x1, blocking collectives, shards(): short = lax.all_gather(short, ('zh', 'c'), axis=0, axis_index_groups=RINGS)  35.6 us
    all_to_all x2, blocking collectives, exchange(): return lax.all_to_all(blocks, axes, 0, 0, tiled=True)  24.9 us
    all_to_all x3, starting transfers between devices, exchange(): return lax.all_to_all(blocks, axes, 0, 0, tiled=True)  18.5 us
    all_gather x1, blocking collectives, shards(): mix = lax.all_gather(mix, 'zo', axis=0)  9.33 us
    pallas_call x1, Pallas kernels, mlp(): pl.pallas_call(mlp_body, out_shape=(pltpu.VMEM((groups, rows, width), jnp...  4.12 us
    pallas_call x1, Pallas kernels, update(): pl.pallas_call(update_body, out_shape=jax.ShapeDtypeStruct(prior.shape, j...  3.22 us
    all_to_all x3, waiting for transfers between devices, exchange(): return lax.all_to_all(blocks, axes, 0, 0, tiled=True)  3.15 us
  transfers between devices with their start and end apart: 4, of which 1 were waited for; matrix products, arithmetic and copies ran while one was open for 0% of the time, Pallas kernels for 7%

profile of v13, /device:TPU:2, one launch (start us, length us, event | category | flops | bytes accessed | tf_op | source)
XLA Modules:
  0.0 122.9 jit_solution(407485090457337805)
XLA Ops:
  7.2 0.0 all-gather.5.cloned.1.call-start
  7.2 2.3 %pack.1 = (bf16[64,1024]{1,0:T(8,128)(2,1)}, bf16[80,512]{1,0:T(8,128)(2,1)S(1)}, bf16[64,16,128]{2,1,0:T(8,128)(2,1)}) custom-call(bf16[16,128]{1,0:T(8,128)(2,1)} %residual.1, bf16[64,128]{1,0:T(8,128)(2,1)} %wq.1, bf16[64,128]{1,0:T(8,128)(2,1)} %wf.1, bf16[64,128]{1,0:T(8,128)(2,1)} %wv.1, bf16[64,128]{1,0:T(8,128)(2,1)} %wg.1, ...), custom_call_target="tpu_custom_call" | custom-call | tf_op jit(solution)/shard_map/pack/pallas_call | solution.py:83
  9.5 0.0 all-gather.5.cloned.1.call-update
  9.6 10.0 %all-to-all-start = ((bf16[64,16,128]{2,1,0:T(8,128)(2,1)}), bf16[64,16,128]{2,1,0:T(8,128)(2,1)S(1)}, u32[]{:S(2)}, u32[]{:S(2)}) async-start(bf16[64,16,128]{2,1,0:T(8,128)(2,1)} %get-tuple-element.12), calls=%async_computation | async-start | bytes 524288 | tf_op jit(solution)/shard_map/all_to_all | solution.py:22
  19.5 35.6 %all-gather = bf16[640,512]{1,0:T(8,128)(2,1)S(1)} all-gather(bf16[80,512]{1,0:T(8,128)(2,1)S(1)} %get-tuple-element.13), channel_id=2, replica_groups={{0,5,8,13,16,21,24,29},{1,4,9,12,17,20,25,28},{2,7,10,15,18,23,26,31},{..., dimensions={0}, use_global_device_ids=true | all-gather | bytes 737280 | tf_op jit(solution)/shard_map/all_gather | solution.py:433
  55.1 0.0 all-to-all-done
  55.1 1.7 %project.1 = (bf16[4,16,512]{2,1,0:T(8,128)(2,1)}, bf16[512,128]{1,0:T(8,128)(2,1)S(1)}) custom-call(bf16[16,4,16,128]{3,2,1,0:T(8,128)(2,1)S(1)} %bitcast.20, f32[16,128]{1,0:T(8,128)} %bitcast.32, bf16[8,80,512]{2,1,0:T(8,128)(2,1)S(1)} %bitcast.19), custom_call_target="tpu_custom_call" | custom-call | tf_op jit(solution)/shard_map/project/pallas_call | solution.py:149
  56.9 3.7 %all-to-all-start.1 = ((bf16[4,16,512]{2,1,0:T(8,128)(2,1)}), bf16[4,16,512]{2,1,0:T(8,128)(2,1)S(1)}, u32[]{:S(2)}, u32[]{:S(2)}) async-start(bf16[4,16,512]{2,1,0:T(8,128)(2,1)} %get-tuple-element.14), calls=%async_computation.1 | async-start | bytes 131072 | tf_op jit(solution)/shard_map/all_to_all | solution.py:22
  60.6 9.3 %all-gather.2 = bf16[1024,128]{1,0:T(8,128)(2,1)S(1)} all-gather(bf16[512,128]{1,0:T(8,128)(2,1)S(1)} %get-tuple-element.16), channel_id=4, replica_groups=mesh['y'=4,'x'=4,'zh'=8,'zo'=2,'c'=2] {'zo'}, dimensions={0}, use_global_device_ids=true | all-gather | bytes 393216 | tf_op jit(solution)/shard_map/all_gather | solution.py:439
  69.9 0.0 all-to-all-done.1.part_ref
  69.9 2.3 %read_out.1 = (bf16[16,128]{1,0:T(8,128)(2,1)S(1)}, f32[16,512]{1,0:T(8,128)S(1)}) custom-call(bf16[4,16,512]{2,1,0:T(8,128)(2,1)S(1)} %all-to-all-done.1.part_ref, f32[16,128,128]{2,1,0:T(8,128)} %bitcast.27, f32[1,128]{1,0:T(1,128)} %bitcast.36, f32[1,128]{1,0:T(1,128)} %bitcast.38), custom_call_target="tpu_custom_call" | custom-call | tf_op jit(solution)/shard_map/read_out/pallas_call | solution.py:198
  72.2 1.8 %all-gather.1 = bf16[32,128]{1,0:T(8,128)(2,1)S(1)} all-gather(bf16[16,128]{1,0:T(8,128)(2,1)S(1)} %get-tuple-element.15), channel_id=3, replica_groups=mesh['y'=4,'x'=4,'zh'=8,'zo'=2,'c'=2] {'c'}, dimensions={0}, use_global_device_ids=true | all-gather | bytes 12288 | tf_op jit(solution)/shard_map/all_gather | solution.py:440
  74.0 0.2 mix_out.1
  74.3 14.1 %all_to_all.25 = f32[32,8,128]{2,1,0:T(8,128)S(1)} all-to-all(f32[32,8,128]{2,1,0:T(8,128)S(1)} %bitcast.23), channel_id=1, replica_groups=mesh['y'=4,'x'=4,'zh'=8,'zo'=2,'c'=2] {'y','x','c'}, dimensions={0} | all-to-all | bytes 262144 | tf_op jit(solution)/shard_map/all_to_all | solution.py:22
  88.4 1.0 row_update.1
  89.4 10.8 %all_to_all.26.row_ref = bf16[16,16,128]{2,1,0:T(8,128)(2,1)S(1)} all-to-all(bf16[16,16,128]{2,1,0:T(8,128)(2,1)S(1)} %row_update.1), channel_id=1, replica_groups=mesh['y'=4,'x'=4,'zh'=8,'zo'=2,'c'=2] {'y','x'}, dimensions={0} | all-to-all | bytes 131072 | tf_op jit(solution)/shard_map/all_to_all | solution.py:22
  100.2 0.0 all-gather.5.cloned.1.call-done.long_ref
  100.2 4.1 %mlp.1 = (bf16[16,16,128]{2,1,0:T(8,128)(2,1)}, f32[16,128]{1,0:T(8,128)S(1)}, f32[1,128]{1,0:T(1,128)S(1)}) custom-call(bf16[16,16,128]{2,1,0:T(8,128)(2,1)S(1)} %all_to_all.26.row_ref, f32[16,128]{1,0:T(8,128)} %bitcast.34, f32[16,128]{1,0:T(8,128)} %bitcast.35, bf16[2048,1024]{1,0:T(8,128)(2,1)} %all-gather.5.cloned.1.call-done.long_ref), custom_call_target="tpu_custom_call" | custom-call | tf_op jit(solution)/shard_map/mlp/pallas_call | solution.py:381
  104.3 4.7 %all-to-all-start.4 = ((bf16[16,16,128]{2,1,0:T(8,128)(2,1)}), bf16[16,16,128]{2,1,0:T(8,128)(2,1)S(1)}, u32[]{:S(2)}, u32[]{:S(2)}) async-start(bf16[16,16,128]{2,1,0:T(8,128)(2,1)} %get-tuple-element.19), calls=%async_computation.4 | async-start | bytes 131072 | tf_op jit(solution)/shard_map/all_to_all | solution.py:22
  109.1 3.2 %update.1 = f32[16,128,128]{2,1,0:T(8,128)} custom-call(f32[16,512]{1,0:T(8,128)S(1)} %get-tuple-element.21.pre_ref, f32[16,128,128]{2,1,0:T(8,128)} %bitcast.28, f32[1,128]{1,0:T(1,128)} %bitcast.37), custom_call_target="tpu_custom_call" | custom-call | tf_op jit(solution)/shard_map/update/pallas_call | solution.py:240
  112.3 3.1 %all-to-all-done.4 = bf16[16,16,128]{2,1,0:T(8,128)(2,1)S(1)} async-done(((bf16[16,16,128]{2,1,0:T(8,128)(2,1)}), bf16[16,16,128]{2,1,0:T(8,128)(2,1)S(1)}, u32[]{:S(2)}, u32[]{:S(2)}) %all-to-all-start.4) | async-done | bytes 65568 | tf_op jit(solution)/shard_map/all_to_all | solution.py:22
  115.5 0.6 add_convert_fusion
  (1 shorter events, 0.0 us)
Async XLA Ops:
  7.2 93.0 %all-gather.5.cloned.1.call-start = ((), (), s32[]{:S(2)}) async-start(), calls=%async_computation.5 | async-start | bytes 4325376 | tf_op jit(solution)/shard_map/all_gather | solution.py:431
  9.6 45.5 %all-to-all-start = ((bf16[64,16,128]{2,1,0:T(8,128)(2,1)}), bf16[64,16,128]{2,1,0:T(8,128)(2,1)S(1)}, u32[]{:S(2)}, u32[]{:S(2)}) async-start(bf16[64,16,128]{2,1,0:T(8,128)(2,1)} %get-tuple-element.12), calls=%async_computation | async-start | bytes 524288 | tf_op jit(solution)/shard_map/all_to_all | solution.py:22
  56.9 13.1 %all-to-all-start.1 = ((bf16[4,16,512]{2,1,0:T(8,128)(2,1)}), bf16[4,16,512]{2,1,0:T(8,128)(2,1)S(1)}, u32[]{:S(2)}, u32[]{:S(2)}) async-start(bf16[4,16,512]{2,1,0:T(8,128)(2,1)} %get-tuple-element.14), calls=%async_computation.1 | async-start | bytes 131072 | tf_op jit(solution)/shard_map/all_to_all | solution.py:22
  104.3 11.1 %all-to-all-start.4 = ((bf16[16,16,128]{2,1,0:T(8,128)(2,1)}), bf16[16,16,128]{2,1,0:T(8,128)(2,1)S(1)}, u32[]{:S(2)}, u32[]{:S(2)}) async-start(bf16[16,16,128]{2,1,0:T(8,128)(2,1)} %get-tuple-element.19), calls=%async_computation.4 | async-start | bytes 131072 | tf_op jit(solution)/shard_map/all_to_all | solution.py:22
Sparse Core Ops, SparseCore 0:
  10.1 80.9 all-gather.4

commit v14 on v12

--- a/solution.py
+++ b/solution.py
@@ -431,6 +431,7 @@
     mix = lax.all_gather(mix, NEAR, axis=0)
     mixed = exchange(mix_out(gated, mix), KV)
     after_row = row_update(mixed, stream, gain_mix_post.reshape(groups, own_cols))
+    after_row, new_state = lax.optimization_barrier((after_row, new_state))
     channel_part, after_own, out_gain = mlp(
         exchange(after_row, KV),
         gain_mlp_pre.reshape(groups, own_cols),

time: 122 us -> 122 us (level)
  starting transfers between devices: 18.5 us -> 21.3 us
  blocking collectives: 70.2 us -> 67.4 us
    all_to_all x2, blocking collectives: 24.5 us -> 21.6 us  [exchange(): return lax.all_to_all(blocks, axes, 0, 0, tiled=True)]
    all_to_all x3, starting transfers between devices: 18.5 us -> 21.3 us  [exchange(): return lax.all_to_all(blocks, axes, 0, 0, tiled=True)]
  transfers between devices with their start and end apart: 4 -> 4, of which waited for: 1 -> 1; matrix products, arithmetic and copies ran while one was open for 0% -> 0% of each run, Pallas kernels for 7% -> 8%
where the time goes in v14:
time: 122 us
  blocking collectives  67.4 us (55%)
  starting transfers between devices  21.3 us (17%)
  Pallas kernels  15 us (12%)
  between operations  14.1 us (12%)
  waiting for transfers between devices  3.08 us (3%)
    all_gather x1, blocking collectives, shards(): short = lax.all_gather(short, ('zh', 'c'), axis=0, axis_index_groups=RINGS)  35.6 us
    all_to_all x2, blocking collectives, exchange(): return lax.all_to_all(blocks, axes, 0, 0, tiled=True)  21.6 us
    all_to_all x3, starting transfers between devices, exchange(): return lax.all_to_all(blocks, axes, 0, 0, tiled=True)  21.3 us
    all_gather x1, blocking collectives, shards(): mix = lax.all_gather(mix, NEAR, axis=0)  10.2 us
    pallas_call x1, Pallas kernels, mlp(): pl.pallas_call(mlp_body, out_shape=(pltpu.VMEM((groups, rows, width), jnp...  3.5 us
    pallas_call x1, Pallas kernels, update(): pl.pallas_call(update_body, out_shape=jax.ShapeDtypeStruct(prior.shape, j...  3.24 us
    all_to_all x3, waiting for transfers between devices, exchange(): return lax.all_to_all(blocks, axes, 0, 0, tiled=True)  3.07 us
  transfers between devices with their start and end apart: 4, of which 1 were waited for; matrix products, arithmetic and copies ran while one was open for 0% of the time, Pallas kernels for 8%

profile of v14, /device:TPU:2, one launch (start us, length us, event | category | flops | bytes accessed | tf_op | source)
XLA Modules:
  0.0 121.5 jit_solution(3340540387628124091)
XLA Ops:
  7.2 0.0 all-gather.4.cloned.1.call-start
  7.2 2.3 %pack.1 = (bf16[64,1024]{1,0:T(8,128)(2,1)}, bf16[80,512]{1,0:T(8,128)(2,1)S(1)}, bf16[64,16,128]{2,1,0:T(8,128)(2,1)}) custom-call(bf16[16,128]{1,0:T(8,128)(2,1)} %residual.1, bf16[64,128]{1,0:T(8,128)(2,1)} %wq.1, bf16[64,128]{1,0:T(8,128)(2,1)} %wf.1, bf16[64,128]{1,0:T(8,128)(2,1)} %wv.1, bf16[64,128]{1,0:T(8,128)(2,1)} %wg.1, ...), custom_call_target="tpu_custom_call" | custom-call | tf_op jit(solution)/shard_map/pack/pallas_call | solution.py:83
  9.5 0.0 all-gather.4.cloned.1.call-update
  9.6 10.0 %all-to-all-start = ((bf16[64,16,128]{2,1,0:T(8,128)(2,1)}), bf16[64,16,128]{2,1,0:T(8,128)(2,1)S(1)}, u32[]{:S(2)}, u32[]{:S(2)}) async-start(bf16[64,16,128]{2,1,0:T(8,128)(2,1)} %get-tuple-element.14), calls=%async_computation | async-start | bytes 524288 | tf_op jit(solution)/shard_map/all_to_all | solution.py:22
  19.5 35.6 %all-gather = bf16[640,512]{1,0:T(8,128)(2,1)S(1)} all-gather(bf16[80,512]{1,0:T(8,128)(2,1)S(1)} %get-tuple-element.15), channel_id=2, replica_groups={{0,5,8,13,16,21,24,29},{1,4,9,12,17,20,25,28},{2,7,10,15,18,23,26,31},{..., dimensions={0}, use_global_device_ids=true | all-gather | bytes 737280 | tf_op jit(solution)/shard_map/all_gather | solution.py:425
  55.1 0.0 all-to-all-done
  55.1 1.7 %project.1 = (bf16[4,16,512]{2,1,0:T(8,128)(2,1)}, bf16[512,128]{1,0:T(8,128)(2,1)S(1)}) custom-call(bf16[16,4,16,128]{3,2,1,0:T(8,128)(2,1)S(1)} %bitcast.17, f32[16,128]{1,0:T(8,128)} %bitcast.26, bf16[8,80,512]{2,1,0:T(8,128)(2,1)S(1)} %bitcast.16), custom_call_target="tpu_custom_call" | custom-call | tf_op jit(solution)/shard_map/project/pallas_call | solution.py:149
  56.9 3.7 %all-to-all-start.1 = ((bf16[4,16,512]{2,1,0:T(8,128)(2,1)}), bf16[4,16,512]{2,1,0:T(8,128)(2,1)S(1)}, u32[]{:S(2)}, u32[]{:S(2)}) async-start(bf16[4,16,512]{2,1,0:T(8,128)(2,1)} %get-tuple-element.16), calls=%async_computation.1 | async-start | bytes 131072 | tf_op jit(solution)/shard_map/all_to_all | solution.py:22
  60.6 10.2 %all-gather.1 = bf16[2048,128]{1,0:T(8,128)(2,1)S(1)} all-gather(bf16[512,128]{1,0:T(8,128)(2,1)S(1)} %get-tuple-element.18), channel_id=3, replica_groups=mesh['y'=4,'x'=4,'zh'=8,'zo'=2,'c'=2] {'zo','c'}, dimensions={0}, use_global_device_ids=true | all-gather | bytes 655360 | tf_op jit(solution)/shard_map/all_gather | solution.py:431
  70.8 0.0 all-to-all-done.1.part_ref
  70.8 2.3 %read_out.1 = (bf16[16,128]{1,0:T(8,128)(2,1)S(1)}, f32[16,512]{1,0:T(8,128)S(1)}) custom-call(bf16[4,16,512]{2,1,0:T(8,128)(2,1)S(1)} %all-to-all-done.1.part_ref, f32[16,128,128]{2,1,0:T(8,128)} %bitcast.21, f32[1,128]{1,0:T(1,128)} %bitcast.30, f32[1,128]{1,0:T(1,128)} %bitcast.32), custom_call_target="tpu_custom_call" | custom-call | tf_op jit(solution)/shard_map/read_out/pallas_call | solution.py:198
  73.1 1.0 mix_out.1
  74.2 7.6 %all-to-all-start.2 = ((bf16[16,16,128]{2,1,0:T(8,128)(2,1)}), bf16[16,16,128]{2,1,0:T(8,128)(2,1)S(1)}, u32[]{:S(2)}, u32[]{:S(2)}) async-start(bf16[16,16,128]{2,1,0:T(8,128)(2,1)} %mix_out.1), calls=%async_computation.2 | async-start | bytes 131072 | tf_op jit(solution)/shard_map/all_to_all | solution.py:22
  81.7 3.2 %update.1 = f32[16,128,128]{2,1,0:T(8,128)} custom-call(f32[16,512]{1,0:T(8,128)S(1)} %get-tuple-element.19.pre_ref, f32[16,128,128]{2,1,0:T(8,128)} %bitcast.22, f32[1,128]{1,0:T(1,128)} %bitcast.31), custom_call_target="tpu_custom_call" | custom-call | tf_op jit(solution)/shard_map/update/pallas_call | solution.py:240
  85.0 3.1 %all-to-all-done.2.sums_ref = bf16[16,16,128]{2,1,0:T(8,128)(2,1)S(1)} async-done(((bf16[16,16,128]{2,1,0:T(8,128)(2,1)}), bf16[16,16,128]{2,1,0:T(8,128)(2,1)S(1)}, u32[]{:S(2)}, u32[]{:S(2)}) %all-to-all-start.2) | async-done | bytes 65568 | tf_op jit(solution)/shard_map/all_to_all | solution.py:22
  88.0 0.9 row_update.1
  88.9 10.8 %all_to_all.25.row_ref = bf16[16,16,128]{2,1,0:T(8,128)(2,1)S(1)} all-to-all(bf16[16,16,128]{2,1,0:T(8,128)(2,1)S(1)} %row_update.1), channel_id=1, replica_groups=mesh['y'=4,'x'=4,'zh'=8,'zo'=2,'c'=2] {'y','x'}, dimensions={0} | all-to-all | bytes 131072 | tf_op jit(solution)/shard_map/all_to_all | solution.py:22
  99.7 0.0 all-gather.4.cloned.1.call-done.long_ref
  99.7 3.5 %mlp.1 = (bf16[16,16,128]{2,1,0:T(8,128)(2,1)S(1)}, f32[16,128]{1,0:T(8,128)S(1)}, f32[1,128]{1,0:T(1,128)S(1)}) custom-call(bf16[16,16,128]{2,1,0:T(8,128)(2,1)S(1)} %all_to_all.25.row_ref, f32[16,128]{1,0:T(8,128)} %bitcast.27, f32[16,128]{1,0:T(8,128)} %bitcast.28, bf16[2048,1024]{1,0:T(8,128)(2,1)} %all-gather.4.cloned.1.call-done.long_ref), custom_call_target="tpu_custom_call" | custom-call | tf_op jit(solution)/shard_map/mlp/pallas_call | solution.py:373
  103.2 10.8 %all_to_all.26 = bf16[16,16,128]{2,1,0:T(8,128)(2,1)S(1)} all-to-all(bf16[16,16,128]{2,1,0:T(8,128)(2,1)S(1)} %get-tuple-element.23), channel_id=1, replica_groups=mesh['y'=4,'x'=4,'zh'=8,'zo'=2,'c'=2] {'y','x'}, dimensions={0} | all-to-all | bytes 131072 | tf_op jit(solution)/shard_map/all_to_all | solution.py:22
  114.1 0.6 add_convert_fusion
  (1 shorter events, 0.0 us)
Async XLA Ops:
  7.2 92.6 %all-gather.4.cloned.1.call-start = ((), (), s32[]{:S(2)}) async-start(), calls=%async_computation.5 | async-start | bytes 4325376 | tf_op jit(solution)/shard_map/all_gather | solution.py:423
  9.6 45.5 %all-to-all-start = ((bf16[64,16,128]{2,1,0:T(8,128)(2,1)}), bf16[64,16,128]{2,1,0:T(8,128)(2,1)S(1)}, u32[]{:S(2)}, u32[]{:S(2)}) async-start(bf16[64,16,128]{2,1,0:T(8,128)(2,1)} %get-tuple-element.14), calls=%async_computation | async-start | bytes 524288 | tf_op jit(solution)/shard_map/all_to_all | solution.py:22
  56.9 13.9 %all-to-all-start.1 = ((bf16[4,16,512]{2,1,0:T(8,128)(2,1)}), bf16[4,16,512]{2,1,0:T(8,128)(2,1)S(1)}, u32[]{:S(2)}, u32[]{:S(2)}) async-start(bf16[4,16,512]{2,1,0:T(8,128)(2,1)} %get-tuple-element.16), calls=%async_computation.1 | async-start | bytes 131072 | tf_op jit(solution)/shard_map/all_to_all | solution.py:22
  74.2 13.9 %all-to-all-start.2 = ((bf16[16,16,128]{2,1,0:T(8,128)(2,1)}), bf16[16,16,128]{2,1,0:T(8,128)(2,1)S(1)}, u32[]{:S(2)}, u32[]{:S(2)}) async-start(bf16[16,16,128]{2,1,0:T(8,128)(2,1)} %mix_out.1), calls=%async_computation.2 | async-start | bytes 131072 | tf_op jit(solution)/shard_map/all_to_all | solution.py:22
Sparse Core Ops, SparseCore 0:
  10.1 80.9 all-gather.3
